TPU v7x, 128 devices: a whole 4x4x4 slice. The times are simulated.
128 devices in a mesh: sp: 16 (over z, y), dp: 8 (over x, core).
Axes of the slice: x: 4, y: 4, z: 4, core: 2. Of those that a mesh axis runs over, the one named last changes fastest.
Arguments:
- residual: bfloat16 [8, 2048, 2048], P('dp', 'sp'), may hold values from -6 to 6
- query: bfloat16 [8, 2048, 16, 128], P('dp', 'sp'), may hold values from -6 to 6
- key_value: bfloat16 [8, 2048, 16, 128], P('dp', 'sp'), may hold values from -6 to 6
- out_weight: bfloat16 [2048, 2048], P(None, 'dp'), may hold values from -0.125 to 0.125
- norm_gain: float32 [2048], replicated, may hold values from 0.1 to 1.9
- query_gain: float32 [64], replicated, may hold values from 1.5 to 4.5
- key_gain: float32 [64], replicated, may hold values from 1.5 to 4.5
- route_ids: int32 [8, 2048, 4], P('dp', 'sp'), may hold values from 0 to 127, all different within a row; in each aligned block of 128 rows (0 to 127, 128 to 255, ..., all dimensions but the last counted through in order) at most 6 rows name the same one
- route_weights: float32 [8, 2048, 4], P('dp', 'sp'), may hold values from 0.2 to 1
- shared_gate: bfloat16 [2048, 512], replicated, may hold values from -0.125 to 0.125
- shared_up: bfloat16 [2048, 512], replicated, may hold values from -0.125 to 0.125
- shared_down: bfloat16 [512, 2048], replicated, may hold values from -0.25 to 0.25
- expert_gate: bfloat16 [128, 2048, 512], P(('sp', 'dp')), may hold values from -0.125 to 0.125
- expert_up: bfloat16 [128, 2048, 512], P(('sp', 'dp')), may hold values from -0.125 to 0.125
- expert_down: bfloat16 [128, 512, 2048], P(('sp', 'dp')), may hold values from -0.25 to 0.25
Outputs:
- result: bfloat16 [8, 2048, 2048], P('dp', 'sp')
Inputs may be any that keep to these rules, and one draw needn't show every extreme that they name: `route_ids`: each row names 4 different experts. Among the rows of one device no expert is named more than 6 times, a bound that some block reaches.
All inputs are finite; a program needn't handle non-finite values.
Results may differ from a plain program's by a relative error of at most 0.014.
The roundings to bfloat16 on the way count: a program that leaves them out, or rounds other values in their place, can miss the bound.
Values may be sent and summed in bfloat16 or wider, within the bound.
No kernel may reach another device: no remote copies, remote signals or barrier semaphores. Data moves between devices by JAX's collectives and lax.ppermute only.
A program may use at most 128 MiB of HBM per device.

v0:
```python
import jax
import jax.numpy as jnp
from jax import lax
from jax.sharding import PartitionSpec as P

GRID_W = 64


norm_eps = 1e-06
rope_theta = 10000.0
routed_scale = 2.5


def rotate_half(values, position, half_width):
    inverse_freq = rope_theta ** (-jnp.arange(0, half_width, 2, dtype=jnp.float32) / half_width)
    angles = position.astype(jnp.float32)[:, None] * inverse_freq[None, :]
    angles = jnp.concatenate([angles, angles], axis=-1)
    cosine = jnp.cos(angles)[:, None, :]
    sine_part = jnp.sin(angles)[:, None, :]
    first_half, second = jnp.split(values, 2, axis=-1)
    turned = jnp.concatenate([-second, first_half], axis=-1)
    return values * cosine + turned * sine_part


def prepare(values, gain_vector, grid_row, grid_col):
    head_dim = values.shape[-1]
    floats = values.astype(jnp.float32)
    normed = floats * lax.rsqrt(jnp.mean(floats * floats, axis=-1, keepdims=True) + norm_eps)
    normed = normed * gain_vector
    half_width = head_dim // 2
    turned = jnp.concatenate(
        [
            rotate_half(normed[..., :half_width], grid_row, half_width),
            rotate_half(normed[..., half_width:], grid_col, half_width),
        ],
        axis=-1,
    )
    return turned.astype(jnp.bfloat16)


def attend(queries, key_rows, values):
    length, groups, repeats, head_dim = queries.shape
    block_rows = min(512, length)
    score_scale = head_dim ** (-0.5)

    def one_block(query_block):
        scores = (
            jnp.einsum("qgrd,kgd->grqk", query_block, key_rows, preferred_element_type=jnp.float32)
            * score_scale
        )
        row_max = jnp.max(scores, axis=-1, keepdims=True)
        weights = jnp.exp(scores - row_max)
        row_total = jnp.sum(weights, axis=-1, keepdims=True)
        rounded = weights.astype(jnp.bfloat16)
        mixed = (
            jnp.einsum("grqk,kgd->grqd", rounded, values, preferred_element_type=jnp.float32)
            / row_total
        )
        return jnp.transpose(mixed, (2, 0, 1, 3)).astype(jnp.bfloat16)

    blocks = queries.reshape(length // block_rows, block_rows, groups, repeats, head_dim)
    return lax.map(one_block, blocks).reshape(length, groups * repeats * head_dim)


def swiglu(row_block, gate_weight, up_weight, down_weight):
    gate_part = jnp.dot(row_block, gate_weight, preferred_element_type=jnp.float32)
    up_part = jnp.dot(row_block, up_weight, preferred_element_type=jnp.float32)
    hidden = (jax.nn.silu(gate_part) * up_part).astype(jnp.bfloat16)
    return jnp.dot(hidden, down_weight, preferred_element_type=jnp.float32)


def per_device(
    residual,
    query,
    key_value,
    out_weight,
    norm_gain,
    query_gain,
    key_gain,
    route_ids,
    route_weights,
    shared_gate,
    shared_up,
    shared_down,
    expert_gate,
    expert_up,
    expert_down,
):
    tokens = residual.shape[1]
    model_width = residual.shape[2]
    head_dim = key_value.shape[3] // 2
    head_rows, pair_rows = (
        lax.all_to_all(query, "sp", split_axis=2, concat_axis=1, tiled=True),
        lax.all_to_all(key_value, "sp", split_axis=2, concat_axis=1, tiled=True),
    )
    length = head_rows.shape[1]
    kv_local = head_rows.shape[2]
    repeats = head_rows.shape[3] // head_dim
    position = jnp.arange(length, dtype=jnp.int32)
    grid_row = position // GRID_W
    grid_col = position % GRID_W
    queries = prepare(
        head_rows[0].reshape(length, kv_local * repeats, head_dim), query_gain, grid_row, grid_col
    )
    queries = queries.reshape(length, kv_local, repeats, head_dim)
    key_rows = prepare(pair_rows[0][..., :head_dim], key_gain, grid_row, grid_col)
    values = pair_rows[0][..., head_dim:]
    attention = attend(queries, key_rows, values)
    returned_heads = lax.all_to_all(
        attention.reshape(1, length, kv_local, repeats * head_dim),
        "sp",
        split_axis=1,
        concat_axis=2,
        tiled=True,
    )
    flat_rows = returned_heads.reshape(tokens, -1)
    projected = jnp.dot(
        flat_rows,
        lax.all_gather(out_weight, "dp", axis=1, tiled=True),
        preferred_element_type=jnp.float32,
    )
    mixed = residual[0].astype(jnp.float32) + projected
    normed = mixed * lax.rsqrt(jnp.mean(mixed * mixed, axis=-1, keepdims=True) + norm_eps)
    normed = (normed * norm_gain).astype(jnp.bfloat16)
    shared = swiglu(normed, shared_gate, shared_up, shared_down)
    local_experts = expert_gate.shape[0]
    experts = local_experts * lax.axis_size(("sp", "dp"))
    top_count = route_ids.shape[2]
    slot_count = max(2, 3 * tokens * top_count // (2 * experts))
    route_list = route_ids[0].reshape(-1)
    raw_weights = route_weights[0]
    gate_values = (
        raw_weights / jnp.sum(raw_weights, axis=-1, keepdims=True) * routed_scale
    ).reshape(-1)
    hit_table = (route_list[:, None] == jnp.arange(experts, dtype=jnp.int32)[None, :]).astype(
        jnp.int32
    )
    slot_rank = jnp.sum((jnp.cumsum(hit_table, axis=0) - hit_table) * hit_table, axis=1)
    slot_place = route_list * slot_count + slot_rank
    outgoing = jnp.zeros((experts * slot_count, model_width), jnp.bfloat16)
    outgoing = outgoing.at[slot_place].set(jnp.repeat(normed, top_count, axis=0))
    outgoing = outgoing.reshape(experts, slot_count, model_width)
    arrived = lax.all_to_all(outgoing, ("sp", "dp"), split_axis=0, concat_axis=0, tiled=True)
    sources = arrived.shape[0] // local_experts
    slot_width = arrived.shape[1]
    grouped = arrived.reshape(sources, local_experts, slot_width, model_width)
    row_block = grouped[:, 0].reshape(-1, model_width)
    output = swiglu(row_block, expert_gate[0], expert_up[0], expert_down[0])
    results = [output.astype(jnp.bfloat16).reshape(sources, slot_width, model_width)]
    returned = lax.all_to_all(
        jnp.stack(results, axis=1).reshape(arrived.shape),
        ("sp", "dp"),
        split_axis=0,
        concat_axis=0,
        tiled=True,
    )
    gathered = returned.reshape(experts * slot_count, model_width)[slot_place]
    routed = jnp.sum(
        (gathered.astype(jnp.float32) * gate_values[:, None]).reshape(
            tokens, top_count, model_width
        ),
        axis=1,
    )
    combined = (mixed + shared + routed).astype(jnp.bfloat16)
    return combined.reshape(1, tokens, model_width)


def solution(mesh):
    in_specs = (
        P("dp", "sp", None),
        P("dp", "sp", None, None),
        P("dp", "sp", None, None),
        P(None, "dp"),
        P(),
        P(),
        P(),
        P("dp", "sp", None),
        P("dp", "sp", None),
        P(),
        P(),
        P(),
        P(("sp", "dp"), None, None),
        P(("sp", "dp"), None, None),
        P(("sp", "dp"), None, None),
    )
    out_specs = P("dp", "sp", None)
    return jax.shard_map(
        per_device, mesh=mesh, in_specs=in_specs, out_specs=out_specs, check_vma=False
    )
```

profile of v0, /device:TPU:1, one launch (start us, length us, event | category | flops | bytes accessed | tf_op | source)
XLA Modules:
  0.0 317.5 jit_solution(13781153775951942175)
XLA Ops:
  9.3 8.6 %all-to-all-start = ((bf16[1,128,16,128]{3,1,0,2:T(8,128)(2,1)}), bf16[1,128,16,128]{3,1,0,2:T(8,128)(2,1)S(1)}, u32[]{:S(2)}, u32[]{:S(2)}) async-start(bf16[1,128,16,128]{3,1,0,2:T(8,128)(2,1)} %copy.34), calls=%async_computation | async-start | bytes 1048576 | tf_op jit(solution)/shard_map/all_to_all | solution.py:93
  21.2 2.6 fusion.51
  23.7 4.6 %all-to-all-done = bf16[1,128,16,128]{3,1,0,2:T(8,128)(2,1)S(1)} async-done(((bf16[1,128,16,128]{3,1,0,2:T(8,128)(2,1)}), bf16[1,128,16,128]{3,1,0,2:T(8,128)(2,1)S(1)}, u32[]{:S(2)}, u32[]{:S(2)}) %all-to-all-start) | async-done | bytes 524320 | tf_op jit(solution)/shard_map/all_to_all | solution.py:93
  29.1 4.2 %all-to-all-start.1 = ((bf16[1,128,16,128]{3,1,0,2:T(8,128)(2,1)}), bf16[1,128,16,128]{3,1,0,2:T(8,128)(2,1)}, u32[]{:S(2)}, u32[]{:S(2)}) async-start(bf16[1,128,16,128]{3,1,0,2:T(8,128)(2,1)} %copy.36), calls=%async_computation.1 | async-start | bytes 1048576 | tf_op jit(solution)/shard_map/all_to_all | solution.py:94
  39.5 3.5 %all-to-all-done.1 = bf16[1,128,16,128]{3,1,0,2:T(8,128)(2,1)} async-done(((bf16[1,128,16,128]{3,1,0,2:T(8,128)(2,1)}), bf16[1,128,16,128]{3,1,0,2:T(8,128)(2,1)}, u32[]{:S(2)}, u32[]{:S(2)}) %all-to-all-start.1) | async-done | bytes 524320 | tf_op jit(solution)/shard_map/all_to_all | solution.py:94
  43.0 2.3 fusion.85
  47.6 3.1 fusion.49
  50.8 18.8 %while.10 = (s32[]{:T(128)}, bf16[4,512,1,2,64]{1,4,3,2,0:T(8,128)(2,1)S(1)}, bf16[4,512,1,2,64]{1,4,3,2,0:T(8,128)(2,1)S(1)}, bf16[2048,1,64]{0,2,1:T(8,128)(2,1)S(1)}, bf16[2048,1,64]{0,2,1:T(8,128)(2,1)}, /*index=5*/s32[]{:T(128)}) while((s32[]{:T(128)}, bf16[4,512,1,2,64]{1,4,3,2,0:T(8,128)(2,1)S(1)}, ...), condition=%wide.region_5.6_spmd, body=%wide.region_2.5_spmd.sunk | while | flops 553777152 | bytes 27021416 | solution.py:62
  71.7 4.3 %reshape.587 = bf16[1,2048,1,128]{3,2,0,1:T(2,128)(2,1)S(1)} reshape(bf16[4,512,1,2,64]{4,3,1,0,2:T(2,128)(2,1)} %copy.49) | data formatting | bytes 1048576 | tf_op jit(solution)/shard_map/reshape;reshape | solution.py:110
  76.5 12.5 %reduce.4 = bf16[2048,128]{1,0:T(8,128)(2,1)} reduce(bf16[2048,1,1,128]{3,2,1,0:T(2,128)(2,1)S(1)} %bitcast.151, bf16[]{:T(256)} %broadcast.319), dimensions={1,2}, to_apply=%bitcast.116.reduce_sub_computation | reduce | bytes 1048578
  90.9 4.2 %all-to-all-start.2 = ((bf16[16,2,8192]{2,1,0:T(2,128)(2,1)}), bf16[16,2,8192]{2,1,0:T(2,128)(2,1)}, u32[]{:S(2)}, u32[]{:S(2)}) async-start(bf16[16,2,8192]{2,1,0:T(2,128)(2,1)} %reshape.590), calls=%async_computation.2 | async-start | bytes 1048576 | tf_op jit(solution)/shard_map/all_to_all | solution.py:109
  95.6 8.5 %all-to-all-done.2 = bf16[16,2,8192]{2,1,0:T(2,128)(2,1)} async-done(((bf16[16,2,8192]{2,1,0:T(2,128)(2,1)}), bf16[16,2,8192]{2,1,0:T(2,128)(2,1)}, u32[]{:S(2)}, u32[]{:S(2)}) %all-to-all-start.2) | async-done | bytes 524320 | tf_op jit(solution)/shard_map/all_to_all | solution.py:109
  104.2 2.2 reshape.591
  107.2 2.1 copy.42
  109.3 4.9 %multiply_reduce_fusion.1 = (f32[128]{0:T(128)S(1)}, f32[128,2048]{1,0:T(8,128)S(1)}) fusion(bf16[128,2048]{0,1:T(8,128)(2,1)} %bitcast.152, bf16[2048,2048]{1,0:T(8,128)(2,1)} %all-gather.2.cloned.1.call-done, bf16[1,128,2048]{2,1,0:T(8,128)(2,1)} %param.17), kind=kOutput, calls=%fused_computation.39 | convolution fusion | flops 1074790272 | bytes 10486272 | tf_op jit(solution)/shard_map/dot_general | solution.py:117
  115.3 2.4 broadcast_in_dim.11
  117.6 3.9 %reshape.581 = bf16[512,2048]{1,0:T(8,128)(2,1)} reshape(bf16[128,4,2048]{2,1,0:T(4,128)(2,1)} %broadcast_in_dim.11) | data formatting | bytes 4194304 | tf_op jit(solution)/shard_map/reshape | solution.py:141
  121.6 6.7 %scatter_custom_fusion = bf16[768,2048]{1,0:T(8,128)(2,1)} fusion(s32[512]{0:T(512)S(1)} %bitcast.158, bf16[512,2048]{1,0:T(8,128)(2,1)} %reshape.581, bf16[]{:T(256)} %constant.70.clone.1), kind=kCustom, calls=%fused_computation.33 | custom fusion | bytes 3146240 | tf_op jit(solution)/shard_map/scatter | solution.py:141
  128.3 6.2 %reshape.562 = bf16[128,6,2048]{2,1,0:T(8,128)(2,1)} reshape(bf16[768,2048]{1,0:T(8,128)(2,1)} %scatter_custom_fusion) | data formatting | bytes 6291456 | tf_op jit(solution)/shard_map/reshape | solution.py:142
  134.5 62.2 %all_to_all.49 = bf16[128,6,2048]{2,1,0:T(8,128)(2,1)} all-to-all(bf16[128,6,2048]{2,1,0:T(8,128)(2,1)} %reshape.562), channel_id=1, replica_groups=mesh['sp'=16,'dp'=8] {'sp','dp'}, dimensions={0} | all-to-all | bytes 6291456 | tf_op jit(solution)/shard_map/all_to_all | solution.py:143
  196.8 6.3 %reshape_squeeze_reshape.3 = bf16[768,2048]{1,0:T(8,128)(2,1)} reshape(bf16[128,6,2048]{2,1,0:T(8,128)(2,1)} %all_to_all.49) | data formatting | bytes 6291456 | tf_op jit(solution)/shard_map/reshape;squeeze;reshape | solution.py:147
  203.1 5.5 %fusion.31 = f32[768,512]{1,0:T(8,128)} fusion(bf16[768,2048]{1,0:T(8,128)(2,1)} %reshape_squeeze_reshape.3, bf16[1,2048,512]{2,1,0:T(8,128)(2,1)} %param.29), kind=kOutput, calls=%fused_computation.30 | convolution fusion | flops 1610612736 | bytes 6815744 | tf_op jit(solution)/shard_map/dot_general | solution.py:66
  208.6 8.2 %convolution_convert_fusion = bf16[768,2048]{1,0:T(8,128)(2,1)} fusion(bf16[1,512,2048]{2,1,0:T(8,128)(2,1)S(1)} %copy-done, f32[768,512]{1,0:T(8,128)} %fusion.31, bf16[768,2048]{1,0:T(8,128)(2,1)} %reshape_squeeze_reshape.3, bf16[1,2048,512]{2,1,0:T(8,128)(2,1)} %param.30), kind=kOutput, calls=%fused_computation.21 | convolution fusion | flops 3225157632 | bytes 12058624 | tf_op jit(solution)/shard_map/dot_general | solution.py:69
  216.7 6.3 %reshape_stack_reshape.3 = bf16[128,6,2048]{2,1,0:T(8,128)(2,1)} reshape(bf16[768,2048]{1,0:T(8,128)(2,1)} %convolution_convert_fusion) | data formatting | bytes 6291456 | tf_op jit(solution)/shard_map/reshape;stack;reshape | solution.py:151
  223.0 5.7 %all-to-all-start.4 = ((bf16[128,6,2048]{2,1,0:T(8,128)(2,1)}), bf16[128,6,2048]{2,1,0:T(8,128)(2,1)}, u32[]{:S(2)}, u32[]{:S(2)}) async-start(bf16[128,6,2048]{2,1,0:T(8,128)(2,1)} %reshape_stack_reshape.3), calls=%async_computation.4 | async-start | bytes 8388608 | tf_op jit(solution)/shard_map/all_to_all | solution.py:150
  228.8 2.2 fusion.86
  231.0 50.3 %all-to-all-done.4 = bf16[128,6,2048]{2,1,0:T(8,128)(2,1)} async-done(((bf16[128,6,2048]{2,1,0:T(8,128)(2,1)}), bf16[128,6,2048]{2,1,0:T(8,128)(2,1)}, u32[]{:S(2)}, u32[]{:S(2)}) %all-to-all-start.4) | async-done | bytes 3145760 | tf_op jit(solution)/shard_map/all_to_all | solution.py:150
  281.4 6.3 %reshape.563 = bf16[768,2048]{1,0:T(8,128)(2,1)} reshape(bf16[128,6,2048]{2,1,0:T(8,128)(2,1)} %all-to-all-done.4) | data formatting | bytes 6291456 | tf_op jit(solution)/shard_map/reshape | solution.py:157
  287.7 7.6 %gather_fusion = bf16[512,2048]{1,0:T(8,128)(2,1)} fusion(bf16[768,2048]{1,0:T(8,128)(2,1)} %reshape.563, s32[1024]{0:T(1024)S(1)} %pad_clamp_fusion), kind=kCustom, calls=%fused_computation | custom fusion | bytes 4196352 | tf_op jit(solution)/shard_map/gather | solution.py:157
  295.3 4.7 %reshape.567 = f32[128,4,2048]{2,1,0:T(4,128)} reshape(bf16[512,2048]{1,0:T(8,128)(2,1)} %gather_fusion) | data formatting | bytes 6291456 | tf_op jit(solution)/shard_map/convert_element_type | solution.py:159
  300.0 6.4 %multiply_reduce_fusion = f32[128,2048]{1,0:T(8,128)} fusion(f32[128,4,2048]{2,1,0:T(4,128)} %reshape.567, f32[128,4]{1,0:T(8,128)S(1)} %copy.48), kind=kLoop, calls=%fused_computation.20 | loop fusion | flops 1835008 | bytes 5244928 | tf_op jit(solution)/shard_map/reduce_sum | solution.py:158
  306.4 4.3 %fusion.27 = bf16[1,128,2048]{2,1,0:T(8,128)(2,1)} fusion(f32[128,2048]{1,0:T(8,128)} %multiply_reduce_fusion, f32[128,2048]{1,0:T(8,128)S(1)} %get-tuple-element.80, bf16[512,2048]{1,0:T(8,128)(2,1)} %param.28, bf16[128,2048]{1,0:T(8,128)(2,1)} %copy-done.1, bf16[2048,512]{1,0:T(8,128)(2,1)} %param.27, f32[128,512]{1,0:T(8,128)S(1)} %fusion.86), kind=kOutput, calls=%fused_computation.26 | convolution fusion | flops 538050560 | bytes 7602176 | tf_op jit(solution)/shard_map/dot_general | solution.py:69
  (103 shorter events, 40.8 us)
Async XLA Ops:
  6.5 202.0 %copy-start = (bf16[1,512,2048]{2,1,0:T(8,128)(2,1)S(1)}, bf16[1,512,2048]{2,1,0:T(8,128)(2,1)}, u32[]{:S(2)}) copy-start(bf16[1,512,2048]{2,1,0:T(8,128)(2,1)} %param.31) | copy-start | bytes 6291460
  6.5 11.4 %copy-start.11 = (s32[1,128,4]{1,2,0:T(4,128)S(1)}, s32[1,128,4]{1,2,0:T(4,128)}, u32[]{:S(2)}) copy-start(s32[1,128,4]{1,2,0:T(4,128)} %param.24) | copy-start | bytes 6148
  6.5 11.7 %copy-start.8 = (bf16[1,128,16,128]{3,2,1,0:T(8,128)(2,1)S(1)}, bf16[1,128,16,128]{3,2,1,0:T(8,128)(2,1)}, u32[]{:S(2)}) copy-start(bf16[1,128,16,128]{3,2,1,0:T(8,128)(2,1)} %param.19) | copy-start | bytes 1572868
  6.5 102.8 %all-gather.2.cloned.1.call-start = ((), (), s32[]{:S(2)}) async-start(), calls=%async_computation.5 | async-start | bytes 9437184 | tf_op jit(solution)/shard_map/all_gather | solution.py:119
  9.3 19.0 %all-to-all-start = ((bf16[1,128,16,128]{3,1,0,2:T(8,128)(2,1)}), bf16[1,128,16,128]{3,1,0,2:T(8,128)(2,1)S(1)}, u32[]{:S(2)}, u32[]{:S(2)}) async-start(bf16[1,128,16,128]{3,1,0,2:T(8,128)(2,1)} %copy.34), calls=%async_computation | async-start | bytes 1048576 | tf_op jit(solution)/shard_map/all_to_all | solution.py:93
  28.3 0.8 copy-start.2
  29.1 13.9 %all-to-all-start.1 = ((bf16[1,128,16,128]{3,1,0,2:T(8,128)(2,1)}), bf16[1,128,16,128]{3,1,0,2:T(8,128)(2,1)}, u32[]{:S(2)}, u32[]{:S(2)}) async-start(bf16[1,128,16,128]{3,1,0,2:T(8,128)(2,1)} %copy.36), calls=%async_computation.1 | async-start | bytes 1048576 | tf_op jit(solution)/shard_map/all_to_all | solution.py:94
  33.4 4.1 %copy-start.13 = (f32[64]{0:T(128)S(1)}, f32[64]{0:T(128)}, u32[]{:S(2)}) copy-start(f32[64]{0:T(128)} %param.22) | copy-start | bytes 772
  37.3 1.0 copy-start.3
  37.3 1.0 copy-start.4
  37.3 1.1 copy-start.5
  39.0 8.5 %copy-start.14 = (f32[64]{0:T(128)S(1)}, f32[64]{0:T(128)}, u32[]{:S(2)}) copy-start(f32[64]{0:T(128)} %param.23) | copy-start | bytes 772
  47.4 3.4 %copy-start.7 = (bf16[4,512,1,2,64]{1,4,3,2,0:T(8,128)(2,1)S(1)}, bf16[4,512,1,2,64]{1,4,3,2,0:T(8,128)(2,1)}, u32[]{:S(2)}) copy-start(bf16[4,512,1,2,64]{1,4,3,2,0:T(8,128)(2,1)} %custom-call.2) | copy-start | bytes 1572868
  52.2 1.7 copy-start.9
  56.9 1.7 copy-start.9
  61.6 1.6 copy-start.9
  66.3 1.6 copy-start.9
  71.7 23.7 %copy-start.6 = (s32[128,4,128]{0,2,1:T(8,128)S(1)}, s32[128,4,128]{0,2,1:T(8,128)}, u32[]{:S(2)}) copy-start(s32[128,4,128]{0,2,1:T(8,128)} %copy.47) | copy-start | bytes 786436
  90.9 13.2 %all-to-all-start.2 = ((bf16[16,2,8192]{2,1,0:T(2,128)(2,1)}), bf16[16,2,8192]{2,1,0:T(2,128)(2,1)}, u32[]{:S(2)}, u32[]{:S(2)}) async-start(bf16[16,2,8192]{2,1,0:T(2,128)(2,1)} %reshape.590), calls=%async_computation.2 | async-start | bytes 1048576 | tf_op jit(solution)/shard_map/all_to_all | solution.py:109
  109.3 5.0 %copy-start.10 = (f32[2048]{0:T(1024)S(1)}, f32[2048]{0:T(1024)}, u32[]{:S(2)}) copy-start(f32[2048]{0:T(1024)} %param.21) | copy-start | bytes 24580
  114.5 0.8 copy-start.1
  223.0 5.7 %copy-start.12 = (f32[1,128,4]{1,2,0:T(4,128)S(1)}, f32[1,128,4]{1,2,0:T(4,128)}, u32[]{:S(2)}) copy-start(f32[1,128,4]{1,2,0:T(4,128)} %param.25) | copy-start | bytes 6148
  223.0 58.4 %all-to-all-start.4 = ((bf16[128,6,2048]{2,1,0:T(8,128)(2,1)}), bf16[128,6,2048]{2,1,0:T(8,128)(2,1)}, u32[]{:S(2)}, u32[]{:S(2)}) async-start(bf16[128,6,2048]{2,1,0:T(8,128)(2,1)} %reshape_stack_reshape.3), calls=%async_computation.4 | async-start | bytes 8388608 | tf_op jit(solution)/shard_map/all_to_all | solution.py:150
Sparse Core Ops, SparseCore 0:
  9.0 57.0 all-gather.1
where the time goes:
time: 319 us; the launch traced here: 317 us
  local copies, waits for them, and re-layouts  78.9 us (25%)
  waiting for transfers between devices  67.6 us (21%)
  blocking collectives  62.2 us (19%)
  matrix products  37.2 us (12%)
  other arithmetic  35 us (11%)
  starting transfers between devices  22.7 us (7%)
  between operations  13.8 us (4%)
    all_to_all x1, blocking collectives, per_device(): lax.all_to_all(outgoing, ('sp', 'dp'), split_axis=0, concat_axis=0, tiled...  62.2 us
    all_to_all x1, waiting for transfers between devices, per_device(): lax.all_to_all(jnp.stack(results, axis=1).reshape(arrived.shape), ('sp',...  50.3 us
    unnamed x38, local copies, waits for them, and re-layouts  13.1 us
    unnamed x1, other arithmetic  12.5 us
    dot_general x2, matrix products, swiglu(): return jnp.dot(hidden, down_weight, preferred_element_type=jnp.float32)  12.5 us
    all_to_all x1, starting transfers between devices, per_device(): lax.all_to_all(query, 'sp', split_axis=2, concat_axis=1, tiled=True)  8.59 us
    all_to_all x1, waiting for transfers between devices, per_device(): lax.all_to_all(attention.reshape(1, length, kv_local, repeats * head_dim)...  8.51 us
    dot_general x2, matrix products, swiglu(): jnp.dot(row_block, gate_weight, preferred_element_type=jnp.float32)  7.69 us
  transfers between devices with their start and end apart: 5, of which 4 were waited for; matrix products, arithmetic and copies ran while one was open for 22% of the time, Pallas kernels for 0%

commit v1 on v0

v1 whole, which is shorter than its diff:
```python
import jax
import jax.numpy as jnp
import numpy as np
from jax import lax
from jax.experimental import pallas as pl
from jax.experimental.pallas import tpu as pltpu
from jax.sharding import PartitionSpec as P

GRID_W = 64
HD = 64
EPS = 1e-06
THETA = 10000.0
ROUTED_SCALE = 2.5
CAP = 6
PAIRS = CAP // 2
QUARTERS = 4
F32 = jnp.float32
BF16 = jnp.bfloat16


def iota(shape, axis):
    return lax.broadcasted_iota(jnp.int32, shape, axis)


def rotary_tables(query_gain, key_gain, first_token, tokens):
    lane = np.arange(128)
    half = (lane % HD) // 32
    freq = (THETA ** (-(2.0 * (lane % 16)) / 32.0)).astype(np.float32)
    position = first_token + jnp.arange(tokens, dtype=jnp.int32)
    row = (position // GRID_W).astype(F32)[:, None]
    col = (position % GRID_W).astype(F32)[:, None]
    angle = jnp.where(half[None, :] == 0, row, col) * freq[None, :]
    cosine, sine = jnp.cos(angle), jnp.sin(angle)
    lower = (lane % 32) < 16
    up, down = (lane + 16) % HD, (lane - 16) % HD

    def tables(gain, scale):
        pair = jnp.concatenate([gain, gain]) * scale
        return (
            pair[None, :] * cosine,
            jnp.where(lower, -gain[up] * scale, 0.0)[None, :] * sine,
            jnp.where(lower, 0.0, gain[down] * scale)[None, :] * sine,
        )

    is_key = (lane < HD)[None, :]
    q_own, q_up, q_down = tables(query_gain, HD**-0.5)
    k_own, k_up, k_down = tables(key_gain, 1.0)
    k_own = jnp.where(is_key, k_own, 1.0)
    k_up = jnp.where(is_key, k_up, 0.0)
    k_down = jnp.where(is_key, k_down, 0.0)
    return jnp.stack([q_own, q_up, q_down, k_own, k_up, k_down])


def prepare_kernel(q_ref, kv_ref, table_ref, out_ref):
    heads = q_ref.shape[0]
    block = (iota((128, 128), 0) // HD == iota((128, 128), 1) // HD).astype(F32).astype(BF16)
    is_key = iota((1, 128), 1) < HD

    def turned(x, base, keys):
        square = x * x
        high = square.astype(BF16)
        low = (square - high.astype(F32)).astype(BF16)
        total = jnp.dot(high, block, preferred_element_type=F32)
        total = total + jnp.dot(low, block, preferred_element_type=F32)
        scale = lax.rsqrt(total * (1.0 / HD) + EPS)
        if keys:
            scale = jnp.where(is_key, scale, 1.0)
        mixed = (
            x * table_ref[base]
            + pltpu.roll(x, 112, 1) * table_ref[base + 1]
            + pltpu.roll(x, 16, 1) * table_ref[base + 2]
        )
        return (mixed * scale).astype(BF16)

    for h in range(heads):
        out_ref[h, :, :128] = turned(q_ref[h].astype(F32), 0, False)
        out_ref[h, :, 128:] = turned(kv_ref[h].astype(F32), 3, True)


def prepare(query, pair, tables):
    heads, tokens, width = query.shape
    step = 4
    return pl.pallas_call(
        prepare_kernel,
        grid=(heads // step,),
        in_specs=[
            pl.BlockSpec((step, tokens, width), lambda i: (i, 0, 0)),
            pl.BlockSpec((step, tokens, width), lambda i: (i, 0, 0)),
            pl.BlockSpec(tables.shape, lambda i: (0, 0, 0)),
        ],
        out_specs=pl.BlockSpec((step, tokens, 2 * width), lambda i: (i, 0, 0)),
        out_shape=jax.ShapeDtypeStruct((heads, tokens, 2 * width), BF16),
        name="prepare",
    )(query, pair, tables)


def attend_kernel(q_ref, kv_ref, out_ref, keys_ref, values_ref):
    @pl.when(pl.program_id(0) == 0)
    def _():
        key = kv_ref[:, 128 : 128 + HD]
        value = kv_ref[:, 128 + HD :]
        keys_ref[...] = jnp.concatenate([key, key], axis=1)
        values_ref[...] = jnp.concatenate([value, value], axis=1)

    first = iota((1, 128), 1) < HD
    query = q_ref[...]
    outs = []
    for head in range(2):
        mine = jnp.where(first if head == 0 else ~first, query, jnp.zeros_like(query))
        scores = lax.dot_general(
            mine, keys_ref[...], (((1,), (1,)), ((), ())), preferred_element_type=F32
        )
        weights = jnp.exp(scores - jnp.max(scores, axis=-1, keepdims=True))
        total = jnp.sum(weights, axis=-1, keepdims=True)
        mixed = jnp.dot(weights.astype(BF16), values_ref[...], preferred_element_type=F32)
        outs.append(mixed / total)
    out_ref[...] = jnp.where(first, outs[0], outs[1]).astype(BF16)


def attend(rows):
    length, width = rows.shape
    block = 256
    return pl.pallas_call(
        attend_kernel,
        grid=(length // block,),
        in_specs=[
            pl.BlockSpec((block, 128), lambda i: (i, 0)),
            pl.BlockSpec((length, width), lambda i: (0, 0)),
        ],
        out_specs=pl.BlockSpec((block, 128), lambda i: (i, 0)),
        out_shape=jax.ShapeDtypeStruct((length, 128), BF16),
        scratch_shapes=[pltpu.VMEM((length, 128), BF16), pltpu.VMEM((length, 128), BF16)],
        name="attend",
    )(rows, rows)


def route_kernel(ids_ref, weights_ref, place_ref, gates_ref):
    tokens, top = ids_ref.shape
    experts = place_ref.shape[0] // CAP
    expert = iota((tokens, experts), 1)
    hits = [(ids_ref[:, k : k + 1] == expert).astype(F32) for k in range(top)]
    used = sum(hits[1:], hits[0])
    earlier = (iota((tokens, tokens), 1) < iota((tokens, tokens), 0)).astype(F32).astype(BF16)
    before = jnp.dot(earlier, used.astype(BF16), preferred_element_type=F32)
    raw = weights_ref[...]
    gate = raw / jnp.sum(raw, axis=-1, keepdims=True) * ROUTED_SCALE
    slots = iota((tokens, experts * CAP), 1)
    place = jnp.zeros((tokens, experts * CAP), F32)
    gated = jnp.zeros((tokens, experts * CAP), F32)
    for k in range(top):
        rank = jnp.sum(hits[k] * before, axis=-1, keepdims=True).astype(jnp.int32)
        slot = (rank // 2) * (2 * experts) + ids_ref[:, k : k + 1] * 2 + rank % 2
        here = slots == slot
        place = jnp.where(here, 1.0, place)
        gated = jnp.where(here, gate[:, k : k + 1], gated)
    place_ref[...] = jnp.transpose(place).astype(BF16)
    gates_ref[...] = gated


def route(ids, weights, experts):
    tokens, top = ids.shape
    return pl.pallas_call(
        route_kernel,
        out_shape=(
            jax.ShapeDtypeStruct((experts * CAP, tokens), BF16),
            jax.ShapeDtypeStruct((tokens, experts * CAP), F32),
        ),
        name="route",
    )(ids, weights)


def wire_permutation(transposed):
    wire = iota((128, 128), 1 if transposed else 0)
    flat = iota((128, 128), 0 if transposed else 1)
    source = (wire // 2 % QUARTERS) * 32 + (wire // 8) * 2 + wire % 2
    return (flat == source).astype(F32).astype(BF16)


def fold(rows, write):
    permute = wire_permutation(False)
    part = rows.shape[1] // QUARTERS
    for g in range(rows.shape[0] // 32):
        stacked = jnp.concatenate(
            [rows[g * 32 : (g + 1) * 32, q * part : (q + 1) * part] for q in range(QUARTERS)], axis=0
        )
        write(g, jnp.dot(permute, stacked, preferred_element_type=F32).astype(BF16))


def unfold(wire_ref, rows_ref):
    permute = wire_permutation(True)
    part = wire_ref.shape[1]
    for g in range(wire_ref.shape[0] // 128):
        block = jnp.dot(
            permute, wire_ref[g * 128 : (g + 1) * 128, :], preferred_element_type=F32
        ).astype(BF16)
        for q in range(QUARTERS):
            rows_ref[g * 32 : (g + 1) * 32, q * part : (q + 1) * part] = block[q * 32 : (q + 1) * 32]


def project_kernel(columns_ref, heads_ref, *refs):
    pieces = refs[:9]
    residual_ref, gain_ref, place_ref, mixed_ref, normed_ref, wire_ref = refs[9:15]
    weight_ref, part_ref, sems = refs[15:]
    half = weight_ref.shape[1] // 2
    targets = [weight_ref.at[s] for s in range(7)] + [
        weight_ref.at[7, pl.ds(0, half)],
        weight_ref.at[7, pl.ds(half, half)],
    ]
    copies = [
        pltpu.make_async_copy(pieces[s], targets[s], sems.at[s]) for s in range(9)
    ]
    for copy in copies:
        copy.start()
    rows = jnp.concatenate([heads_ref[h] for h in range(heads_ref.shape[0])], axis=1)
    for s in range(8):
        copies[s].wait()
        if s == 7:
            copies[8].wait()
        part_ref[columns_ref[s]] = jnp.dot(rows, weight_ref[s], preferred_element_type=F32)
    width = part_ref.shape[2]
    square = None
    for j in range(8):
        block = part_ref[j] + residual_ref[:, j * width : (j + 1) * width].astype(F32)
        mixed_ref[:, j * width : (j + 1) * width] = block
        part = jnp.sum(block * block, axis=-1, keepdims=True)
        square = part if square is None else square + part
    scale = lax.rsqrt(square * (1.0 / (8 * width)) + EPS)
    normed = (mixed_ref[...] * scale * gain_ref[...]).astype(BF16)
    normed_ref[...] = normed
    span = place_ref.shape[0] // PAIRS
    part = normed.shape[1] // QUARTERS
    for c in range(PAIRS):
        slots = jnp.dot(
            place_ref[c * span : (c + 1) * span, :], normed, preferred_element_type=F32
        ).astype(BF16)

        def write(g, block):
            wire_ref[g * 128 : (g + 1) * 128, c * part : (c + 1) * part] = block

        fold(slots, write)


def project(columns, heads, pieces, residual, gain, place):
    tokens, width = residual.shape
    peers = place.shape[0] // CAP
    vmem = pl.BlockSpec(memory_space=pltpu.VMEM)
    return pl.pallas_call(
        project_kernel,
        in_specs=[pl.BlockSpec(memory_space=pltpu.SMEM), vmem]
        + [pl.BlockSpec(memory_space=pl.ANY)] * 9
        + [vmem] * 3,
        out_specs=[vmem] * 3,
        out_shape=(
            jax.ShapeDtypeStruct((tokens, width), F32),
            jax.ShapeDtypeStruct((tokens, width), BF16),
            jax.ShapeDtypeStruct((peers * 8, width * CAP // 8), BF16),
        ),
        scratch_shapes=[
            pltpu.VMEM((8,) + pieces[0].shape, BF16),
            pltpu.VMEM((8, tokens, width // 8), F32),
            pltpu.SemaphoreType.DMA((9,)),
        ],
        name="project",
    )(columns, heads, *pieces, residual, gain, place)


def expert_kernel(wire_ref, gate_ref, up_ref, down_ref, out_ref, rows_ref):
    unfold(wire_ref, rows_ref)
    rows = rows_ref[...]
    gate = jnp.dot(rows, gate_ref[...], preferred_element_type=F32)
    up = jnp.dot(rows, up_ref[...], preferred_element_type=F32)
    hidden = (gate / (1.0 + jnp.exp(-gate)) * up).astype(BF16)
    output = jnp.dot(hidden, down_ref[...], preferred_element_type=F32).astype(BF16)

    def write(g, block):
        out_ref[g * 128 : (g + 1) * 128, :] = block

    fold(output, write)


def expert(wire, gate, up, down):
    rows, width = wire.shape
    part = width // PAIRS

    def whole(array):
        return pl.BlockSpec(array.shape, lambda c: (0, 0))

    return pl.pallas_call(
        expert_kernel,
        grid=(PAIRS,),
        in_specs=[pl.BlockSpec((rows, part), lambda c: (0, c)), whole(gate), whole(up), whole(down)],
        out_specs=pl.BlockSpec((rows, part), lambda c: (0, c)),
        out_shape=jax.ShapeDtypeStruct(wire.shape, BF16),
        scratch_shapes=[pltpu.VMEM((rows // QUARTERS, part * QUARTERS), BF16)],
        name="expert",
    )(wire, gate, up, down)


def combine_kernel(wire_ref, gates_ref, mixed_ref, shared_ref, out_ref, rows_ref, total_ref):
    c = pl.program_id(0)
    unfold(wire_ref, rows_ref)
    gates = gates_ref[...]
    tokens = gates.shape[0]
    high = gates.astype(BF16)
    rest = gates - high.astype(F32)
    middle = rest.astype(BF16)
    low = (rest - middle.astype(F32)).astype(BF16)
    parts = jnp.dot(
        jnp.concatenate([high, middle, low], axis=0), rows_ref[...], preferred_element_type=F32
    )
    routed = parts[:tokens] + (parts[tokens : 2 * tokens] + parts[2 * tokens :])

    @pl.when(c == 0)
    def _():
        total_ref[...] = routed

    @pl.when(c > 0)
    def _():
        total_ref[...] = total_ref[...] + routed

    @pl.when(c == pl.num_programs(0) - 1)
    def _():
        out_ref[...] = (mixed_ref[...] + shared_ref[...] + total_ref[...]).astype(BF16)


def combine(wire, gates, mixed, shared):
    rows, width = wire.shape
    tokens = mixed.shape[0]
    part = width // PAIRS

    def whole(array):
        return pl.BlockSpec(array.shape, lambda c: (0, 0))

    return pl.pallas_call(
        combine_kernel,
        grid=(PAIRS,),
        in_specs=[
            pl.BlockSpec((rows, part), lambda c: (0, c)),
            pl.BlockSpec((tokens, gates.shape[1] // PAIRS), lambda c: (0, c)),
            whole(mixed),
            whole(shared),
        ],
        out_specs=pl.BlockSpec(mixed.shape, lambda c: (0, 0)),
        out_shape=jax.ShapeDtypeStruct(mixed.shape, BF16),
        scratch_shapes=[
            pltpu.VMEM((rows // QUARTERS, part * QUARTERS), BF16),
            pltpu.VMEM(mixed.shape, F32),
        ],
        name="combine",
    )(wire, gates, mixed, shared)


def swiglu(row_block, gate_weight, up_weight, down_weight):
    gate_part = jnp.dot(row_block, gate_weight, preferred_element_type=F32)
    up_part = jnp.dot(row_block, up_weight, preferred_element_type=F32)
    hidden = (jax.nn.silu(gate_part) * up_part).astype(BF16)
    return jnp.dot(hidden, down_weight, preferred_element_type=F32)


def shift(values, target):
    size = lax.axis_size("dp")
    pairs = [(d, 2 * (target(d // 2, d % 2)[0] % (size // 2)) + target(d // 2, d % 2)[1]) for d in range(size)]
    return lax.ppermute(values, "dp", pairs)


def right(x, core):
    return x + 1, core


def left(x, core):
    return x - 1, core


def partner(x, core):
    return x, 1 - core


def per_device(
    residual,
    query,
    key_value,
    out_weight,
    norm_gain,
    query_gain,
    key_gain,
    route_ids,
    route_weights,
    shared_gate,
    shared_up,
    shared_down,
    expert_gate,
    expert_up,
    expert_down,
):
    tokens, width = residual.shape[1:]
    experts = expert_gate.shape[0] * lax.axis_size(("sp", "dp"))
    ring = lax.axis_size("dp") // 2
    half = out_weight.shape[0] // 2

    from_left = shift(out_weight, right)
    from_right = shift(out_weight, left)
    own_pair = shift(out_weight, partner)

    tables = rotary_tables(query_gain, key_gain, lax.axis_index("sp") * tokens, tokens)
    outgoing = prepare(
        jnp.transpose(query[0], (1, 0, 2)), jnp.transpose(key_value[0], (1, 0, 2)), tables
    )
    rows = lax.all_to_all(outgoing, "sp", split_axis=0, concat_axis=0, tiled=True)
    place, gates = route(route_ids[0], route_weights[0], experts)

    rows, from_left, from_right = lax.optimization_barrier((rows, from_left, from_right))
    far_top = shift(from_left[:half], right)
    far_bottom = shift(from_right[half:], left)
    left_pair = shift(from_left, partner)
    right_pair = shift(from_right, partner)
    attention = attend(rows.reshape(-1, rows.shape[2]))
    attention, far_top, far_bottom = lax.optimization_barrier((attention, far_top, far_bottom))
    far_top_pair = shift(far_top, partner)
    far_bottom_pair = shift(far_bottom, partner)
    heads = lax.all_to_all(
        attention.reshape(-1, tokens, attention.shape[1]), "sp", split_axis=0, concat_axis=0, tiled=True
    )

    me = lax.axis_index("dp")
    x, core = me // 2, me % 2

    def column(dx, flip):
        return 2 * ((x + dx) % ring) + (1 - core if flip else core)

    columns = jnp.stack(
        [
            column(0, False),
            column(0, True),
            column(-1, False),
            column(1, False),
            column(-1, True),
            column(1, True),
            column(2, False),
            column(2, True),
        ]
    ).astype(jnp.int32)
    far = jnp.concatenate([far_top, far_bottom], axis=0)
    pieces = [
        out_weight,
        own_pair,
        from_left,
        from_right,
        left_pair,
        right_pair,
        far,
        far_top_pair,
        far_bottom_pair,
    ]
    mixed, normed, wire = project(
        columns, heads, pieces, residual[0], norm_gain.reshape(1, -1), place
    )
    wire_shape = (wire.shape[0] // 8, 8, wire.shape[1])

    def exchange(values):
        return lax.all_to_all(
            values.reshape(wire_shape), ("sp", "dp"), split_axis=0, concat_axis=0, tiled=True
        ).reshape(values.shape)

    arrived = exchange(wire)
    shared = swiglu(normed, shared_gate, shared_up, shared_down)
    output = expert(arrived, expert_gate[0], expert_up[0], expert_down[0])
    returned = exchange(output)
    return combine(returned, gates, mixed, shared).reshape(1, tokens, width)


def solution(mesh):
    in_specs = (
        P("dp", "sp", None),
        P("dp", "sp", None, None),
        P("dp", "sp", None, None),
        P(None, "dp"),
        P(),
        P(),
        P(),
        P("dp", "sp", None),
        P("dp", "sp", None),
        P(),
        P(),
        P(),
        P(("sp", "dp"), None, None),
        P(("sp", "dp"), None, None),
        P(("sp", "dp"), None, None),
    )
    out_specs = P("dp", "sp", None)
    return jax.shard_map(
        per_device, mesh=mesh, in_specs=in_specs, out_specs=out_specs, check_vma=False
    )
```

time: 319 us -> 212 us (0.66)
  local copies, waits for them, and re-layouts: 78.9 us -> 14.8 us
  Pallas kernels: 0 us -> 51.5 us
  matrix products: 37.2 us -> 5.43 us
  waiting for transfers between devices: 67.6 us -> 39.7 us
  other arithmetic: 35 us -> 7.66 us
  between operations: 13.8 us -> 0.32 us
  blocking collectives: 62.2 us -> 72.1 us
    pallas_call x0 -> x6, Pallas kernels: none -> 51.5 us  [the longest x1 16.7 us: attend(): pl.pallas_call(attend_kernel, grid=(length // block,), in_specs=[pl.Block...]
    dot_general x13 -> x2, matrix products: 37.2 us -> 5.43 us  [the longest x1 3.39 us: swiglu(): return jnp.dot(hidden, down_weight, preferred_element_type=F32)]
    all_to_all x4 -> x2, waiting for transfers between devices: 66.9 us -> 39.7 us  [the longest x1 35.9 us: exchange(): lax.all_to_all(values.reshape(wire_shape), ('sp', 'dp'), split_axis=0, co...]
    another operation x7 -> x1, local copies, waits for them, and re-layouts: 19.6 us -> 0.61 us  [per_device(): jnp.stack([column(0, False), column(0, True), column(-1, False), column(1...]
    reshape x3 -> x0, local copies, waits for them, and re-layouts: 16.5 us -> none  [the longest x1 6.32 us: per_device(): gathered = returned.reshape(experts * slot_count, model_width)[slot_place]]
    reduce_sum x9 -> x0, other arithmetic: 13.4 us -> none  [the longest x4 6.57 us: one_block(): row_total = jnp.sum(weights, axis=-1, keepdims=True)]
    all_to_all x4 -> x2, starting transfers between devices: 22.7 us -> 10.2 us  [the longest x1 5.78 us: exchange(): lax.all_to_all(values.reshape(wire_shape), ('sp', 'dp'), split_axis=0, co...]
    unnamed x38 -> x22, local copies, waits for them, and re-layouts: 13.1 us -> 2.27 us
  transfers between devices with their start and end apart: 5 -> 11, of which waited for: 4 -> 2; matrix products, arithmetic and copies ran while one was open for 22% -> 11% of each run, Pallas kernels for 0% -> 11%
where the time goes in v1:
time: 212 us; the launch traced here: 211 us
  blocking collectives  72.1 us (34%)
  Pallas kernels  51.5 us (24%)
  waiting for transfers between devices  39.7 us (19%)
  starting transfers between devices  19.7 us (9%)
  local copies, waits for them, and re-layouts  14.8 us (7%)
  other arithmetic  7.66 us (4%)
  matrix products  5.43 us (3%)
    all_to_all x1, blocking collectives, exchange(): lax.all_to_all(values.reshape(wire_shape), ('sp', 'dp'), split_axis=0, co...  48.2 us
    all_to_all x1, waiting for transfers between devices, exchange(): lax.all_to_all(values.reshape(wire_shape), ('sp', 'dp'), split_axis=0, co...  35.9 us
    all_to_all x1, blocking collectives, per_device(): lax.all_to_all(outgoing, 'sp', split_axis=0, concat_axis=0, tiled=True)  23.9 us
    pallas_call x1, Pallas kernels, attend(): pl.pallas_call(attend_kernel, grid=(length // block,), in_specs=[pl.Block...  16.7 us
    pallas_call x1, Pallas kernels, expert(): pl.pallas_call(expert_kernel, grid=(PAIRS,), in_specs=[pl.BlockSpec((rows...  11.8 us
    pallas_call x1, Pallas kernels, project(): pl.pallas_call(project_kernel, in_specs=[pl.BlockSpec(memory_space=pltpu....  9.83 us
    ppermute x9, starting transfers between devices, shift(): return lax.ppermute(values, 'dp', pairs)  9.46 us
    pallas_call x1, Pallas kernels, combine(): pl.pallas_call(combine_kernel, grid=(PAIRS,), in_specs=[pl.BlockSpec((row...  6.11 us
  transfers between devices with their start and end apart: 11, of which 2 were waited for; matrix products, arithmetic and copies ran while one was open for 11% of the time, Pallas kernels for 11%

profile of v1, /device:TPU:1, one launch (start us, length us, event | category | flops | bytes accessed | tf_op | source)
XLA Modules:
  0.0 211.1 jit_solution(15433461984682073036)
XLA Ops:
  0.0 3.4 %collective-permute-start.1 = (bf16[2048,256]{1,0:T(8,128)(2,1)}, bf16[2048,256]{1,0:T(8,128)(2,1)S(1)}, u32[]{:S(2)}, u32[]{:S(2)}) collective-permute-start(bf16[2048,256]{1,0:T(8,128)(2,1)} %refs_0_.1), channel_id=1, source_target_pairs={{0,6},{1,7},{2,0},{3,1},{4,2},{5,3},{6,4},{7,5},{8,14},{9,15},{10,... | collective-permute-start | bytes 3145736 | tf_op jit(solution)/shard_map/ppermute | solution.py:363
  3.4 1.3 maximum_multiply_fusion
  4.7 0.8 pad_maximum_fusion.1
  5.5 0.7 pad_clamp_fusion
  6.2 1.6 gather_fusion.3
  7.8 1.6 gather_fusion.1
  9.4 1.6 gather_fusion.2
  11.0 1.6 gather_fusion
  12.6 1.0 multiply_dynamic-update-slice_fusion.2
  14.9 2.5 %copy_bitcast_fusion = (bf16[16,128,128]{2,1,0:T(8,128)(2,1)}, bf16[16,128,128]{2,1,0:T(8,128)(2,1)}) fusion(bf16[1,128,16,128]{3,2,1,0:T(8,128)(2,1)} %param.27, bf16[1,128,16,128]{3,2,1,0:T(8,128)(2,1)} %param.26), kind=kLoop, calls=%fused_computation.5 | loop fusion | bytes 2097152 | tf_op jit(solution)/shard_map/transpose | solution.py:406
  17.6 0.7 copy-done.3
  18.4 4.3 %prepare.1 = bf16[16,128,256]{2,1,0:T(8,128)(2,1)} custom-call(bf16[16,128,128]{2,1,0:T(8,128)(2,1)} %get-tuple-element.36.q_ref, bf16[16,128,128]{2,1,0:T(8,128)(2,1)} %get-tuple-element.35.kv_ref, f32[6,128,128]{2,1,0:T(8,128)} %copy-done.3), custom_call_target="tpu_custom_call" | custom-call | tf_op jit(solution)/shard_map/prepare/pallas_call | solution.py:83
  22.7 23.9 %all_to_all.20 = bf16[16,128,256]{2,1,0:T(8,128)(2,1)} all-to-all(bf16[16,128,256]{2,1,0:T(8,128)(2,1)} %prepare.1), channel_id=1, replica_groups=mesh['sp'=16,'dp'=8] {'sp'}, dimensions={0} | all-to-all | bytes 2097152 | tf_op jit(solution)/shard_map/all_to_all | solution.py:408
  46.6 2.3 %slice.6 = bf16[1024,256]{1,0:T(8,128)(2,1)} slice(bf16[2048,256]{1,0:T(8,128)(2,1)} %collective-permute-done.refs_2_), slice={[0:1024], [0:256]} | slice | bytes 1048576 | tf_op jit(solution)/shard_map/slice | solution.py:412
  48.9 0.8 slice.7
  49.8 2.4 %collective-permute-start.3 = (bf16[1024,256]{1,0:T(8,128)(2,1)}, bf16[1024,256]{1,0:T(8,128)(2,1)}, u32[]{:S(2)}, u32[]{:S(2)}) collective-permute-start(bf16[1024,256]{1,0:T(8,128)(2,1)} %slice.7), channel_id=1, source_target_pairs={{0,6},{1,7},{2,0},{3,1},{4,2},{5,3},{6,4},{7,5},{8,14},{9,15},{10,... | collective-permute-start | bytes 1572872 | tf_op jit(solution)/shard_map/ppermute | solution.py:363
  52.2 2.6 %collective-permute-start.4 = (bf16[2048,256]{1,0:T(8,128)(2,1)}, bf16[2048,256]{1,0:T(8,128)(2,1)}, u32[]{:S(2)}, u32[]{:S(2)}) collective-permute-start(bf16[2048,256]{1,0:T(8,128)(2,1)} %refs_0_.1), channel_id=1, source_target_pairs={{0,1},{1,0},{2,3},{3,2},{4,5},{5,4},{6,7},{7,6},{8,9},{9,8},{10,11... | collective-permute-start | bytes 3145736 | tf_op jit(solution)/shard_map/ppermute | solution.py:363
  55.3 16.7 %attend.1 = bf16[2048,128]{1,0:T(8,128)(2,1)} custom-call(bf16[2048,256]{1,0:T(8,128)(2,1)} %bitcast.37, bf16[2048,256]{1,0:T(8,128)(2,1)} %bitcast.38), custom_call_target="tpu_custom_call" | custom-call | tf_op jit(solution)/shard_map/attend/pallas_call | solution.py:123
  72.6 4.4 %all-to-all-start.1 = ((bf16[16,128,128]{2,1,0:T(8,128)(2,1)}), bf16[16,128,128]{2,1,0:T(8,128)(2,1)}, u32[]{:S(2)}, u32[]{:S(2)}) async-start(bf16[16,128,128]{2,1,0:T(8,128)(2,1)} %bitcast.40), calls=%async_computation.1 | async-start | bytes 1048576 | tf_op jit(solution)/shard_map/all_to_all | solution.py:420
  77.1 0.7 copy.32
  77.8 0.7 copy.33
  78.6 2.7 %route.1 = (bf16[768,128]{1,0:T(8,128)(2,1)}, f32[128,768]{1,0:T(8,128)}) custom-call(s32[128,4]{1,0:T(8,128)} %bitcast.45, f32[128,4]{1,0:T(8,128)} %bitcast.46), custom_call_target="tpu_custom_call" | custom-call | tf_op jit(solution)/shard_map/route/pallas_call | solution.py:162
  81.9 2.3 %pad_maximum_fusion.refs_6_ = bf16[2048,256]{1,0:T(8,128)(2,1)} fusion(bf16[1024,256]{1,0:T(8,128)(2,1)} %collective-permute-done.3, bf16[1024,256]{1,0:T(8,128)(2,1)} %collective-permute-done.2), kind=kLoop, calls=%fused_computation.4 | loop fusion | flops 2097152 | bytes 2097152 | tf_op jit(solution)/shard_map/concatenate | solution.py:442
  84.3 3.8 %all-to-all-done.1.heads_ref = bf16[16,128,128]{2,1,0:T(8,128)(2,1)} async-done(((bf16[16,128,128]{2,1,0:T(8,128)(2,1)}), bf16[16,128,128]{2,1,0:T(8,128)(2,1)}, u32[]{:S(2)}, u32[]{:S(2)}) %all-to-all-start.1) | async-done | bytes 524320 | tf_op jit(solution)/shard_map/all_to_all | solution.py:420
  88.1 9.8 %project.1 = (f32[128,2048]{1,0:T(8,128)}, bf16[128,2048]{1,0:T(8,128)(2,1)}, bf16[1024,1536]{1,0:T(8,128)(2,1)}) custom-call(s32[8]{0:T(128)} %stack.44.columns_ref, bf16[16,128,128]{2,1,0:T(8,128)(2,1)} %all-to-all-done.1.heads_ref, bf16[2048,256]{1,0:T(8,128)(2,1)} %refs_0_.1, bf16[2048,256]{1,0:T(8,128)(2,1)} %collective-permute-done.4.refs_1_, ...), custom_call_target="tpu_custom_call" | custom-call | tf_op jit(solution)/shard_map/project/pallas_call | solution.py:247
  97.9 48.2 %all_to_all.21 = bf16[128,8,1536]{2,1,0:T(8,128)(2,1)} all-to-all(bf16[128,8,1536]{2,1,0:T(8,128)(2,1)} %bitcast.39), channel_id=1, replica_groups=mesh['sp'=16,'dp'=8] {'sp','dp'}, dimensions={0} | all-to-all | bytes 6291456 | tf_op jit(solution)/shard_map/all_to_all | solution.py:460
  146.1 11.8 %expert.1 = bf16[1024,1536]{1,0:T(8,128)(2,1)} custom-call(bf16[1024,1536]{1,0:T(8,128)(2,1)} %bitcast.36, bf16[2048,512]{1,0:T(8,128)(2,1)} %bitcast.41, bf16[2048,512]{1,0:T(8,128)(2,1)} %bitcast.42, bf16[512,2048]{1,0:T(8,128)(2,1)} %bitcast.43), custom_call_target="tpu_custom_call" | custom-call | tf_op jit(solution)/shard_map/expert/pallas_call | solution.py:288
  157.9 5.8 %all-to-all-start.3 = ((bf16[128,8,1536]{2,1,0:T(8,128)(2,1)}), bf16[128,8,1536]{2,1,0:T(8,128)(2,1)}, u32[]{:S(2)}, u32[]{:S(2)}) async-start(bf16[128,8,1536]{2,1,0:T(8,128)(2,1)} %bitcast.35), calls=%async_computation.3 | async-start | bytes 6291456 | tf_op jit(solution)/shard_map/all_to_all | solution.py:460
  163.7 2.0 fusion.9
  165.8 3.4 %fusion.shared_ref = f32[128,2048]{1,0:T(8,128)} fusion(bf16[512,2048]{1,0:T(8,128)(2,1)S(1)} %copy-done, f32[128,512]{1,0:T(8,128)S(1)} %fusion.9, bf16[128,2048]{1,0:T(8,128)(2,1)S(1)} %copy-done.2, bf16[2048,512]{1,0:T(8,128)(2,1)} %param.35), kind=kOutput, calls=%fused_computation.8 | convolution fusion | flops 537264128 | bytes 6029312 | tf_op jit(solution)/shard_map/dot_general | solution.py:357
  169.2 35.9 %all-to-all-done.3 = bf16[128,8,1536]{2,1,0:T(8,128)(2,1)} async-done(((bf16[128,8,1536]{2,1,0:T(8,128)(2,1)}), bf16[128,8,1536]{2,1,0:T(8,128)(2,1)}, u32[]{:S(2)}, u32[]{:S(2)}) %all-to-all-start.3) | async-done | bytes 3145760 | tf_op jit(solution)/shard_map/all_to_all | solution.py:460
  205.0 6.1 %combine.1 = bf16[128,2048]{1,0:T(8,128)(2,1)} custom-call(bf16[1024,1536]{1,0:T(8,128)(2,1)} %bitcast.24.wire_ref, f32[128,768]{1,0:T(8,128)} %get-tuple-element.24.gates_ref, f32[128,2048]{1,0:T(8,128)} %get-tuple-element.25.mixed_ref, f32[128,2048]{1,0:T(8,128)} %fusion.shared_ref), custom_call_target="tpu_custom_call" | custom-call | tf_op jit(solution)/shard_map/combine/pallas_call | solution.py:334
  (42 shorter events, 3.3 us)
Async XLA Ops:
  0.0 165.8 %copy-start = (bf16[512,2048]{1,0:T(8,128)(2,1)S(1)}, bf16[512,2048]{1,0:T(8,128)(2,1)}, u32[]{:S(2)}) copy-start(bf16[512,2048]{1,0:T(8,128)(2,1)} %param.36) | copy-start | bytes 6291460
  0.0 12.6 %copy-start.9 = (pred[128]{0:T(512)(128)(4,1)S(1)}, pred[128]{0:T(512)(128)(4,1)}, u32[]{:S(2)}) copy-start(pred[128]{0:T(512)(128)(4,1)} %constant.119.clone) | copy-start | bytes 388
  0.0 12.6 %copy-start.4 = (f32[128]{0:T(128)S(1)}, f32[128]{0:T(128)}, u32[]{:S(2)}) copy-start(f32[128]{0:T(128)} %constant.131) | copy-start | bytes 1540
  0.0 12.6 %copy-start.5 = (pred[128]{0:T(512)(128)(4,1)S(1)}, pred[128]{0:T(512)(128)(4,1)}, u32[]{:S(2)}) copy-start(pred[128]{0:T(512)(128)(4,1)} %constant.130) | copy-start | bytes 388
  0.0 14.2 %copy-start.6 = (pred[128]{0:T(512)(128)(4,1)S(1)}, pred[128]{0:T(512)(128)(4,1)}, u32[]{:S(2)}) copy-start(pred[128]{0:T(512)(128)(4,1)} %constant.134) | copy-start | bytes 388
  0.0 46.6 %collective-permute-start.1 = (bf16[2048,256]{1,0:T(8,128)(2,1)}, bf16[2048,256]{1,0:T(8,128)(2,1)S(1)}, u32[]{:S(2)}, u32[]{:S(2)}) collective-permute-start(bf16[2048,256]{1,0:T(8,128)(2,1)} %refs_0_.1), channel_id=1, source_target_pairs={{0,6},{1,7},{2,0},{3,1},{4,2},{5,3},{6,4},{7,5},{8,14},{9,15},{10,... | collective-permute-start | bytes 3145736 | tf_op jit(solution)/shard_map/ppermute | solution.py:363
  3.4 43.2 %collective-permute-start = (bf16[2048,256]{1,0:T(8,128)(2,1)}, bf16[2048,256]{1,0:T(8,128)(2,1)}, u32[]{:S(2)}, u32[]{:S(2)}) collective-permute-start(bf16[2048,256]{1,0:T(8,128)(2,1)} %refs_0_.1), channel_id=1, source_target_pairs={{0,2},{1,3},{2,4},{3,5},{4,6},{5,7},{6,0},{7,1},{8,10},{9,11},{10,... | collective-permute-start | bytes 3145736 | tf_op jit(solution)/shard_map/ppermute | solution.py:363
  17.6 0.8 copy-start.3
  46.6 25.4 %copy-start.1 = (bf16[2048,256]{1,0:T(8,128)(2,1)}, bf16[2048,256]{1,0:T(8,128)(2,1)S(1)}, u32[]{:S(2)}) copy-start(bf16[2048,256]{1,0:T(8,128)(2,1)S(1)} %collective-permute-done.1.refs_3_) | copy-start | bytes 3145732
  49.8 27.3 %copy-start.7 = (s32[1,128,4]{1,2,0:T(4,128)S(1)}, s32[1,128,4]{1,2,0:T(4,128)}, u32[]{:S(2)}) copy-start(s32[1,128,4]{1,2,0:T(4,128)} %param.32) | copy-start | bytes 6148
  49.8 28.1 %copy-start.8 = (f32[1,128,4]{1,2,0:T(4,128)S(1)}, f32[1,128,4]{1,2,0:T(4,128)}, u32[]{:S(2)}) copy-start(f32[1,128,4]{1,2,0:T(4,128)} %param.33) | copy-start | bytes 6148
  49.8 22.2 %collective-permute-start.3 = (bf16[1024,256]{1,0:T(8,128)(2,1)}, bf16[1024,256]{1,0:T(8,128)(2,1)}, u32[]{:S(2)}, u32[]{:S(2)}) collective-permute-start(bf16[1024,256]{1,0:T(8,128)(2,1)} %slice.7), channel_id=1, source_target_pairs={{0,6},{1,7},{2,0},{3,1},{4,2},{5,3},{6,4},{7,5},{8,14},{9,15},{10,... | collective-permute-start | bytes 1572872 | tf_op jit(solution)/shard_map/ppermute | solution.py:363
  52.2 19.8 %collective-permute-start.2 = (bf16[1024,256]{1,0:T(8,128)(2,1)}, bf16[1024,256]{1,0:T(8,128)(2,1)}, u32[]{:S(2)}, u32[]{:S(2)}) collective-permute-start(bf16[1024,256]{1,0:T(8,128)(2,1)} %slice.6), channel_id=1, source_target_pairs={{0,2},{1,3},{2,4},{3,5},{4,6},{5,7},{6,0},{7,1},{8,10},{9,11},{10,... | collective-permute-start | bytes 1572872 | tf_op jit(solution)/shard_map/ppermute | solution.py:363
  52.2 32.1 %collective-permute-start.4 = (bf16[2048,256]{1,0:T(8,128)(2,1)}, bf16[2048,256]{1,0:T(8,128)(2,1)}, u32[]{:S(2)}, u32[]{:S(2)}) collective-permute-start(bf16[2048,256]{1,0:T(8,128)(2,1)} %refs_0_.1), channel_id=1, source_target_pairs={{0,1},{1,0},{2,3},{3,2},{4,5},{5,4},{6,7},{7,6},{8,9},{9,8},{10,11... | collective-permute-start | bytes 3145736 | tf_op jit(solution)/shard_map/ppermute | solution.py:363
  54.8 33.3 %collective-permute-start.5 = (bf16[2048,256]{1,0:T(8,128)(2,1)}, bf16[2048,256]{1,0:T(8,128)(2,1)}, u32[]{:S(2)}, u32[]{:S(2)}) collective-permute-start(bf16[2048,256]{1,0:T(8,128)(2,1)} %collective-permute-done.refs_2_), channel_id=1, source_target_pairs={{0,1},{1,0},{2,3},{3,2},{4,5},{5,4},{6,7},{7,6},{8,9},{9,8},{10,11... | collective-permute-start | bytes 3145736 | tf_op jit(solution)/shard_map/ppermute | solution.py:363
  54.8 33.3 %collective-permute-start.6 = (bf16[2048,256]{1,0:T(8,128)(2,1)S(1)}, bf16[2048,256]{1,0:T(8,128)(2,1)}, u32[]{:S(2)}, u32[]{:S(2)}) collective-permute-start(bf16[2048,256]{1,0:T(8,128)(2,1)S(1)} %collective-permute-done.1.refs_3_), channel_id=1, source_target_pairs={{0,1},{1,0},{2,3},{3,2},{4,5},{5,4},{6,7},{7,6},{8,9},{9,8},{10,11... | collective-permute-start | bytes 3145736 | tf_op jit(solution)/shard_map/ppermute | solution.py:363
  72.0 16.1 %collective-permute-start.7 = (bf16[1024,256]{1,0:T(8,128)(2,1)}, bf16[1024,256]{1,0:T(8,128)(2,1)}, u32[]{:S(2)}, u32[]{:S(2)}) collective-permute-start(bf16[1024,256]{1,0:T(8,128)(2,1)} %collective-permute-done.2), channel_id=1, source_target_pairs={{0,1},{1,0},{2,3},{3,2},{4,5},{5,4},{6,7},{7,6},{8,9},{9,8},{10,11... | collective-permute-start | bytes 1572872 | tf_op jit(solution)/shard_map/ppermute | solution.py:363
  72.1 16.0 %collective-permute-start.8 = (bf16[1024,256]{1,0:T(8,128)(2,1)}, bf16[1024,256]{1,0:T(8,128)(2,1)}, u32[]{:S(2)}, u32[]{:S(2)}) collective-permute-start(bf16[1024,256]{1,0:T(8,128)(2,1)} %collective-permute-done.3), channel_id=1, source_target_pairs={{0,1},{1,0},{2,3},{3,2},{4,5},{5,4},{6,7},{7,6},{8,9},{9,8},{10,11... | collective-permute-start | bytes 1572872 | tf_op jit(solution)/shard_map/ppermute | solution.py:363
  72.6 15.5 %all-to-all-start.1 = ((bf16[16,128,128]{2,1,0:T(8,128)(2,1)}), bf16[16,128,128]{2,1,0:T(8,128)(2,1)}, u32[]{:S(2)}, u32[]{:S(2)}) async-start(bf16[16,128,128]{2,1,0:T(8,128)(2,1)} %bitcast.40), calls=%async_computation.1 | async-start | bytes 1048576 | tf_op jit(solution)/shard_map/all_to_all | solution.py:420
  157.9 5.8 %copy-start.2 = (bf16[128,2048]{1,0:T(8,128)(2,1)S(1)}, bf16[128,2048]{1,0:T(8,128)(2,1)}, u32[]{:S(2)}) copy-start(bf16[128,2048]{1,0:T(8,128)(2,1)} %get-tuple-element.26) | copy-start | bytes 1572868
  157.9 47.1 %all-to-all-start.3 = ((bf16[128,8,1536]{2,1,0:T(8,128)(2,1)}), bf16[128,8,1536]{2,1,0:T(8,128)(2,1)}, u32[]{:S(2)}, u32[]{:S(2)}) async-start(bf16[128,8,1536]{2,1,0:T(8,128)(2,1)} %bitcast.35), calls=%async_computation.3 | async-start | bytes 6291456 | tf_op jit(solution)/shard_map/all_to_all | solution.py:460

commit v2 on v1

v2 whole, which is shorter than its diff:
```python
import jax
import jax.numpy as jnp
import numpy as np
from jax import lax
from jax.experimental import pallas as pl
from jax.experimental.pallas import tpu as pltpu
from jax.sharding import PartitionSpec as P

GRID_W = 64
HD = 64
EPS = 1e-06
THETA = 10000.0
ROUTED_SCALE = 2.5
CAP = 6
PAIRS = CAP // 2
QUARTERS = 4
F32 = jnp.float32
BF16 = jnp.bfloat16


def iota(shape, axis):
    return lax.broadcasted_iota(jnp.int32, shape, axis)


LANES = 2 * HD


def local(values):
    return pltpu.with_memory_space_constraint(values, pltpu.VMEM)


def distant(values):
    return pltpu.with_memory_space_constraint(values, pltpu.HBM)


def limit(mib):
    return pltpu.CompilerParams(vmem_limit_bytes=mib * 2**20)


def angle_tables(tokens, blocks):
    lane = np.arange(LANES)
    by_row = lane % HD < HD // 2
    freq = THETA ** (-(2.0 * (lane % (HD // 4))) / (HD // 2))
    col = (np.arange(tokens) % GRID_W)[:, None] * freq[None, :]
    row = np.arange(blocks * tokens // GRID_W)[:, None] * freq[None, :]
    col = np.where(by_row, 0.0, np.stack([np.cos(col), np.sin(col)]))
    row = np.where(by_row, np.stack([np.cos(row), np.sin(row)]), 0.0)
    row = row.reshape(2, blocks, tokens // GRID_W, LANES).transpose(1, 0, 2, 3)
    return col.astype(np.float32), row.astype(np.float32)


def prepare_kernel(
    block_ref, q_ref, kv_ref, col_ref, row_ref, q_gain_ref, k_gain_ref, out_ref, table_ref
):
    del block_ref
    tokens, heads = q_ref.shape[:2]
    shape = (tokens, LANES)
    lane = iota(shape, 1)
    is_key = lane < HD
    block = (iota((LANES, LANES), 0) // HD == iota((LANES, LANES), 1) // HD).astype(F32).astype(BF16)

    @pl.when(pl.program_id(0) == 0)
    def _():
        lower = lane % (HD // 2) < HD // 4

        def angles(which):
            rows = [
                col_ref[which, r * GRID_W : (r + 1) * GRID_W, :] + row_ref[0, which, r : r + 1, :]
                for r in range(tokens // GRID_W)
            ]
            return jnp.concatenate(rows, axis=0)

        cosine, sine = angles(0), angles(1)

        def tables(gain_ref, scale):
            gain = gain_ref[...] * scale
            gain = jnp.broadcast_to(jnp.concatenate([gain, gain], axis=1), shape)
            up = pltpu.roll(gain, LANES - HD // 4, 1)
            down = pltpu.roll(gain, HD // 4, 1)
            return (
                gain * cosine,
                jnp.where(lower, -up * sine, 0.0),
                jnp.where(lower, 0.0, down * sine),
            )

        for i, table in enumerate(tables(q_gain_ref, HD**-0.5)):
            table_ref[i] = table
        own, up, down = tables(k_gain_ref, 1.0)
        table_ref[3] = jnp.where(is_key, own, 1.0)
        table_ref[4] = jnp.where(is_key, up, 0.0)
        table_ref[5] = jnp.where(is_key, down, 0.0)

    def turned(x, base, keys):
        square = x * x
        high = square.astype(BF16)
        low = (square - high.astype(F32)).astype(BF16)
        total = jnp.dot(high, block, preferred_element_type=F32)
        total = total + jnp.dot(low, block, preferred_element_type=F32)
        scale = lax.rsqrt(total * (1.0 / HD) + EPS)
        if keys:
            scale = jnp.where(is_key, scale, 1.0)
        mixed = (
            x * table_ref[base]
            + pltpu.roll(x, LANES - HD // 4, 1) * table_ref[base + 1]
            + pltpu.roll(x, HD // 4, 1) * table_ref[base + 2]
        )
        return (mixed * scale).astype(BF16)

    query = jnp.swapaxes(q_ref[...].astype(F32), 0, 1)
    pair = jnp.swapaxes(kv_ref[...].astype(F32), 0, 1)
    for h in range(heads):
        out_ref[h, :, :LANES] = turned(query[h], 0, False)
        out_ref[h, :, LANES:] = turned(pair[h], 3, True)


def prepare(query, pair, query_gain, key_gain, block, blocks):
    tokens, heads, width = query.shape
    step = 8
    col, row = angle_tables(tokens, blocks)
    gains = [gain.reshape(1, -1) for gain in (query_gain, key_gain)]
    return pl.pallas_call(
        prepare_kernel,
        grid_spec=pltpu.PrefetchScalarGridSpec(
            num_scalar_prefetch=1,
            grid=(heads // step,),
            in_specs=[
                pl.BlockSpec((tokens, step, width), lambda i, b: (0, i, 0)),
                pl.BlockSpec((tokens, step, width), lambda i, b: (0, i, 0)),
                pl.BlockSpec(col.shape, lambda i, b: (0, 0, 0)),
                pl.BlockSpec((1,) + row.shape[1:], lambda i, b: (b[0], 0, 0, 0)),
                pl.BlockSpec((1, HD), lambda i, b: (0, 0)),
                pl.BlockSpec((1, HD), lambda i, b: (0, 0)),
            ],
            out_specs=pl.BlockSpec((step, tokens, 2 * width), lambda i, b: (i, 0, 0)),
            scratch_shapes=[pltpu.VMEM((6, tokens, width), F32)],
        ),
        out_shape=jax.ShapeDtypeStruct((heads, tokens, 2 * width), BF16),
        compiler_params=limit(16),
        name="prepare",
    )(jnp.full((1,), block, jnp.int32), query, pair, col, row, *gains)


def attend_kernel(q_ref, kv_ref, out_ref, keys_ref, values_ref):
    @pl.when(pl.program_id(0) == 0)
    def _():
        key = kv_ref[:, 128 : 128 + HD]
        value = kv_ref[:, 128 + HD :]
        keys_ref[...] = jnp.concatenate([key, key], axis=1)
        values_ref[:, :128] = jnp.concatenate([value, value], axis=1)
        values_ref[:, 128:] = jnp.ones_like(values_ref[:, 128:])

    first = iota((1, 128), 1) < HD
    block = 512
    parts = [(r, head) for r in range(q_ref.shape[0] // block) for head in range(2)]

    def score(part):
        r, head = part
        query = q_ref[r * block : (r + 1) * block, :]
        mine = jnp.where(first if head == 0 else ~first, query, jnp.zeros_like(query))
        return lax.dot_general(
            mine, keys_ref[...], (((1,), (1,)), ((), ())), preferred_element_type=F32
        )

    def mix(scores):
        weights = jnp.exp(scores - jnp.max(scores, axis=-1, keepdims=True)).astype(BF16)
        mixed = jnp.dot(weights, values_ref[...], preferred_element_type=F32)
        return mixed[:, :128] / mixed[:, 128:]

    outs = []
    ahead = score(parts[0])
    for n in range(len(parts)):
        scores = ahead
        if n + 1 < len(parts):
            ahead = score(parts[n + 1])
        outs.append(mix(scores))
    for r in range(len(parts) // 2):
        out_ref[r * block : (r + 1) * block, :] = jnp.where(
            first, outs[2 * r], outs[2 * r + 1]
        ).astype(BF16)


def attend(rows):
    length, width = rows.shape
    block = 512
    return pl.pallas_call(
        attend_kernel,
        grid=(length // block,),
        in_specs=[
            pl.BlockSpec((block, 128), lambda i: (i, 0)),
            pl.BlockSpec((length, width), lambda i: (0, 0)),
        ],
        out_specs=pl.BlockSpec((block, 128), lambda i: (i, 0)),
        out_shape=pltpu.HBM((length, 128), BF16),
        scratch_shapes=[pltpu.VMEM((length, 128), BF16), pltpu.VMEM((length, 256), BF16)],
        compiler_params=limit(32),
        name="attend",
    )(rows, rows)


def route_kernel(ids_ref, weights_ref, place_ref, gates_ref):
    tokens, top = ids_ref.shape
    experts = place_ref.shape[0] // CAP
    expert = iota((tokens, experts), 1)
    hits = [(ids_ref[:, k : k + 1] == expert).astype(F32) for k in range(top)]
    used = sum(hits[1:], hits[0])
    earlier = (iota((tokens, tokens), 1) < iota((tokens, tokens), 0)).astype(F32).astype(BF16)
    before = jnp.dot(earlier, used.astype(BF16), preferred_element_type=F32)
    raw = weights_ref[...]
    gate = raw / jnp.sum(raw, axis=-1, keepdims=True) * ROUTED_SCALE
    slots = iota((tokens, experts * CAP), 1)
    place = jnp.zeros((tokens, experts * CAP), F32)
    gated = jnp.zeros((tokens, experts * CAP), F32)
    for k in range(top):
        rank = jnp.sum(hits[k] * before, axis=-1, keepdims=True).astype(jnp.int32)
        slot = (rank // 2) * (2 * experts) + ids_ref[:, k : k + 1] * 2 + rank % 2
        here = slots == slot
        place = jnp.where(here, 1.0, place)
        gated = jnp.where(here, gate[:, k : k + 1], gated)
    place_ref[...] = jnp.transpose(place).astype(BF16)
    gates_ref[...] = gated


def route(ids, weights, experts):
    tokens, top = ids.shape
    return pl.pallas_call(
        route_kernel,
        out_shape=(
            pltpu.VMEM((experts * CAP, tokens), BF16),
            pltpu.VMEM((tokens, experts * CAP), F32),
        ),
        compiler_params=limit(8),
        name="route",
    )(ids, weights)


def wire_permutation(transposed):
    wire = iota((128, 128), 1 if transposed else 0)
    flat = iota((128, 128), 0 if transposed else 1)
    source = (wire // 2 % QUARTERS) * 32 + (wire // 8) * 2 + wire % 2
    return (flat == source).astype(F32).astype(BF16)


def fold(rows, write):
    permute = wire_permutation(False)
    part = rows.shape[1] // QUARTERS
    for g in range(rows.shape[0] // 32):
        stacked = jnp.concatenate(
            [rows[g * 32 : (g + 1) * 32, q * part : (q + 1) * part] for q in range(QUARTERS)], axis=0
        )
        write(g, jnp.dot(permute, stacked, preferred_element_type=F32).astype(BF16))


def unfold(wire_ref, rows_ref):
    permute = wire_permutation(True)
    part = wire_ref.shape[1]
    for g in range(wire_ref.shape[0] // 128):
        block = jnp.dot(
            permute, wire_ref[g * 128 : (g + 1) * 128, :], preferred_element_type=F32
        ).astype(BF16)
        for q in range(QUARTERS):
            rows_ref[g * 32 : (g + 1) * 32, q * part : (q + 1) * part] = block[q * 32 : (q + 1) * 32]


def project_kernel(columns_ref, heads_ref, *refs):
    pieces = refs[:8]
    residual_hbm, gain_ref, place_ref, mixed_hbm, normed_hbm, wire_ref = refs[8:14]
    weight_ref, residual_ref, part_ref, mixed_ref, normed_ref, sems = refs[14:]
    copies = [
        pltpu.make_async_copy(pieces[s], weight_ref.at[s], sems.at[s]) for s in range(8)
    ]
    copies.append(pltpu.make_async_copy(residual_hbm, residual_ref, sems.at[8]))
    copies.append(pltpu.make_async_copy(mixed_ref, mixed_hbm, sems.at[9]))
    copies.append(pltpu.make_async_copy(normed_ref, normed_hbm, sems.at[10]))
    for copy in copies[:9]:
        copy.start()
    rows = jnp.concatenate([heads_ref[h] for h in range(heads_ref.shape[0])], axis=1)
    for s in range(8):
        copies[s].wait()
        part_ref[columns_ref[s]] = jnp.dot(rows, weight_ref[s], preferred_element_type=F32)
    copies[8].wait()
    width = part_ref.shape[2]
    square = None
    for j in range(8):
        block = part_ref[j] + residual_ref[:, j * width : (j + 1) * width].astype(F32)
        mixed_ref[:, j * width : (j + 1) * width] = block
        part = jnp.sum(block * block, axis=-1, keepdims=True)
        square = part if square is None else square + part
    scale = lax.rsqrt(square * (1.0 / (8 * width)) + EPS)
    normed = (mixed_ref[...] * scale * gain_ref[...]).astype(BF16)
    normed_ref[...] = normed
    copies[9].start()
    copies[10].start()
    span = place_ref.shape[0] // PAIRS
    part = normed.shape[1] // QUARTERS
    for c in range(PAIRS):
        slots = jnp.dot(
            place_ref[c * span : (c + 1) * span, :], normed, preferred_element_type=F32
        ).astype(BF16)

        def write(g, block):
            wire_ref[g * 128 : (g + 1) * 128, c * part : (c + 1) * part] = block

        fold(slots, write)
    copies[9].wait()
    copies[10].wait()


def project(columns, heads, pieces, residual, gain, place):
    tokens, width = residual.shape
    peers = place.shape[0] // CAP
    vmem = pl.BlockSpec(memory_space=pltpu.VMEM)
    return pl.pallas_call(
        project_kernel,
        in_specs=[pl.BlockSpec(memory_space=pltpu.SMEM), vmem]
        + [pl.BlockSpec(memory_space=pl.ANY)] * 9
        + [vmem] * 2,
        out_specs=[pl.BlockSpec(memory_space=pl.ANY)] * 2 + [vmem],
        out_shape=(
            pltpu.HBM((tokens, width), F32),
            pltpu.HBM((tokens, width), BF16),
            pltpu.VMEM((peers * 8, width * CAP // 8), BF16),
        ),
        scratch_shapes=[
            pltpu.VMEM((8,) + pieces[0].shape, BF16),
            pltpu.VMEM(residual.shape, BF16),
            pltpu.VMEM((8, tokens, width // 8), F32),
            pltpu.VMEM((tokens, width), F32),
            pltpu.VMEM((tokens, width), BF16),
            pltpu.SemaphoreType.DMA((11,)),
        ],
        compiler_params=limit(32),
        name="project",
    )(
        columns,
        local(heads),
        *(distant(piece) for piece in pieces),
        distant(residual),
        gain,
        local(place),
    )


def expert_kernel(wire_ref, gate_ref, up_ref, down_ref, out_hbm, rows_ref, out_ref, sems):
    part = wire_ref.shape[1] // PAIRS
    span = rows_ref.shape[0] // PAIRS
    for c in range(PAIRS):
        unfold(
            wire_ref.at[:, pl.ds(c * part, part)], rows_ref.at[pl.ds(c * span, span)]
        )
    rows = rows_ref[...]
    gate = jnp.dot(rows, gate_ref[...], preferred_element_type=F32)
    up = jnp.dot(rows, up_ref[...], preferred_element_type=F32)
    hidden = (gate / (1.0 + jnp.exp(-gate)) * up).astype(BF16)
    copies = []
    for c in range(PAIRS):
        output = jnp.dot(
            hidden[c * span : (c + 1) * span], down_ref[...], preferred_element_type=F32
        ).astype(BF16)

        def write(g, block):
            out_ref[g * 128 : (g + 1) * 128, c * part : (c + 1) * part] = block

        fold(output, write)
        lanes = pl.ds(c * part, part)
        copies.append(
            pltpu.make_async_copy(out_ref.at[:, lanes], out_hbm.at[:, lanes], sems.at[c])
        )
        copies[c].start()
    for copy in copies:
        copy.wait()


def expert(wire, gate, up, down):
    rows, width = wire.shape
    vmem = pl.BlockSpec(memory_space=pltpu.VMEM)
    return pl.pallas_call(
        expert_kernel,
        in_specs=[vmem] * 4,
        out_specs=pl.BlockSpec(memory_space=pl.ANY),
        out_shape=pltpu.HBM(wire.shape, BF16),
        scratch_shapes=[
            pltpu.VMEM((rows * CAP // 8, width * 8 // CAP), BF16),
            pltpu.VMEM(wire.shape, BF16),
            pltpu.SemaphoreType.DMA((PAIRS,)),
        ],
        compiler_params=limit(32),
        name="expert",
    )(local(wire), local(gate), local(up), local(down))


def shared_kernel(normed_ref, mixed_ref, gate_ref, up_ref, down_ref, out_ref):
    rows = normed_ref[...]
    gate = jnp.dot(rows, gate_ref[...], preferred_element_type=F32)
    up = jnp.dot(rows, up_ref[...], preferred_element_type=F32)
    hidden = (gate / (1.0 + jnp.exp(-gate)) * up).astype(BF16)
    output = jnp.dot(hidden, down_ref[...], preferred_element_type=F32)

    @pl.when(pl.program_id(0) == 0)
    def _():
        out_ref[...] = mixed_ref[...] + output

    @pl.when(pl.program_id(0) > 0)
    def _():
        out_ref[...] = out_ref[...] + output


def shared(normed, mixed, gate, up, down):
    block = 256

    def whole(array):
        return pl.BlockSpec(array.shape, lambda i: (0, 0))

    columns = pl.BlockSpec((gate.shape[0], block), lambda i: (0, i))
    return pl.pallas_call(
        shared_kernel,
        grid=(gate.shape[1] // block,),
        in_specs=[
            whole(normed),
            whole(mixed),
            columns,
            columns,
            pl.BlockSpec((block, down.shape[1]), lambda i: (i, 0)),
        ],
        out_specs=whole(mixed),
        out_shape=pltpu.HBM(mixed.shape, F32),
        compiler_params=limit(20),
        name="shared",
    )(*(distant(array) for array in (normed, mixed, gate, up, down)))


def combine_kernel(wire_ref, gates_ref, base_hbm, out_ref, rows_ref, base_ref, sem):
    copy = pltpu.make_async_copy(base_hbm, base_ref, sem)
    copy.start()
    gates = gates_ref[...]
    tokens = gates.shape[0]
    high = gates.astype(BF16)
    rest = gates - high.astype(F32)
    middle = rest.astype(BF16)
    low = (rest - middle.astype(F32)).astype(BF16)
    stacked = jnp.concatenate([high, middle, low], axis=0)
    part = wire_ref.shape[1] // PAIRS
    span = rows_ref.shape[0] // PAIRS
    for c in range(PAIRS):
        unfold(
            wire_ref.at[:, pl.ds(c * part, part)], rows_ref.at[pl.ds(c * span, span)]
        )
    copy.wait()
    block = 512
    for n in range(base_ref.shape[1] // block):
        lanes = slice(n * block, (n + 1) * block)
        parts = jnp.dot(stacked, rows_ref[:, lanes], preferred_element_type=F32)
        routed = parts[:tokens] + (parts[tokens : 2 * tokens] + parts[2 * tokens :])
        out_ref[:, lanes] = (base_ref[:, lanes] + routed).astype(BF16)


def combine(wire, gates, base):
    rows, width = wire.shape
    vmem = pl.BlockSpec(memory_space=pltpu.VMEM)
    return pl.pallas_call(
        combine_kernel,
        in_specs=[vmem, vmem, pl.BlockSpec(memory_space=pl.ANY)],
        out_specs=vmem,
        out_shape=jax.ShapeDtypeStruct(base.shape, BF16),
        scratch_shapes=[
            pltpu.VMEM((rows * CAP // 8, width * 8 // CAP), BF16),
            pltpu.VMEM(base.shape, F32),
            pltpu.SemaphoreType.DMA,
        ],
        compiler_params=limit(24),
        name="combine",
    )(local(wire), local(gates), distant(base))


def shift(values, target):
    size = lax.axis_size("dp")

    def place(d):
        x, core = target(d // 2, d % 2)
        return 2 * (x % (size // 2)) + core

    return lax.ppermute(values, "dp", [(d, place(d)) for d in range(size)])


def apart(x, core):
    return x + 1 - 2 * core, core


def across(x, core):
    return x - 1 + 2 * core, core


def partner(x, core):
    return x, 1 - core


def per_device(
    residual,
    query,
    key_value,
    out_weight,
    norm_gain,
    query_gain,
    key_gain,
    route_ids,
    route_weights,
    shared_gate,
    shared_up,
    shared_down,
    expert_gate,
    expert_up,
    expert_down,
):
    tokens, width = residual.shape[1:]
    experts = expert_gate.shape[0] * lax.axis_size(("sp", "dp"))
    ring = lax.axis_size("dp") // 2
    blocks = lax.axis_size("sp")

    near = shift(out_weight, apart)
    other = shift(out_weight, across)
    own_pair = shift(out_weight, partner)
    outgoing = prepare(
        query[0], key_value[0], query_gain, key_gain, lax.axis_index("sp"), blocks
    )
    rows = lax.all_to_all(outgoing, "sp", split_axis=0, concat_axis=0, tiled=True)
    rows, near, other = lax.optimization_barrier((rows, near, other))
    far = shift(near, apart)
    near_pair = shift(near, partner)
    other_pair = shift(other, partner)
    attention = attend(rows.reshape(-1, rows.shape[2]))
    far, ids, _ = lax.optimization_barrier((far, route_ids[0], attention))
    place, gates = route(ids, route_weights[0], experts)
    far_pair = shift(far, partner)
    heads = lax.all_to_all(
        attention.reshape(-1, tokens, attention.shape[1]), "sp", split_axis=0, concat_axis=0, tiled=True
    )

    me = lax.axis_index("dp")
    x, core = me // 2, me % 2
    away = 1 - 2 * core
    steps = jnp.array([0, 0, -1, 1, 1, -1, 2, 2], jnp.int32) * away
    flips = jnp.array([0, 1, 0, 0, 1, 1, 0, 1], jnp.int32)
    columns = 2 * ((x + steps) % ring) + (core + flips) % 2
    pieces = [out_weight, own_pair, near, other, near_pair, other_pair, far, far_pair]
    mixed, normed, wire = project(
        columns, heads, pieces, residual[0], norm_gain.reshape(1, -1), place
    )
    wire_shape = (wire.shape[0] // 8, 8, wire.shape[1])

    def exchange(values):
        return lax.all_to_all(
            values.reshape(wire_shape), ("sp", "dp"), split_axis=0, concat_axis=0, tiled=True
        ).reshape(values.shape)

    arrived = exchange(wire)
    base = shared(normed, mixed, shared_gate, shared_up, shared_down)
    output = expert(arrived, expert_gate[0], expert_up[0], expert_down[0])
    returned = exchange(output)
    return combine(returned, gates, base).reshape(1, tokens, width)


def solution(mesh):
    in_specs = (
        P("dp", "sp", None),
        P("dp", "sp", None, None),
        P("dp", "sp", None, None),
        P(None, "dp"),
        P(),
        P(),
        P(),
        P("dp", "sp", None),
        P("dp", "sp", None),
        P(),
        P(),
        P(),
        P(("sp", "dp"), None, None),
        P(("sp", "dp"), None, None),
        P(("sp", "dp"), None, None),
    )
    out_specs = P("dp", "sp", None)
    return jax.shard_map(
        per_device, mesh=mesh, in_specs=in_specs, out_specs=out_specs, check_vma=False
    )
```

time: 212 us -> 181 us (0.85)
  Pallas kernels: 51.5 us -> 39.2 us
  local copies, waits for them, and re-layouts: 14.8 us -> 5.32 us
  other arithmetic: 7.66 us -> 0.01 us
  waiting for transfers between devices: 39.7 us -> 46.8 us
  matrix products: 5.43 us -> 0 us
  blocking collectives: 72.1 us -> 69.9 us
    gather x4 -> x0, local copies, waits for them, and re-layouts: 6.35 us -> none  [the longest x2 3.18 us: tables(): gain[up]]
    all_to_all x1, waiting for transfers between devices: 3.79 us -> 10 us  [per_device(): lax.all_to_all(attention.reshape(-1, tokens, attention.shape[1]), 'sp', s...]
    pallas_call x1, Pallas kernels: 16.7 us -> 10.9 us  [attend(): pl.pallas_call(attend_kernel, grid=(length // block,), in_specs=[pl.Block...]
    dot_general x2 -> x0, matrix products: 5.43 us -> none  [the longest x1 3.39 us: swiglu(): return jnp.dot(hidden, down_weight, preferred_element_type=F32)]
    pallas_call x4 -> x5, Pallas kernels: 25 us -> 20.9 us  [the longest x1 8.06 us: expert(): pl.pallas_call(expert_kernel, in_specs=[vmem] * 4, out_specs=pl.BlockSpec...]
    slice x2 -> x0, local copies, waits for them, and re-layouts: 3.15 us -> none  [the longest x1 2.32 us: per_device(): far_top = shift(from_left[:half], right)]
    concatenate x2 -> x0, other arithmetic: 3.14 us -> none  [the longest x1 2.33 us: per_device(): far = jnp.concatenate([far_top, far_bottom], axis=0)]
    unnamed x22 -> x32, local copies, waits for them, and re-layouts: 2.27 us -> 5.32 us
  transfers between devices with their start and end apart: 11 -> 9, of which waited for: 2 -> 3; matrix products, arithmetic and copies ran while one was open for 11% -> 0% of each run, Pallas kernels for 11% -> 11%
where the time goes in v2:
time: 181 us; the launch traced here: 180 us
  blocking collectives  69.9 us (39%)
  waiting for transfers between devices  46.8 us (26%)
  Pallas kernels  39.2 us (22%)
  starting transfers between devices  18.4 us (10%)
  local copies, waits for them, and re-layouts  5.32 us (3%)
    all_to_all x1, blocking collectives, exchange(): lax.all_to_all(values.reshape(wire_shape), ('sp', 'dp'), split_axis=0, co...  46 us
    all_to_all x1, waiting for transfers between devices, exchange(): lax.all_to_all(values.reshape(wire_shape), ('sp', 'dp'), split_axis=0, co...  36.3 us
    all_to_all x1, blocking collectives, per_device(): lax.all_to_all(outgoing, 'sp', split_axis=0, concat_axis=0, tiled=True)  23.9 us
    pallas_call x1, Pallas kernels, attend(): pl.pallas_call(attend_kernel, grid=(length // block,), in_specs=[pl.Block...  10.9 us
    ppermute x7, starting transfers between devices, shift(): return lax.ppermute(values, 'dp', [(d, place(d)) for d in range(size)])  10.1 us
    all_to_all x1, waiting for transfers between devices, per_device(): lax.all_to_all(attention.reshape(-1, tokens, attention.shape[1]), 'sp', s...  10 us
    pallas_call x1, Pallas kernels, expert(): pl.pallas_call(expert_kernel, in_specs=[vmem] * 4, out_specs=pl.BlockSpec...  8.06 us
    pallas_call x1, Pallas kernels, project(): pl.pallas_call(project_kernel, in_specs=[pl.BlockSpec(memory_space=pltpu....  7.46 us
  transfers between devices with their start and end apart: 9, of which 3 were waited for; matrix products, arithmetic and copies ran while one was open for 0% of the time, Pallas kernels for 11%

profile of v2, /device:TPU:1, one launch (start us, length us, event | category | flops | bytes accessed | tf_op | source)
XLA Modules:
  0.0 180.0 jit_solution(2082810557001169182)
XLA Ops:
  0.0 2.0 %collective-permute-start.1 = (bf16[2048,256]{1,0:T(8,128)(2,1)}, bf16[2048,256]{1,0:T(8,128)(2,1)}, u32[]{:S(2)}, u32[]{:S(2)}) collective-permute-start(bf16[2048,256]{1,0:T(8,128)(2,1)} %refs_0_.1), channel_id=1, source_target_pairs={{0,6},{1,3},{2,0},{3,5},{4,2},{5,7},{6,4},{7,1},{8,14},{9,11},{10,... | collective-permute-start | bytes 3145736 | tf_op jit(solution)/shard_map/ppermute | solution.py:481
  2.0 1.3 collective-permute-start
  3.3 1.0 copy-done.3
  4.3 1.0 copy-done.4
  5.4 0.9 copy-done.5
  6.3 0.8 copy-done.6
  7.0 0.7 copy-done.8
  7.7 0.7 copy-done.9
  8.4 2.1 %prepare.1 = bf16[16,128,256]{2,1,0:T(8,128)(2,1)S(1)} custom-call(s32[1]{0:T(128)} %bitcast.block_ref, bf16[128,16,128]{2,1,0:T(8,128)(2,1)S(1)} %bitcast.27, bf16[128,16,128]{2,1,0:T(8,128)(2,1)S(1)} %bitcast.28, f32[2,128,128]{2,1,0:T(8,128)S(1)} %copy-done.5, f32[16,2,2,128]{3,2,1,0:T(2,128)S(1)} %copy-done.6, f32[1,64]{1,0:T(1,128)S(1)} %bitcast.32, ...), custom_call_target="tpu_custom_call" | custom-call | tf_op jit(solution)/shard_map/prepare/pallas_call | solution.py:121
  10.5 23.9 %all_to_all.20 = bf16[16,128,256]{2,1,0:T(8,128)(2,1)S(1)} all-to-all(bf16[16,128,256]{2,1,0:T(8,128)(2,1)S(1)} %prepare.1), channel_id=1, replica_groups=mesh['sp'=16,'dp'=8] {'sp'}, dimensions={0} | all-to-all | bytes 2097152 | tf_op jit(solution)/shard_map/all_to_all | solution.py:524
  34.4 0.1 collective-permute-start.5
  34.5 2.2 %collective-permute-start.2 = (bf16[2048,256]{1,0:T(8,128)(2,1)S(1)}, bf16[2048,256]{1,0:T(8,128)(2,1)}, u32[]{:S(2)}, u32[]{:S(2)}) collective-permute-start(bf16[2048,256]{1,0:T(8,128)(2,1)S(1)} %copy-done.10), channel_id=1, source_target_pairs={{0,1},{1,0},{2,3},{3,2},{4,5},{5,4},{6,7},{7,6},{8,9},{9,8},{10,11... | collective-permute-start | bytes 3145736 | tf_op jit(solution)/shard_map/ppermute | solution.py:481
  36.7 0.1 copy.20
  36.8 0.1 collective-permute-start.3
  36.9 10.9 %attend.1 = bf16[2048,128]{1,0:T(8,128)(2,1)} custom-call(bf16[2048,256]{1,0:T(8,128)(2,1)S(1)} %bitcast.21, bf16[2048,256]{1,0:T(8,128)(2,1)S(1)} %bitcast.22), custom_call_target="tpu_custom_call" | custom-call | tf_op jit(solution)/shard_map/attend/pallas_call | solution.py:185
  47.8 0.5 collective-permute-start.4
  48.3 0.4 collective-permute-done.5.refs_6_
  48.8 4.0 %collective-permute-start.6 = (bf16[2048,256]{1,0:T(8,128)(2,1)}, bf16[2048,256]{1,0:T(8,128)(2,1)}, u32[]{:S(2)}, u32[]{:S(2)}) collective-permute-start(bf16[2048,256]{1,0:T(8,128)(2,1)} %collective-permute-done.5.refs_6_), channel_id=1, source_target_pairs={{0,1},{1,0},{2,3},{3,2},{4,5},{5,4},{6,7},{7,6},{8,9},{9,8},{10,11... | collective-permute-start | bytes 3145736 | tf_op jit(solution)/shard_map/ppermute | solution.py:481
  52.8 3.6 %all-to-all-start.1 = ((bf16[16,128,128]{2,1,0:T(8,128)(2,1)}), bf16[16,128,128]{2,1,0:T(8,128)(2,1)S(1)}, u32[]{:S(2)}, u32[]{:S(2)}) async-start(bf16[16,128,128]{2,1,0:T(8,128)(2,1)} %bitcast.35), calls=%async_computation.1 | async-start | bytes 1048576 | tf_op jit(solution)/shard_map/all_to_all | solution.py:533
  56.4 0.1 copy.21
  56.5 1.1 route.1
  57.6 10.0 %all-to-all-done.1.heads_ref = bf16[16,128,128]{2,1,0:T(8,128)(2,1)S(1)} async-done(((bf16[16,128,128]{2,1,0:T(8,128)(2,1)}), bf16[16,128,128]{2,1,0:T(8,128)(2,1)S(1)}, u32[]{:S(2)}, u32[]{:S(2)}) %all-to-all-start.1) | async-done | bytes 524320 | tf_op jit(solution)/shard_map/all_to_all | solution.py:533
  67.7 7.5 %project.1 = (f32[128,2048]{1,0:T(8,128)}, bf16[128,2048]{1,0:T(8,128)(2,1)}, bf16[1024,1536]{1,0:T(8,128)(2,1)S(1)}) custom-call(s32[8]{0:T(128)S(1)} %fusion.columns_ref, bf16[16,128,128]{2,1,0:T(8,128)(2,1)S(1)} %all-to-all-done.1.heads_ref, bf16[2048,256]{1,0:T(8,128)(2,1)} %refs_0_.1, bf16[2048,256]{1,0:T(8,128)(2,1)} %collective-permute-done.2.refs_1_, ...), custom_call_target="tpu_custom_call" | custom-call | tf_op jit(solution)/shard_map/project/pallas_call | solution.py:312
  75.1 0.0 copy-start
  75.2 0.0 copy-start.1
  75.2 0.0 copy-start.2
  75.2 46.0 %all_to_all.21 = bf16[128,8,1536]{2,1,0:T(8,128)(2,1)S(1)} all-to-all(bf16[128,8,1536]{2,1,0:T(8,128)(2,1)S(1)} %bitcast.23), channel_id=1, replica_groups=mesh['sp'=16,'dp'=8] {'sp','dp'}, dimensions={0} | all-to-all | bytes 6291456 | tf_op jit(solution)/shard_map/all_to_all | solution.py:550
  121.2 8.1 %expert.1 = bf16[1024,1536]{1,0:T(8,128)(2,1)} custom-call(bf16[1024,1536]{1,0:T(8,128)(2,1)S(1)} %bitcast.20, bf16[2048,512]{1,0:T(8,128)(2,1)S(1)} %bitcast.24, bf16[2048,512]{1,0:T(8,128)(2,1)S(1)} %bitcast.25, bf16[512,2048]{1,0:T(8,128)(2,1)S(1)} %bitcast.26), custom_call_target="tpu_custom_call" | custom-call | tf_op jit(solution)/shard_map/expert/pallas_call | solution.py:376
  129.3 4.7 %all-to-all-start.3 = ((bf16[128,8,1536]{2,1,0:T(8,128)(2,1)}), bf16[128,8,1536]{2,1,0:T(8,128)(2,1)S(1)}, u32[]{:S(2)}, u32[]{:S(2)}) async-start(bf16[128,8,1536]{2,1,0:T(8,128)(2,1)} %bitcast.34), calls=%async_computation.3 | async-start | bytes 6291456 | tf_op jit(solution)/shard_map/all_to_all | solution.py:550
  133.9 5.3 %shared.1.base_hbm = f32[128,2048]{1,0:T(8,128)} custom-call(bf16[128,2048]{1,0:T(8,128)(2,1)} %get-tuple-element.23.normed_ref, f32[128,2048]{1,0:T(8,128)} %get-tuple-element.24.mixed_ref, bf16[2048,512]{1,0:T(8,128)(2,1)} %gate_ref.1, bf16[2048,512]{1,0:T(8,128)(2,1)} %up_ref.1, bf16[512,2048]{1,0:T(8,128)(2,1)} %down_ref.1), custom_call_target="tpu_custom_call" | custom-call | tf_op jit(solution)/shard_map/shared/pallas_call | solution.py:414
  139.2 36.3 %all-to-all-done.3 = bf16[128,8,1536]{2,1,0:T(8,128)(2,1)S(1)} async-done(((bf16[128,8,1536]{2,1,0:T(8,128)(2,1)}), bf16[128,8,1536]{2,1,0:T(8,128)(2,1)S(1)}, u32[]{:S(2)}, u32[]{:S(2)}) %all-to-all-start.3) | async-done | bytes 3145760 | tf_op jit(solution)/shard_map/all_to_all | solution.py:550
  175.6 4.3 %combine.1 = bf16[128,2048]{1,0:T(8,128)(2,1)} custom-call(bf16[1024,1536]{1,0:T(8,128)(2,1)S(1)} %bitcast.19, f32[128,768]{1,0:T(8,128)S(1)} %get-tuple-element.22.gates_ref, f32[128,2048]{1,0:T(8,128)} %shared.1.base_hbm), custom_call_target="tpu_custom_call" | custom-call | tf_op jit(solution)/shard_map/combine/pallas_call | solution.py:459
  (28 shorter events, 0.1 us)
Async XLA Ops:
  0.0 34.4 %collective-permute-start.1 = (bf16[2048,256]{1,0:T(8,128)(2,1)}, bf16[2048,256]{1,0:T(8,128)(2,1)}, u32[]{:S(2)}, u32[]{:S(2)}) collective-permute-start(bf16[2048,256]{1,0:T(8,128)(2,1)} %refs_0_.1), channel_id=1, source_target_pairs={{0,6},{1,3},{2,0},{3,5},{4,2},{5,7},{6,4},{7,1},{8,14},{9,11},{10,... | collective-permute-start | bytes 3145736 | tf_op jit(solution)/shard_map/ppermute | solution.py:481
  2.0 32.4 %collective-permute-start = (bf16[2048,256]{1,0:T(8,128)(2,1)}, bf16[2048,256]{1,0:T(8,128)(2,1)}, u32[]{:S(2)}, u32[]{:S(2)}) collective-permute-start(bf16[2048,256]{1,0:T(8,128)(2,1)} %refs_0_.1), channel_id=1, source_target_pairs={{0,2},{1,7},{2,4},{3,1},{4,6},{5,3},{6,0},{7,5},{8,10},{9,15},{10,... | collective-permute-start | bytes 3145736 | tf_op jit(solution)/shard_map/ppermute | solution.py:481
  3.3 1.0 copy-start.3
  4.3 1.0 copy-start.4
  5.4 0.9 copy-start.5
  6.3 0.8 copy-start.6
  7.0 0.7 copy-start.8
  7.7 0.7 copy-start.9
  8.4 26.2 %copy-start.10 = (bf16[2048,256]{1,0:T(8,128)(2,1)S(1)}, bf16[2048,256]{1,0:T(8,128)(2,1)}, u32[]{:S(2)}) copy-start(bf16[2048,256]{1,0:T(8,128)(2,1)} %refs_0_.1) | copy-start | bytes 3145732
  8.4 28.4 %copy-start.11 = (s32[1,128,4]{1,2,0:T(4,128)S(1)}, s32[1,128,4]{1,2,0:T(4,128)}, u32[]{:S(2)}) copy-start(s32[1,128,4]{1,2,0:T(4,128)} %param.26) | copy-start | bytes 6148
  34.4 22.0 %copy-start.12 = (f32[1,128,4]{1,2,0:T(4,128)S(1)}, f32[1,128,4]{1,2,0:T(4,128)}, u32[]{:S(2)}) copy-start(f32[1,128,4]{1,2,0:T(4,128)} %param.27) | copy-start | bytes 6148
  34.4 22.1 %copy-start.13 = (s32[8]{0:T(128)S(1)}, s32[8]{0:T(128)}, u32[]{:S(2)}) copy-start(s32[8]{0:T(128)} %constant.65.clone) | copy-start | bytes 100
  34.4 22.1 %copy-start.14 = (s32[8]{0:T(128)S(1)}, s32[8]{0:T(128)}, u32[]{:S(2)}) copy-start(s32[8]{0:T(128)} %constant.64.clone) | copy-start | bytes 100
  34.4 33.3 %copy-start.7 = (f32[2048]{0:T(1024)S(1)}, f32[2048]{0:T(1024)}, u32[]{:S(2)}) copy-start(f32[2048]{0:T(1024)} %param.23) | copy-start | bytes 24580
  34.4 14.3 %collective-permute-start.5 = (bf16[2048,256]{1,0:T(8,128)(2,1)}, bf16[2048,256]{1,0:T(8,128)(2,1)}, u32[]{:S(2)}, u32[]{:S(2)}) collective-permute-start(bf16[2048,256]{1,0:T(8,128)(2,1)} %collective-permute-done.refs_2_), channel_id=1, source_target_pairs={{0,2},{1,7},{2,4},{3,1},{4,6},{5,3},{6,0},{7,5},{8,10},{9,15},{10,... | collective-permute-start | bytes 3145736 | tf_op jit(solution)/shard_map/ppermute | solution.py:481
  34.5 23.1 %collective-permute-start.2 = (bf16[2048,256]{1,0:T(8,128)(2,1)S(1)}, bf16[2048,256]{1,0:T(8,128)(2,1)}, u32[]{:S(2)}, u32[]{:S(2)}) collective-permute-start(bf16[2048,256]{1,0:T(8,128)(2,1)S(1)} %copy-done.10), channel_id=1, source_target_pairs={{0,1},{1,0},{2,3},{3,2},{4,5},{5,4},{6,7},{7,6},{8,9},{9,8},{10,11... | collective-permute-start | bytes 3145736 | tf_op jit(solution)/shard_map/ppermute | solution.py:481
  36.8 30.8 %collective-permute-start.3 = (bf16[2048,256]{1,0:T(8,128)(2,1)}, bf16[2048,256]{1,0:T(8,128)(2,1)}, u32[]{:S(2)}, u32[]{:S(2)}) collective-permute-start(bf16[2048,256]{1,0:T(8,128)(2,1)} %collective-permute-done.refs_2_), channel_id=1, source_target_pairs={{0,1},{1,0},{2,3},{3,2},{4,5},{5,4},{6,7},{7,6},{8,9},{9,8},{10,11... | collective-permute-start | bytes 3145736 | tf_op jit(solution)/shard_map/ppermute | solution.py:481
  47.8 19.8 %collective-permute-start.4 = (bf16[2048,256]{1,0:T(8,128)(2,1)}, bf16[2048,256]{1,0:T(8,128)(2,1)}, u32[]{:S(2)}, u32[]{:S(2)}) collective-permute-start(bf16[2048,256]{1,0:T(8,128)(2,1)} %collective-permute-done.1.refs_3_), channel_id=1, source_target_pairs={{0,1},{1,0},{2,3},{3,2},{4,5},{5,4},{6,7},{7,6},{8,9},{9,8},{10,11... | collective-permute-start | bytes 3145736 | tf_op jit(solution)/shard_map/ppermute | solution.py:481
  48.8 18.9 %collective-permute-start.6 = (bf16[2048,256]{1,0:T(8,128)(2,1)}, bf16[2048,256]{1,0:T(8,128)(2,1)}, u32[]{:S(2)}, u32[]{:S(2)}) collective-permute-start(bf16[2048,256]{1,0:T(8,128)(2,1)} %collective-permute-done.5.refs_6_), channel_id=1, source_target_pairs={{0,1},{1,0},{2,3},{3,2},{4,5},{5,4},{6,7},{7,6},{8,9},{9,8},{10,11... | collective-permute-start | bytes 3145736 | tf_op jit(solution)/shard_map/ppermute | solution.py:481
  52.8 14.9 %all-to-all-start.1 = ((bf16[16,128,128]{2,1,0:T(8,128)(2,1)}), bf16[16,128,128]{2,1,0:T(8,128)(2,1)S(1)}, u32[]{:S(2)}, u32[]{:S(2)}) async-start(bf16[16,128,128]{2,1,0:T(8,128)(2,1)} %bitcast.35), calls=%async_computation.1 | async-start | bytes 1048576 | tf_op jit(solution)/shard_map/all_to_all | solution.py:533
  75.1 46.1 %copy-start = (bf16[1,2048,512]{2,1,0:T(8,128)(2,1)S(1)}, bf16[1,2048,512]{2,1,0:T(8,128)(2,1)}, u32[]{:S(2)}) copy-start(bf16[1,2048,512]{2,1,0:T(8,128)(2,1)} %param.31) | copy-start | bytes 6291460
  75.2 46.0 %copy-start.1 = (bf16[1,2048,512]{2,1,0:T(8,128)(2,1)S(1)}, bf16[1,2048,512]{2,1,0:T(8,128)(2,1)}, u32[]{:S(2)}) copy-start(bf16[1,2048,512]{2,1,0:T(8,128)(2,1)} %param.32) | copy-start | bytes 6291460
  75.2 46.0 %copy-start.2 = (bf16[1,512,2048]{2,1,0:T(8,128)(2,1)S(1)}, bf16[1,512,2048]{2,1,0:T(8,128)(2,1)}, u32[]{:S(2)}) copy-start(bf16[1,512,2048]{2,1,0:T(8,128)(2,1)} %param.33) | copy-start | bytes 6291460
  129.3 46.3 %all-to-all-start.3 = ((bf16[128,8,1536]{2,1,0:T(8,128)(2,1)}), bf16[128,8,1536]{2,1,0:T(8,128)(2,1)S(1)}, u32[]{:S(2)}, u32[]{:S(2)}) async-start(bf16[128,8,1536]{2,1,0:T(8,128)(2,1)} %bitcast.34), calls=%async_computation.3 | async-start | bytes 6291456 | tf_op jit(solution)/shard_map/all_to_all | solution.py:550

commit v3 on v2

--- a/solution.py
+++ b/solution.py
@@ -5,6 +5,7 @@
 from jax.experimental import pallas as pl
 from jax.experimental.pallas import tpu as pltpu
 from jax.sharding import PartitionSpec as P
+
 
 GRID_W = 64
 HD = 64
@@ -137,7 +138,10 @@
         out_shape=jax.ShapeDtypeStruct((heads, tokens, 2 * width), BF16),
         compiler_params=limit(16),
         name="prepare",
-    )(jnp.full((1,), block, jnp.int32), query, pair, col, row, *gains)
+    )(
+        jnp.full((1,), block, jnp.int32),
+        *(distant(array) for array in (query, pair, jnp.asarray(col), jnp.asarray(row), *gains)),
+    )
 
 
 def attend_kernel(q_ref, kv_ref, out_ref, keys_ref, values_ref):
@@ -221,7 +225,7 @@
 
 
 def route(ids, weights, experts):
-    tokens, top = ids.shape
+    tokens, _ = ids.shape
     return pl.pallas_call(
         route_kernel,
         out_shape=(
@@ -517,22 +521,22 @@
 
     near = shift(out_weight, apart)
     other = shift(out_weight, across)
-    own_pair = shift(out_weight, partner)
-    outgoing = prepare(
-        query[0], key_value[0], query_gain, key_gain, lax.axis_index("sp"), blocks
-    )
+    outgoing = prepare(query[0], key_value[0], query_gain, key_gain, lax.axis_index("sp"), blocks)
     rows = lax.all_to_all(outgoing, "sp", split_axis=0, concat_axis=0, tiled=True)
     rows, near, other = lax.optimization_barrier((rows, near, other))
     far = shift(near, apart)
-    near_pair = shift(near, partner)
-    other_pair = shift(other, partner)
     attention = attend(rows.reshape(-1, rows.shape[2]))
-    far, ids, _ = lax.optimization_barrier((far, route_ids[0], attention))
-    place, gates = route(ids, route_weights[0], experts)
-    far_pair = shift(far, partner)
+    place, gates = route(route_ids[0], route_weights[0], experts)
     heads = lax.all_to_all(
-        attention.reshape(-1, tokens, attention.shape[1]), "sp", split_axis=0, concat_axis=0, tiled=True
+        attention.reshape(-1, tokens, attention.shape[1]),
+        "sp",
+        split_axis=0,
+        concat_axis=0,
+        tiled=True,
     )
+    own_pair, near_pair, other_pair, far_pair = [
+        shift(piece, partner) for piece in (out_weight, near, other, far)
+    ]
 
     me = lax.axis_index("dp")
     x, core = me // 2, me % 2

time: 181 us -> 187 us (1.033)
  waiting for transfers between devices: 46.8 us -> 57.8 us
  local copies, waits for them, and re-layouts: 5.32 us -> 0.27 us
    ppermute x7, waiting for transfers between devices: 0.45 us -> 11.6 us  [shift(): return lax.ppermute(values, 'dp', [(d, place(d)) for d in range(size)])]
    unnamed x32 -> x22, local copies, waits for them, and re-layouts: 5.32 us -> 0.27 us
where the time goes in v3:
time: 187 us
  blocking collectives  70 us (37%)
  waiting for transfers between devices  57.8 us (31%)
  Pallas kernels  40.2 us (21%)
  starting transfers between devices  18.2 us (10%)
    all_to_all x1, blocking collectives, exchange(): lax.all_to_all(values.reshape(wire_shape), ('sp', 'dp'), split_axis=0, co...  46 us
    all_to_all x1, waiting for transfers between devices, exchange(): lax.all_to_all(values.reshape(wire_shape), ('sp', 'dp'), split_axis=0, co...  36.3 us
    all_to_all x1, blocking collectives, per_device(): lax.all_to_all(outgoing, 'sp', split_axis=0, concat_axis=0, tiled=True)  24 us
    ppermute x7, waiting for transfers between devices, shift(): return lax.ppermute(values, 'dp', [(d, place(d)) for d in range(size)])  11.6 us
    pallas_call x1, Pallas kernels, attend(): pl.pallas_call(attend_kernel, grid=(length // block,), in_specs=[pl.Block...  10.9 us
    ppermute x7, starting transfers between devices, shift(): return lax.ppermute(values, 'dp', [(d, place(d)) for d in range(size)])  9.99 us
    all_to_all x1, waiting for transfers between devices, per_device(): lax.all_to_all(attention.reshape(-1, tokens, attention.shape[1]), 'sp', s...  9.89 us
    pallas_call x1, Pallas kernels, expert(): pl.pallas_call(expert_kernel, in_specs=[vmem] * 4, out_specs=pl.BlockSpec...  8.01 us
  transfers between devices with their start and end apart: 9, of which 3 were waited for; matrix products, arithmetic and copies ran while one was open for 0% of the time, Pallas kernels for 11%

profile of v3, /device:TPU:1, one launch (start us, length us, event | category | flops | bytes accessed | tf_op | source)
XLA Modules:
  0.0 186.9 jit_solution(4577105123098129063)
XLA Ops:
  0.0 2.0 %collective-permute-start.1 = (bf16[2048,256]{1,0:T(8,128)(2,1)}, bf16[2048,256]{1,0:T(8,128)(2,1)S(1)}, u32[]{:S(2)}, u32[]{:S(2)}) collective-permute-start(bf16[2048,256]{1,0:T(8,128)(2,1)} %refs_0_.1), channel_id=1, source_target_pairs={{0,6},{1,3},{2,0},{3,5},{4,2},{5,7},{6,4},{7,1},{8,14},{9,11},{10,... | collective-permute-start | bytes 3145736 | tf_op jit(solution)/shard_map/ppermute | solution.py:485
  2.0 1.3 collective-permute-start
  3.3 3.1 %prepare.1 = bf16[16,128,256]{2,1,0:T(8,128)(2,1)S(1)} custom-call(s32[1]{0:T(128)} %bitcast.block_ref, bf16[128,16,128]{2,1,0:T(8,128)(2,1)} %bitcast.32, bf16[128,16,128]{2,1,0:T(8,128)(2,1)} %bitcast.33, f32[2,128,128]{2,1,0:T(8,128)} %constant.62.clone.col_ref, f32[16,2,2,128]{3,2,1,0:T(2,128)} %constant.63.clone.row_ref, f32[1,64]{1,0:T(1,128)} %bitcast.35, ...), custom_call_target="tpu_custom_call" | custom-call | tf_op jit(solution)/shard_map/prepare/pallas_call | solution.py:122
  6.4 24.0 %all_to_all.20 = bf16[16,128,256]{2,1,0:T(8,128)(2,1)S(1)} all-to-all(bf16[16,128,256]{2,1,0:T(8,128)(2,1)S(1)} %prepare.1), channel_id=1, replica_groups=mesh['sp'=16,'dp'=8] {'sp'}, dimensions={0} | all-to-all | bytes 2097152 | tf_op jit(solution)/shard_map/all_to_all | solution.py:525
  30.4 0.0 copy-start.3
  30.4 0.0 collective-permute-done.1.refs_3_
  30.4 0.0 collective-permute-done.refs_2_
  30.5 0.1 collective-permute-start.5
  30.6 2.2 %collective-permute-start.2 = (bf16[2048,256]{1,0:T(8,128)(2,1)S(1)}, bf16[2048,256]{1,0:T(8,128)(2,1)}, u32[]{:S(2)}, u32[]{:S(2)}) collective-permute-start(bf16[2048,256]{1,0:T(8,128)(2,1)S(1)} %copy-done.4), channel_id=1, source_target_pairs={{0,1},{1,0},{2,3},{3,2},{4,5},{5,4},{6,7},{7,6},{8,9},{9,8},{10,11... | collective-permute-start | bytes 3145736 | tf_op jit(solution)/shard_map/ppermute | solution.py:485
  32.7 0.0 collective-permute-start.3
  32.7 0.5 collective-permute-start.4
  33.2 11.6 %collective-permute-done.5.refs_6_ = bf16[2048,256]{1,0:T(8,128)(2,1)} collective-permute-done((bf16[2048,256]{1,0:T(8,128)(2,1)}, bf16[2048,256]{1,0:T(8,128)(2,1)}, u32[]{:S(2)}, u32[]{:S(2)}) %collective-permute-start.5) | collective-permute-done | bytes 1048608 | tf_op jit(solution)/shard_map/ppermute | solution.py:485
  44.8 4.0 %collective-permute-start.6 = (bf16[2048,256]{1,0:T(8,128)(2,1)}, bf16[2048,256]{1,0:T(8,128)(2,1)}, u32[]{:S(2)}, u32[]{:S(2)}) collective-permute-start(bf16[2048,256]{1,0:T(8,128)(2,1)} %collective-permute-done.5.refs_6_), channel_id=1, source_target_pairs={{0,1},{1,0},{2,3},{3,2},{4,5},{5,4},{6,7},{7,6},{8,9},{9,8},{10,11... | collective-permute-start | bytes 3145736 | tf_op jit(solution)/shard_map/ppermute | solution.py:485
  48.7 10.9 %attend.1 = bf16[2048,128]{1,0:T(8,128)(2,1)} custom-call(bf16[2048,256]{1,0:T(8,128)(2,1)S(1)} %bitcast.21, bf16[2048,256]{1,0:T(8,128)(2,1)S(1)} %bitcast.22), custom_call_target="tpu_custom_call" | custom-call | tf_op jit(solution)/shard_map/attend/pallas_call | solution.py:189
  59.6 3.6 %all-to-all-start.1 = ((bf16[16,128,128]{2,1,0:T(8,128)(2,1)}), bf16[16,128,128]{2,1,0:T(8,128)(2,1)S(1)}, u32[]{:S(2)}, u32[]{:S(2)}) async-start(bf16[16,128,128]{2,1,0:T(8,128)(2,1)} %bitcast.31), calls=%async_computation.1 | async-start | bytes 1048576 | tf_op jit(solution)/shard_map/all_to_all | solution.py:530
  63.3 0.1 copy.20
  63.4 0.1 copy.21
  63.5 1.1 route.1
  64.6 0.0 collective-permute-done.2.refs_1_
  64.6 9.9 %all-to-all-done.1.heads_ref = bf16[16,128,128]{2,1,0:T(8,128)(2,1)S(1)} async-done(((bf16[16,128,128]{2,1,0:T(8,128)(2,1)}), bf16[16,128,128]{2,1,0:T(8,128)(2,1)S(1)}, u32[]{:S(2)}, u32[]{:S(2)}) %all-to-all-start.1) | async-done | bytes 524320 | tf_op jit(solution)/shard_map/all_to_all | solution.py:530
  74.5 0.0 collective-permute-done.3.refs_4_
  74.5 0.0 collective-permute-done.6.refs_7_
  74.5 7.5 %project.1 = (f32[128,2048]{1,0:T(8,128)}, bf16[128,2048]{1,0:T(8,128)(2,1)}, bf16[1024,1536]{1,0:T(8,128)(2,1)S(1)}) custom-call(s32[8]{0:T(128)S(1)} %fusion.columns_ref, bf16[16,128,128]{2,1,0:T(8,128)(2,1)S(1)} %all-to-all-done.1.heads_ref, bf16[2048,256]{1,0:T(8,128)(2,1)} %refs_0_.1, bf16[2048,256]{1,0:T(8,128)(2,1)} %collective-permute-done.2.refs_1_, ...), custom_call_target="tpu_custom_call" | custom-call | tf_op jit(solution)/shard_map/project/pallas_call | solution.py:316
  82.0 0.0 copy-start
  82.0 0.0 copy-start.1
  82.0 0.0 copy-start.2
  82.0 46.0 %all_to_all.21 = bf16[128,8,1536]{2,1,0:T(8,128)(2,1)S(1)} all-to-all(bf16[128,8,1536]{2,1,0:T(8,128)(2,1)S(1)} %bitcast.23), channel_id=1, replica_groups=mesh['sp'=16,'dp'=8] {'sp','dp'}, dimensions={0} | all-to-all | bytes 6291456 | tf_op jit(solution)/shard_map/all_to_all | solution.py:554
  128.1 8.0 %expert.1 = bf16[1024,1536]{1,0:T(8,128)(2,1)} custom-call(bf16[1024,1536]{1,0:T(8,128)(2,1)S(1)} %bitcast.20, bf16[2048,512]{1,0:T(8,128)(2,1)S(1)} %bitcast.24, bf16[2048,512]{1,0:T(8,128)(2,1)S(1)} %bitcast.25, bf16[512,2048]{1,0:T(8,128)(2,1)S(1)} %bitcast.26), custom_call_target="tpu_custom_call" | custom-call | tf_op jit(solution)/shard_map/expert/pallas_call | solution.py:380
  136.1 4.7 %all-to-all-start.3 = ((bf16[128,8,1536]{2,1,0:T(8,128)(2,1)}), bf16[128,8,1536]{2,1,0:T(8,128)(2,1)S(1)}, u32[]{:S(2)}, u32[]{:S(2)}) async-start(bf16[128,8,1536]{2,1,0:T(8,128)(2,1)} %bitcast.30), calls=%async_computation.3 | async-start | bytes 6291456 | tf_op jit(solution)/shard_map/all_to_all | solution.py:554
  140.8 5.3 %shared.1.base_hbm = f32[128,2048]{1,0:T(8,128)} custom-call(bf16[128,2048]{1,0:T(8,128)(2,1)} %get-tuple-element.19.normed_ref, f32[128,2048]{1,0:T(8,128)} %get-tuple-element.20.mixed_ref, bf16[2048,512]{1,0:T(8,128)(2,1)} %gate_ref.1, bf16[2048,512]{1,0:T(8,128)(2,1)} %up_ref.1, bf16[512,2048]{1,0:T(8,128)(2,1)} %down_ref.1), custom_call_target="tpu_custom_call" | custom-call | tf_op jit(solution)/shard_map/shared/pallas_call | solution.py:418
  146.1 36.3 %all-to-all-done.3 = bf16[128,8,1536]{2,1,0:T(8,128)(2,1)S(1)} async-done(((bf16[128,8,1536]{2,1,0:T(8,128)(2,1)}), bf16[128,8,1536]{2,1,0:T(8,128)(2,1)S(1)}, u32[]{:S(2)}, u32[]{:S(2)}) %all-to-all-start.3) | async-done | bytes 3145760 | tf_op jit(solution)/shard_map/all_to_all | solution.py:554
  182.4 4.3 %combine.1 = bf16[128,2048]{1,0:T(8,128)(2,1)} custom-call(bf16[1024,1536]{1,0:T(8,128)(2,1)S(1)} %bitcast.19, f32[128,768]{1,0:T(8,128)S(1)} %get-tuple-element.18.gates_ref, f32[128,2048]{1,0:T(8,128)} %shared.1.base_hbm), custom_call_target="tpu_custom_call" | custom-call | tf_op jit(solution)/shard_map/combine/pallas_call | solution.py:463
  (18 shorter events, 0.0 us)
Async XLA Ops:
  0.0 30.4 %collective-permute-start.1 = (bf16[2048,256]{1,0:T(8,128)(2,1)}, bf16[2048,256]{1,0:T(8,128)(2,1)S(1)}, u32[]{:S(2)}, u32[]{:S(2)}) collective-permute-start(bf16[2048,256]{1,0:T(8,128)(2,1)} %refs_0_.1), channel_id=1, source_target_pairs={{0,6},{1,3},{2,0},{3,5},{4,2},{5,7},{6,4},{7,1},{8,14},{9,11},{10,... | collective-permute-start | bytes 3145736 | tf_op jit(solution)/shard_map/ppermute | solution.py:485
  2.0 28.4 %collective-permute-start = (bf16[2048,256]{1,0:T(8,128)(2,1)}, bf16[2048,256]{1,0:T(8,128)(2,1)}, u32[]{:S(2)}, u32[]{:S(2)}) collective-permute-start(bf16[2048,256]{1,0:T(8,128)(2,1)} %refs_0_.1), channel_id=1, source_target_pairs={{0,2},{1,7},{2,4},{3,1},{4,6},{5,3},{6,0},{7,5},{8,10},{9,15},{10,... | collective-permute-start | bytes 3145736 | tf_op jit(solution)/shard_map/ppermute | solution.py:485
  3.3 27.2 %copy-start.4 = (bf16[2048,256]{1,0:T(8,128)(2,1)S(1)}, bf16[2048,256]{1,0:T(8,128)(2,1)}, u32[]{:S(2)}) copy-start(bf16[2048,256]{1,0:T(8,128)(2,1)} %refs_0_.1) | copy-start | bytes 3145732
  30.4 32.8 %copy-start.6 = (s32[1,128,4]{1,2,0:T(4,128)S(1)}, s32[1,128,4]{1,2,0:T(4,128)}, u32[]{:S(2)}) copy-start(s32[1,128,4]{1,2,0:T(4,128)} %param.26) | copy-start | bytes 6148
  30.4 33.0 %copy-start.7 = (f32[1,128,4]{1,2,0:T(4,128)S(1)}, f32[1,128,4]{1,2,0:T(4,128)}, u32[]{:S(2)}) copy-start(f32[1,128,4]{1,2,0:T(4,128)} %param.27) | copy-start | bytes 6148
  30.4 34.2 %copy-start.8 = (s32[8]{0:T(128)S(1)}, s32[8]{0:T(128)}, u32[]{:S(2)}) copy-start(s32[8]{0:T(128)} %constant.65.clone) | copy-start | bytes 100
  30.4 34.2 %copy-start.9 = (s32[8]{0:T(128)S(1)}, s32[8]{0:T(128)}, u32[]{:S(2)}) copy-start(s32[8]{0:T(128)} %constant.64.clone) | copy-start | bytes 100
  30.4 44.1 %copy-start.3 = (f32[2048]{0:T(1024)S(1)}, f32[2048]{0:T(1024)}, u32[]{:S(2)}) copy-start(f32[2048]{0:T(1024)} %param.23) | copy-start | bytes 24580
  30.4 44.1 %copy-start.5 = (bf16[2048,256]{1,0:T(8,128)(2,1)}, bf16[2048,256]{1,0:T(8,128)(2,1)S(1)}, u32[]{:S(2)}) copy-start(bf16[2048,256]{1,0:T(8,128)(2,1)S(1)} %collective-permute-done.1.refs_3_) | copy-start | bytes 3145732
  30.5 14.3 %collective-permute-start.5 = (bf16[2048,256]{1,0:T(8,128)(2,1)}, bf16[2048,256]{1,0:T(8,128)(2,1)}, u32[]{:S(2)}, u32[]{:S(2)}) collective-permute-start(bf16[2048,256]{1,0:T(8,128)(2,1)} %collective-permute-done.refs_2_), channel_id=1, source_target_pairs={{0,2},{1,7},{2,4},{3,1},{4,6},{5,3},{6,0},{7,5},{8,10},{9,15},{10,... | collective-permute-start | bytes 3145736 | tf_op jit(solution)/shard_map/ppermute | solution.py:485
  30.6 34.1 %collective-permute-start.2 = (bf16[2048,256]{1,0:T(8,128)(2,1)S(1)}, bf16[2048,256]{1,0:T(8,128)(2,1)}, u32[]{:S(2)}, u32[]{:S(2)}) collective-permute-start(bf16[2048,256]{1,0:T(8,128)(2,1)S(1)} %copy-done.4), channel_id=1, source_target_pairs={{0,1},{1,0},{2,3},{3,2},{4,5},{5,4},{6,7},{7,6},{8,9},{9,8},{10,11... | collective-permute-start | bytes 3145736 | tf_op jit(solution)/shard_map/ppermute | solution.py:485
  32.7 41.8 %collective-permute-start.3 = (bf16[2048,256]{1,0:T(8,128)(2,1)}, bf16[2048,256]{1,0:T(8,128)(2,1)}, u32[]{:S(2)}, u32[]{:S(2)}) collective-permute-start(bf16[2048,256]{1,0:T(8,128)(2,1)} %collective-permute-done.refs_2_), channel_id=1, source_target_pairs={{0,1},{1,0},{2,3},{3,2},{4,5},{5,4},{6,7},{7,6},{8,9},{9,8},{10,11... | collective-permute-start | bytes 3145736 | tf_op jit(solution)/shard_map/ppermute | solution.py:485
  32.7 41.8 %collective-permute-start.4 = (bf16[2048,256]{1,0:T(8,128)(2,1)S(1)}, bf16[2048,256]{1,0:T(8,128)(2,1)}, u32[]{:S(2)}, u32[]{:S(2)}) collective-permute-start(bf16[2048,256]{1,0:T(8,128)(2,1)S(1)} %collective-permute-done.1.refs_3_), channel_id=1, source_target_pairs={{0,1},{1,0},{2,3},{3,2},{4,5},{5,4},{6,7},{7,6},{8,9},{9,8},{10,11... | collective-permute-start | bytes 3145736 | tf_op jit(solution)/shard_map/ppermute | solution.py:485
  44.8 29.7 %collective-permute-start.6 = (bf16[2048,256]{1,0:T(8,128)(2,1)}, bf16[2048,256]{1,0:T(8,128)(2,1)}, u32[]{:S(2)}, u32[]{:S(2)}) collective-permute-start(bf16[2048,256]{1,0:T(8,128)(2,1)} %collective-permute-done.5.refs_6_), channel_id=1, source_target_pairs={{0,1},{1,0},{2,3},{3,2},{4,5},{5,4},{6,7},{7,6},{8,9},{9,8},{10,11... | collective-permute-start | bytes 3145736 | tf_op jit(solution)/shard_map/ppermute | solution.py:485
  59.6 14.9 %all-to-all-start.1 = ((bf16[16,128,128]{2,1,0:T(8,128)(2,1)}), bf16[16,128,128]{2,1,0:T(8,128)(2,1)S(1)}, u32[]{:S(2)}, u32[]{:S(2)}) async-start(bf16[16,128,128]{2,1,0:T(8,128)(2,1)} %bitcast.31), calls=%async_computation.1 | async-start | bytes 1048576 | tf_op jit(solution)/shard_map/all_to_all | solution.py:530
  82.0 46.1 %copy-start = (bf16[1,2048,512]{2,1,0:T(8,128)(2,1)S(1)}, bf16[1,2048,512]{2,1,0:T(8,128)(2,1)}, u32[]{:S(2)}) copy-start(bf16[1,2048,512]{2,1,0:T(8,128)(2,1)} %param.31) | copy-start | bytes 6291460
  82.0 46.1 %copy-start.1 = (bf16[1,2048,512]{2,1,0:T(8,128)(2,1)S(1)}, bf16[1,2048,512]{2,1,0:T(8,128)(2,1)}, u32[]{:S(2)}) copy-start(bf16[1,2048,512]{2,1,0:T(8,128)(2,1)} %param.32) | copy-start | bytes 6291460
  82.0 46.0 %copy-start.2 = (bf16[1,512,2048]{2,1,0:T(8,128)(2,1)S(1)}, bf16[1,512,2048]{2,1,0:T(8,128)(2,1)}, u32[]{:S(2)}) copy-start(bf16[1,512,2048]{2,1,0:T(8,128)(2,1)} %param.33) | copy-start | bytes 6291460
  136.1 46.3 %all-to-all-start.3 = ((bf16[128,8,1536]{2,1,0:T(8,128)(2,1)}), bf16[128,8,1536]{2,1,0:T(8,128)(2,1)S(1)}, u32[]{:S(2)}, u32[]{:S(2)}) async-start(bf16[128,8,1536]{2,1,0:T(8,128)(2,1)} %bitcast.30), calls=%async_computation.3 | async-start | bytes 6291456 | tf_op jit(solution)/shard_map/all_to_all | solution.py:554

commit v4 on v3

--- a/solution.py
+++ b/solution.py
@@ -196,7 +196,7 @@
         out_specs=pl.BlockSpec((block, 128), lambda i: (i, 0)),
         out_shape=pltpu.HBM((length, 128), BF16),
         scratch_shapes=[pltpu.VMEM((length, 128), BF16), pltpu.VMEM((length, 256), BF16)],
-        compiler_params=limit(32),
+        compiler_params=limit(24),
         name="attend",
     )(rows, rows)
 
@@ -266,22 +266,24 @@
 
 
 def project_kernel(columns_ref, heads_ref, *refs):
-    pieces = refs[:8]
+    placed, pieces = refs[:2], refs[2:8]
     residual_hbm, gain_ref, place_ref, mixed_hbm, normed_hbm, wire_ref = refs[8:14]
     weight_ref, residual_ref, part_ref, mixed_ref, normed_ref, sems = refs[14:]
     copies = [
-        pltpu.make_async_copy(pieces[s], weight_ref.at[s], sems.at[s]) for s in range(8)
+        pltpu.make_async_copy(pieces[s], weight_ref.at[s], sems.at[s]) for s in range(6)
     ]
-    copies.append(pltpu.make_async_copy(residual_hbm, residual_ref, sems.at[8]))
-    copies.append(pltpu.make_async_copy(mixed_ref, mixed_hbm, sems.at[9]))
-    copies.append(pltpu.make_async_copy(normed_ref, normed_hbm, sems.at[10]))
-    for copy in copies[:9]:
+    copies.append(pltpu.make_async_copy(residual_hbm, residual_ref, sems.at[6]))
+    copies.append(pltpu.make_async_copy(mixed_ref, mixed_hbm, sems.at[7]))
+    copies.append(pltpu.make_async_copy(normed_ref, normed_hbm, sems.at[8]))
+    for copy in copies[:7]:
         copy.start()
     rows = jnp.concatenate([heads_ref[h] for h in range(heads_ref.shape[0])], axis=1)
     for s in range(8):
-        copies[s].wait()
-        part_ref[columns_ref[s]] = jnp.dot(rows, weight_ref[s], preferred_element_type=F32)
-    copies[8].wait()
+        if s >= 2:
+            copies[s - 2].wait()
+        weight = weight_ref[s - 2] if s >= 2 else placed[s][...]
+        part_ref[columns_ref[s]] = jnp.dot(rows, weight, preferred_element_type=F32)
+    copies[6].wait()
     width = part_ref.shape[2]
     square = None
     for j in range(8):
@@ -292,8 +294,8 @@
     scale = lax.rsqrt(square * (1.0 / (8 * width)) + EPS)
     normed = (mixed_ref[...] * scale * gain_ref[...]).astype(BF16)
     normed_ref[...] = normed
-    copies[9].start()
-    copies[10].start()
+    copies[7].start()
+    copies[8].start()
     span = place_ref.shape[0] // PAIRS
     part = normed.shape[1] // QUARTERS
     for c in range(PAIRS):
@@ -305,8 +307,8 @@
             wire_ref[g * 128 : (g + 1) * 128, c * part : (c + 1) * part] = block
 
         fold(slots, write)
-    copies[9].wait()
-    copies[10].wait()
+    copies[7].wait()
+    copies[8].wait()
 
 
 def project(columns, heads, pieces, residual, gain, place):
@@ -315,8 +317,9 @@
     vmem = pl.BlockSpec(memory_space=pltpu.VMEM)
     return pl.pallas_call(
         project_kernel,
-        in_specs=[pl.BlockSpec(memory_space=pltpu.SMEM), vmem]
-        + [pl.BlockSpec(memory_space=pl.ANY)] * 9
+        in_specs=[pl.BlockSpec(memory_space=pltpu.SMEM)]
+        + [vmem] * 3
+        + [pl.BlockSpec(memory_space=pl.ANY)] * 7
         + [vmem] * 2,
         out_specs=[pl.BlockSpec(memory_space=pl.ANY)] * 2 + [vmem],
         out_shape=(
@@ -325,19 +328,20 @@
             pltpu.VMEM((peers * 8, width * CAP // 8), BF16),
         ),
         scratch_shapes=[
-            pltpu.VMEM((8,) + pieces[0].shape, BF16),
+            pltpu.VMEM((6,) + pieces[0].shape, BF16),
             pltpu.VMEM(residual.shape, BF16),
             pltpu.VMEM((8, tokens, width // 8), F32),
             pltpu.VMEM((tokens, width), F32),
             pltpu.VMEM((tokens, width), BF16),
-            pltpu.SemaphoreType.DMA((11,)),
+            pltpu.SemaphoreType.DMA((9,)),
         ],
-        compiler_params=limit(32),
+        compiler_params=limit(24),
         name="project",
     )(
         columns,
         local(heads),
-        *(distant(piece) for piece in pieces),
+        *(local(piece) for piece in pieces[:2]),
+        *(distant(piece) for piece in pieces[2:]),
         distant(residual),
         gain,
         local(place),
@@ -432,29 +436,36 @@
     )(*(distant(array) for array in (normed, mixed, gate, up, down)))
 
 
-def combine_kernel(wire_ref, gates_ref, base_hbm, out_ref, rows_ref, base_ref, sem):
-    copy = pltpu.make_async_copy(base_hbm, base_ref, sem)
-    copy.start()
+def combine_kernel(wire_ref, gates_ref, base_hbm, out_hbm, rows_ref, base_ref, out_ref, sems):
+    blocks = sems.shape[0] - 1
+    block = base_ref.shape[1] // blocks
+    fetch = pltpu.make_async_copy(base_hbm, base_ref, sems.at[blocks])
+    fetch.start()
     gates = gates_ref[...]
     tokens = gates.shape[0]
     high = gates.astype(BF16)
-    rest = gates - high.astype(F32)
-    middle = rest.astype(BF16)
-    low = (rest - middle.astype(F32)).astype(BF16)
-    stacked = jnp.concatenate([high, middle, low], axis=0)
+    low = (gates - high.astype(F32)).astype(BF16)
+    stacked = jnp.concatenate([high, low], axis=0)
     part = wire_ref.shape[1] // PAIRS
     span = rows_ref.shape[0] // PAIRS
     for c in range(PAIRS):
         unfold(
             wire_ref.at[:, pl.ds(c * part, part)], rows_ref.at[pl.ds(c * span, span)]
         )
-    copy.wait()
-    block = 512
-    for n in range(base_ref.shape[1] // block):
+    fetch.wait()
+    copies = []
+    for n in range(blocks):
         lanes = slice(n * block, (n + 1) * block)
         parts = jnp.dot(stacked, rows_ref[:, lanes], preferred_element_type=F32)
-        routed = parts[:tokens] + (parts[tokens : 2 * tokens] + parts[2 * tokens :])
+        routed = parts[:tokens] + parts[tokens:]
         out_ref[:, lanes] = (base_ref[:, lanes] + routed).astype(BF16)
+        lanes = pl.ds(n * block, block)
+        copies.append(
+            pltpu.make_async_copy(out_ref.at[:, lanes], out_hbm.at[:, lanes], sems.at[n])
+        )
+        copies[n].start()
+    for copy in copies:
+        copy.wait()
 
 
 def combine(wire, gates, base):
@@ -463,12 +474,13 @@
     return pl.pallas_call(
         combine_kernel,
         in_specs=[vmem, vmem, pl.BlockSpec(memory_space=pl.ANY)],
-        out_specs=vmem,
-        out_shape=jax.ShapeDtypeStruct(base.shape, BF16),
+        out_specs=pl.BlockSpec(memory_space=pl.ANY),
+        out_shape=pltpu.HBM(base.shape, BF16),
         scratch_shapes=[
             pltpu.VMEM((rows * CAP // 8, width * 8 // CAP), BF16),
             pltpu.VMEM(base.shape, F32),
-            pltpu.SemaphoreType.DMA,
+            pltpu.VMEM(base.shape, BF16),
+            pltpu.SemaphoreType.DMA((5,)),
         ],
         compiler_params=limit(24),
         name="combine",
@@ -541,10 +553,10 @@
     me = lax.axis_index("dp")
     x, core = me // 2, me % 2
     away = 1 - 2 * core
-    steps = jnp.array([0, 0, -1, 1, 1, -1, 2, 2], jnp.int32) * away
-    flips = jnp.array([0, 1, 0, 0, 1, 1, 0, 1], jnp.int32)
+    steps = jnp.array([0, 1, -1, 0, 1, -1, 2, 2], jnp.int32) * away
+    flips = jnp.array([0, 0, 0, 1, 1, 1, 0, 1], jnp.int32)
     columns = 2 * ((x + steps) % ring) + (core + flips) % 2
-    pieces = [out_weight, own_pair, near, other, near_pair, other_pair, far, far_pair]
+    pieces = [out_weight, other, near, own_pair, near_pair, other_pair, far, far_pair]
     mixed, normed, wire = project(
         columns, heads, pieces, residual[0], norm_gain.reshape(1, -1), place
     )

time: 187 us -> 185 us (0.989)
  Pallas kernels: 40.2 us -> 37.9 us
where the time goes in v4:
time: 185 us; the launch traced here: 184 us
  blocking collectives  69.8 us (38%)
  waiting for transfers between devices  57.8 us (31%)
  Pallas kernels  37.9 us (20%)
  starting transfers between devices  18.2 us (10%)
    all_to_all x1, blocking collectives, exchange(): lax.all_to_all(values.reshape(wire_shape), ('sp', 'dp'), split_axis=0, co...  45.9 us
    all_to_all x1, waiting for transfers between devices, exchange(): lax.all_to_all(values.reshape(wire_shape), ('sp', 'dp'), split_axis=0, co...  36.3 us
    all_to_all x1, blocking collectives, per_device(): lax.all_to_all(outgoing, 'sp', split_axis=0, concat_axis=0, tiled=True)  24 us
    ppermute x7, waiting for transfers between devices, shift(): return lax.ppermute(values, 'dp', [(d, place(d)) for d in range(size)])  11.6 us
    pallas_call x1, Pallas kernels, attend(): pl.pallas_call(attend_kernel, grid=(length // block,), in_specs=[pl.Block...  10.9 us
    ppermute x7, starting transfers between devices, shift(): return lax.ppermute(values, 'dp', [(d, place(d)) for d in range(size)])  9.99 us
    all_to_all x1, waiting for transfers between devices, per_device(): lax.all_to_all(attention.reshape(-1, tokens, attention.shape[1]), 'sp', s...  9.87 us
    pallas_call x1, Pallas kernels, expert(): pl.pallas_call(expert_kernel, in_specs=[vmem] * 4, out_specs=pl.BlockSpec...  8.04 us
  transfers between devices with their start and end apart: 9, of which 3 were waited for; matrix products, arithmetic and copies ran while one was open for 0% of the time, Pallas kernels for 11%

profile of v4, /device:TPU:1, one launch (start us, length us, event | category | flops | bytes accessed | tf_op | source)
XLA Modules:
  0.0 184.5 jit_solution(9249294596115429847)
XLA Ops:
  0.0 2.0 %collective-permute-start.1 = (bf16[2048,256]{1,0:T(8,128)(2,1)}, bf16[2048,256]{1,0:T(8,128)(2,1)S(1)}, u32[]{:S(2)}, u32[]{:S(2)}) collective-permute-start(bf16[2048,256]{1,0:T(8,128)(2,1)} %refs_0_.1), channel_id=1, source_target_pairs={{0,6},{1,3},{2,0},{3,5},{4,2},{5,7},{6,4},{7,1},{8,14},{9,11},{10,... | collective-permute-start | bytes 3145736 | tf_op jit(solution)/shard_map/ppermute | solution.py:497
  2.0 1.3 collective-permute-start
  3.3 3.1 %prepare.1 = bf16[16,128,256]{2,1,0:T(8,128)(2,1)S(1)} custom-call(s32[1]{0:T(128)} %bitcast.block_ref, bf16[128,16,128]{2,1,0:T(8,128)(2,1)} %bitcast.32, bf16[128,16,128]{2,1,0:T(8,128)(2,1)} %bitcast.33, f32[2,128,128]{2,1,0:T(8,128)} %constant.62.clone.col_ref, f32[16,2,2,128]{3,2,1,0:T(2,128)} %constant.63.clone.row_ref, f32[1,64]{1,0:T(1,128)} %bitcast.35, ...), custom_call_target="tpu_custom_call" | custom-call | tf_op jit(solution)/shard_map/prepare/pallas_call | solution.py:122
  6.4 24.0 %all_to_all.20 = bf16[16,128,256]{2,1,0:T(8,128)(2,1)S(1)} all-to-all(bf16[16,128,256]{2,1,0:T(8,128)(2,1)S(1)} %prepare.1), channel_id=1, replica_groups=mesh['sp'=16,'dp'=8] {'sp'}, dimensions={0} | all-to-all | bytes 2097152 | tf_op jit(solution)/shard_map/all_to_all | solution.py:537
  30.4 0.0 copy-start.4
  30.4 0.0 collective-permute-done.1.refs_1_
  30.4 0.1 collective-permute-start.5
  30.5 2.2 %collective-permute-start.2 = (bf16[2048,256]{1,0:T(8,128)(2,1)S(1)}, bf16[2048,256]{1,0:T(8,128)(2,1)}, u32[]{:S(2)}, u32[]{:S(2)}) collective-permute-start(bf16[2048,256]{1,0:T(8,128)(2,1)S(1)} %copy-done.3), channel_id=1, source_target_pairs={{0,1},{1,0},{2,3},{3,2},{4,5},{5,4},{6,7},{7,6},{8,9},{9,8},{10,11... | collective-permute-start | bytes 3145736 | tf_op jit(solution)/shard_map/ppermute | solution.py:497
  32.7 0.0 collective-permute-start.3
  32.7 0.5 collective-permute-start.4
  33.2 11.6 %collective-permute-done.5.refs_6_ = bf16[2048,256]{1,0:T(8,128)(2,1)} collective-permute-done((bf16[2048,256]{1,0:T(8,128)(2,1)}, bf16[2048,256]{1,0:T(8,128)(2,1)}, u32[]{:S(2)}, u32[]{:S(2)}) %collective-permute-start.5) | collective-permute-done | bytes 1048608 | tf_op jit(solution)/shard_map/ppermute | solution.py:497
  44.8 4.0 %collective-permute-start.6 = (bf16[2048,256]{1,0:T(8,128)(2,1)}, bf16[2048,256]{1,0:T(8,128)(2,1)}, u32[]{:S(2)}, u32[]{:S(2)}) collective-permute-start(bf16[2048,256]{1,0:T(8,128)(2,1)} %collective-permute-done.5.refs_6_), channel_id=1, source_target_pairs={{0,1},{1,0},{2,3},{3,2},{4,5},{5,4},{6,7},{7,6},{8,9},{9,8},{10,11... | collective-permute-start | bytes 3145736 | tf_op jit(solution)/shard_map/ppermute | solution.py:497
  48.7 10.9 %attend.1 = bf16[2048,128]{1,0:T(8,128)(2,1)} custom-call(bf16[2048,256]{1,0:T(8,128)(2,1)S(1)} %bitcast.21, bf16[2048,256]{1,0:T(8,128)(2,1)S(1)} %bitcast.22), custom_call_target="tpu_custom_call" | custom-call | tf_op jit(solution)/shard_map/attend/pallas_call | solution.py:189
  59.6 3.6 %all-to-all-start.1 = ((bf16[16,128,128]{2,1,0:T(8,128)(2,1)}), bf16[16,128,128]{2,1,0:T(8,128)(2,1)S(1)}, u32[]{:S(2)}, u32[]{:S(2)}) async-start(bf16[16,128,128]{2,1,0:T(8,128)(2,1)} %bitcast.31), calls=%async_computation.1 | async-start | bytes 1048576 | tf_op jit(solution)/shard_map/all_to_all | solution.py:542
  63.2 0.1 copy.20
  63.4 0.1 copy.21
  63.5 1.1 route.1
  64.6 0.0 collective-permute-done.2.refs_3_
  64.6 9.9 %all-to-all-done.1.heads_ref = bf16[16,128,128]{2,1,0:T(8,128)(2,1)S(1)} async-done(((bf16[16,128,128]{2,1,0:T(8,128)(2,1)}), bf16[16,128,128]{2,1,0:T(8,128)(2,1)S(1)}, u32[]{:S(2)}, u32[]{:S(2)}) %all-to-all-start.1) | async-done | bytes 524320 | tf_op jit(solution)/shard_map/all_to_all | solution.py:542
  74.5 0.0 collective-permute-done.4.refs_5_
  74.5 0.0 collective-permute-done.3.refs_4_
  74.5 0.0 collective-permute-done.6.refs_7_
  74.5 6.6 %project.1 = (f32[128,2048]{1,0:T(8,128)}, bf16[128,2048]{1,0:T(8,128)(2,1)}, bf16[1024,1536]{1,0:T(8,128)(2,1)S(1)}) custom-call(s32[8]{0:T(128)S(1)} %fusion.columns_ref, bf16[16,128,128]{2,1,0:T(8,128)(2,1)S(1)} %all-to-all-done.1.heads_ref, bf16[2048,256]{1,0:T(8,128)(2,1)S(1)} %copy-done.3, bf16[2048,256]{1,0:T(8,128)(2,1)S(1)} %collective-permute-done.1.refs_1_, ...), custom_call_target="tpu_custom_call" | custom-call | tf_op jit(solution)/shard_map/project/pallas_call | solution.py:318
  81.1 0.0 copy-start
  81.1 0.0 copy-start.1
  81.2 0.0 copy-start.2
  81.2 45.9 %all_to_all.21 = bf16[128,8,1536]{2,1,0:T(8,128)(2,1)S(1)} all-to-all(bf16[128,8,1536]{2,1,0:T(8,128)(2,1)S(1)} %bitcast.23), channel_id=1, replica_groups=mesh['sp'=16,'dp'=8] {'sp','dp'}, dimensions={0} | all-to-all | bytes 6291456 | tf_op jit(solution)/shard_map/all_to_all | solution.py:566
  127.0 8.0 %expert.1 = bf16[1024,1536]{1,0:T(8,128)(2,1)} custom-call(bf16[1024,1536]{1,0:T(8,128)(2,1)S(1)} %bitcast.20, bf16[2048,512]{1,0:T(8,128)(2,1)S(1)} %bitcast.24, bf16[2048,512]{1,0:T(8,128)(2,1)S(1)} %bitcast.25, bf16[512,2048]{1,0:T(8,128)(2,1)S(1)} %bitcast.26), custom_call_target="tpu_custom_call" | custom-call | tf_op jit(solution)/shard_map/expert/pallas_call | solution.py:384
  135.1 4.7 %all-to-all-start.3 = ((bf16[128,8,1536]{2,1,0:T(8,128)(2,1)}), bf16[128,8,1536]{2,1,0:T(8,128)(2,1)S(1)}, u32[]{:S(2)}, u32[]{:S(2)}) async-start(bf16[128,8,1536]{2,1,0:T(8,128)(2,1)} %bitcast.30), calls=%async_computation.3 | async-start | bytes 6291456 | tf_op jit(solution)/shard_map/all_to_all | solution.py:566
  139.8 5.3 %shared.1.base_hbm = f32[128,2048]{1,0:T(8,128)} custom-call(bf16[128,2048]{1,0:T(8,128)(2,1)} %get-tuple-element.19.normed_ref, f32[128,2048]{1,0:T(8,128)} %get-tuple-element.20.mixed_ref, bf16[2048,512]{1,0:T(8,128)(2,1)} %gate_ref.1, bf16[2048,512]{1,0:T(8,128)(2,1)} %up_ref.1, bf16[512,2048]{1,0:T(8,128)(2,1)} %down_ref.1), custom_call_target="tpu_custom_call" | custom-call | tf_op jit(solution)/shard_map/shared/pallas_call | solution.py:422
  145.0 36.3 %all-to-all-done.3 = bf16[128,8,1536]{2,1,0:T(8,128)(2,1)S(1)} async-done(((bf16[128,8,1536]{2,1,0:T(8,128)(2,1)}), bf16[128,8,1536]{2,1,0:T(8,128)(2,1)S(1)}, u32[]{:S(2)}, u32[]{:S(2)}) %all-to-all-start.3) | async-done | bytes 3145760 | tf_op jit(solution)/shard_map/all_to_all | solution.py:566
  181.4 2.9 %combine.1 = bf16[128,2048]{1,0:T(8,128)(2,1)} custom-call(bf16[1024,1536]{1,0:T(8,128)(2,1)S(1)} %bitcast.19, f32[128,768]{1,0:T(8,128)S(1)} %get-tuple-element.18.gates_ref, f32[128,2048]{1,0:T(8,128)} %shared.1.base_hbm), custom_call_target="tpu_custom_call" | custom-call | tf_op jit(solution)/shard_map/combine/pallas_call | solution.py:474
  (16 shorter events, 0.0 us)
Async XLA Ops:
  0.0 30.4 %collective-permute-start.1 = (bf16[2048,256]{1,0:T(8,128)(2,1)}, bf16[2048,256]{1,0:T(8,128)(2,1)S(1)}, u32[]{:S(2)}, u32[]{:S(2)}) collective-permute-start(bf16[2048,256]{1,0:T(8,128)(2,1)} %refs_0_.1), channel_id=1, source_target_pairs={{0,6},{1,3},{2,0},{3,5},{4,2},{5,7},{6,4},{7,1},{8,14},{9,11},{10,... | collective-permute-start | bytes 3145736 | tf_op jit(solution)/shard_map/ppermute | solution.py:497
  2.0 28.4 %collective-permute-start = (bf16[2048,256]{1,0:T(8,128)(2,1)}, bf16[2048,256]{1,0:T(8,128)(2,1)}, u32[]{:S(2)}, u32[]{:S(2)}) collective-permute-start(bf16[2048,256]{1,0:T(8,128)(2,1)} %refs_0_.1), channel_id=1, source_target_pairs={{0,2},{1,7},{2,4},{3,1},{4,6},{5,3},{6,0},{7,5},{8,10},{9,15},{10,... | collective-permute-start | bytes 3145736 | tf_op jit(solution)/shard_map/ppermute | solution.py:497
  3.3 27.2 %copy-start.3 = (bf16[2048,256]{1,0:T(8,128)(2,1)S(1)}, bf16[2048,256]{1,0:T(8,128)(2,1)}, u32[]{:S(2)}) copy-start(bf16[2048,256]{1,0:T(8,128)(2,1)} %refs_0_.1) | copy-start | bytes 3145732
  30.4 32.8 %copy-start.5 = (s32[1,128,4]{1,2,0:T(4,128)S(1)}, s32[1,128,4]{1,2,0:T(4,128)}, u32[]{:S(2)}) copy-start(s32[1,128,4]{1,2,0:T(4,128)} %param.26) | copy-start | bytes 6148
  30.4 33.0 %copy-start.6 = (f32[1,128,4]{1,2,0:T(4,128)S(1)}, f32[1,128,4]{1,2,0:T(4,128)}, u32[]{:S(2)}) copy-start(f32[1,128,4]{1,2,0:T(4,128)} %param.27) | copy-start | bytes 6148
  30.4 34.1 %copy-start.7 = (s32[8]{0:T(128)S(1)}, s32[8]{0:T(128)}, u32[]{:S(2)}) copy-start(s32[8]{0:T(128)} %constant.65.clone) | copy-start | bytes 100
  30.4 34.2 %copy-start.8 = (s32[8]{0:T(128)S(1)}, s32[8]{0:T(128)}, u32[]{:S(2)}) copy-start(s32[8]{0:T(128)} %constant.64.clone) | copy-start | bytes 100
  30.4 44.1 %copy-start.4 = (f32[2048]{0:T(1024)S(1)}, f32[2048]{0:T(1024)}, u32[]{:S(2)}) copy-start(f32[2048]{0:T(1024)} %param.23) | copy-start | bytes 24580
  30.4 14.3 %collective-permute-start.5 = (bf16[2048,256]{1,0:T(8,128)(2,1)}, bf16[2048,256]{1,0:T(8,128)(2,1)}, u32[]{:S(2)}, u32[]{:S(2)}) collective-permute-start(bf16[2048,256]{1,0:T(8,128)(2,1)} %collective-permute-done.refs_2_), channel_id=1, source_target_pairs={{0,2},{1,7},{2,4},{3,1},{4,6},{5,3},{6,0},{7,5},{8,10},{9,15},{10,... | collective-permute-start | bytes 3145736 | tf_op jit(solution)/shard_map/ppermute | solution.py:497
  30.5 34.1 %collective-permute-start.2 = (bf16[2048,256]{1,0:T(8,128)(2,1)S(1)}, bf16[2048,256]{1,0:T(8,128)(2,1)}, u32[]{:S(2)}, u32[]{:S(2)}) collective-permute-start(bf16[2048,256]{1,0:T(8,128)(2,1)S(1)} %copy-done.3), channel_id=1, source_target_pairs={{0,1},{1,0},{2,3},{3,2},{4,5},{5,4},{6,7},{7,6},{8,9},{9,8},{10,11... | collective-permute-start | bytes 3145736 | tf_op jit(solution)/shard_map/ppermute | solution.py:497
  32.7 41.8 %collective-permute-start.3 = (bf16[2048,256]{1,0:T(8,128)(2,1)}, bf16[2048,256]{1,0:T(8,128)(2,1)}, u32[]{:S(2)}, u32[]{:S(2)}) collective-permute-start(bf16[2048,256]{1,0:T(8,128)(2,1)} %collective-permute-done.refs_2_), channel_id=1, source_target_pairs={{0,1},{1,0},{2,3},{3,2},{4,5},{5,4},{6,7},{7,6},{8,9},{9,8},{10,11... | collective-permute-start | bytes 3145736 | tf_op jit(solution)/shard_map/ppermute | solution.py:497
  32.7 41.8 %collective-permute-start.4 = (bf16[2048,256]{1,0:T(8,128)(2,1)S(1)}, bf16[2048,256]{1,0:T(8,128)(2,1)}, u32[]{:S(2)}, u32[]{:S(2)}) collective-permute-start(bf16[2048,256]{1,0:T(8,128)(2,1)S(1)} %collective-permute-done.1.refs_1_), channel_id=1, source_target_pairs={{0,1},{1,0},{2,3},{3,2},{4,5},{5,4},{6,7},{7,6},{8,9},{9,8},{10,11... | collective-permute-start | bytes 3145736 | tf_op jit(solution)/shard_map/ppermute | solution.py:497
  44.8 29.7 %collective-permute-start.6 = (bf16[2048,256]{1,0:T(8,128)(2,1)}, bf16[2048,256]{1,0:T(8,128)(2,1)}, u32[]{:S(2)}, u32[]{:S(2)}) collective-permute-start(bf16[2048,256]{1,0:T(8,128)(2,1)} %collective-permute-done.5.refs_6_), channel_id=1, source_target_pairs={{0,1},{1,0},{2,3},{3,2},{4,5},{5,4},{6,7},{7,6},{8,9},{9,8},{10,11... | collective-permute-start | bytes 3145736 | tf_op jit(solution)/shard_map/ppermute | solution.py:497
  59.6 14.8 %all-to-all-start.1 = ((bf16[16,128,128]{2,1,0:T(8,128)(2,1)}), bf16[16,128,128]{2,1,0:T(8,128)(2,1)S(1)}, u32[]{:S(2)}, u32[]{:S(2)}) async-start(bf16[16,128,128]{2,1,0:T(8,128)(2,1)} %bitcast.31), calls=%async_computation.1 | async-start | bytes 1048576 | tf_op jit(solution)/shard_map/all_to_all | solution.py:542
  81.1 45.9 %copy-start = (bf16[1,2048,512]{2,1,0:T(8,128)(2,1)S(1)}, bf16[1,2048,512]{2,1,0:T(8,128)(2,1)}, u32[]{:S(2)}) copy-start(bf16[1,2048,512]{2,1,0:T(8,128)(2,1)} %param.31) | copy-start | bytes 6291460
  81.1 45.9 %copy-start.1 = (bf16[1,2048,512]{2,1,0:T(8,128)(2,1)S(1)}, bf16[1,2048,512]{2,1,0:T(8,128)(2,1)}, u32[]{:S(2)}) copy-start(bf16[1,2048,512]{2,1,0:T(8,128)(2,1)} %param.32) | copy-start | bytes 6291460
  81.2 45.9 %copy-start.2 = (bf16[1,512,2048]{2,1,0:T(8,128)(2,1)S(1)}, bf16[1,512,2048]{2,1,0:T(8,128)(2,1)}, u32[]{:S(2)}) copy-start(bf16[1,512,2048]{2,1,0:T(8,128)(2,1)} %param.33) | copy-start | bytes 6291460
  135.1 46.3 %all-to-all-start.3 = ((bf16[128,8,1536]{2,1,0:T(8,128)(2,1)}), bf16[128,8,1536]{2,1,0:T(8,128)(2,1)S(1)}, u32[]{:S(2)}, u32[]{:S(2)}) async-start(bf16[128,8,1536]{2,1,0:T(8,128)(2,1)} %bitcast.30), calls=%async_computation.3 | async-start | bytes 6291456 | tf_op jit(solution)/shard_map/all_to_all | solution.py:566

commit v5 on v4

--- a/solution.py
+++ b/solution.py
@@ -14,7 +14,6 @@
 ROUTED_SCALE = 2.5
 CAP = 6
 PAIRS = CAP // 2
-QUARTERS = 4
 F32 = jnp.float32
 BF16 = jnp.bfloat16
 
@@ -216,7 +215,7 @@
     gated = jnp.zeros((tokens, experts * CAP), F32)
     for k in range(top):
         rank = jnp.sum(hits[k] * before, axis=-1, keepdims=True).astype(jnp.int32)
-        slot = (rank // 2) * (2 * experts) + ids_ref[:, k : k + 1] * 2 + rank % 2
+        slot = rank * experts + ids_ref[:, k : k + 1]
         here = slots == slot
         place = jnp.where(here, 1.0, place)
         gated = jnp.where(here, gate[:, k : k + 1], gated)
@@ -237,32 +236,52 @@
     )(ids, weights)
 
 
-def wire_permutation(transposed):
-    wire = iota((128, 128), 1 if transposed else 0)
-    flat = iota((128, 128), 0 if transposed else 1)
-    source = (wire // 2 % QUARTERS) * 32 + (wire // 8) * 2 + wire % 2
-    return (flat == source).astype(F32).astype(BF16)
-
-
-def fold(rows, write):
-    permute = wire_permutation(False)
-    part = rows.shape[1] // QUARTERS
-    for g in range(rows.shape[0] // 32):
-        stacked = jnp.concatenate(
-            [rows[g * 32 : (g + 1) * 32, q * part : (q + 1) * part] for q in range(QUARTERS)], axis=0
+CHUNKS = 8
+
+
+def fold(rows, wire_ref, slot):
+    peers, width = rows.shape
+    for half in range(width // (CHUNKS * 128)):
+        first = half * CHUNKS * 128
+        chunks = jnp.stack(
+            [rows[:, first + n * 128 : first + (n + 1) * 128] for n in range(CHUNKS)]
         )
-        write(g, jnp.dot(permute, stacked, preferred_element_type=F32).astype(BF16))
+        block = jnp.swapaxes(chunks, 0, 1).reshape(peers * CHUNKS, 128)
+        lane = (slot * (width // (CHUNKS * 128)) + half) * 128
+        wire_ref[:, lane : lane + 128] = block.astype(BF16)
 
 
 def unfold(wire_ref, rows_ref):
-    permute = wire_permutation(True)
-    part = wire_ref.shape[1]
-    for g in range(wire_ref.shape[0] // 128):
+    group = 128 // CHUNKS
+    peers = wire_ref.shape[0] // CHUNKS
+    halves = rows_ref.shape[1] // (CHUNKS * 128)
+    sent, kept = iota((128, 128), 1), iota((128, 128), 0)
+    permute = (sent == kept % group * CHUNKS + kept // group).astype(F32).astype(BF16)
+    for g in range(peers // group):
         block = jnp.dot(
             permute, wire_ref[g * 128 : (g + 1) * 128, :], preferred_element_type=F32
         ).astype(BF16)
-        for q in range(QUARTERS):
-            rows_ref[g * 32 : (g + 1) * 32, q * part : (q + 1) * part] = block[q * 32 : (q + 1) * 32]
+        for slot in range(CAP):
+            first = slot * peers + g * group
+            for chunk in range(halves * CHUNKS):
+                lane = (slot * halves + chunk // CHUNKS) * 128
+                row = chunk % CHUNKS * group
+                rows_ref[first : first + group, chunk * 128 : (chunk + 1) * 128] = block[
+                    row : row + group, lane : lane + 128
+                ]
+
+
+def unfold_slots(wire_ref, rows_ref, slots):
+    peers = wire_ref.shape[0] // CHUNKS
+    halves = rows_ref.shape[1] // (CHUNKS * 128)
+    for slot in slots:
+        for half in range(halves):
+            lane = (slot * halves + half) * 128
+            block = wire_ref[:, lane : lane + 128].astype(F32).reshape(peers, CHUNKS, 128)
+            chunks = jnp.swapaxes(block, 0, 1).astype(BF16)
+            for n in range(CHUNKS):
+                at = (half * CHUNKS + n) * 128
+                rows_ref[slot * peers : (slot + 1) * peers, at : at + 128] = chunks[n]
 
 
 def project_kernel(columns_ref, heads_ref, *refs):
@@ -296,17 +315,12 @@
     normed_ref[...] = normed
     copies[7].start()
     copies[8].start()
-    span = place_ref.shape[0] // PAIRS
-    part = normed.shape[1] // QUARTERS
-    for c in range(PAIRS):
-        slots = jnp.dot(
-            place_ref[c * span : (c + 1) * span, :], normed, preferred_element_type=F32
-        ).astype(BF16)
-
-        def write(g, block):
-            wire_ref[g * 128 : (g + 1) * 128, c * part : (c + 1) * part] = block
-
-        fold(slots, write)
+    peers = place_ref.shape[0] // CAP
+    for slot in range(CAP):
+        rows = jnp.dot(
+            place_ref[slot * peers : (slot + 1) * peers, :], normed, preferred_element_type=F32
+        )
+        fold(rows, wire_ref, slot)
     copies[7].wait()
     copies[8].wait()
 
@@ -349,31 +363,31 @@
 
 
 def expert_kernel(wire_ref, gate_ref, up_ref, down_ref, out_hbm, rows_ref, out_ref, sems):
-    part = wire_ref.shape[1] // PAIRS
-    span = rows_ref.shape[0] // PAIRS
-    for c in range(PAIRS):
-        unfold(
-            wire_ref.at[:, pl.ds(c * part, part)], rows_ref.at[pl.ds(c * span, span)]
-        )
-    rows = rows_ref[...]
-    gate = jnp.dot(rows, gate_ref[...], preferred_element_type=F32)
-    up = jnp.dot(rows, up_ref[...], preferred_element_type=F32)
-    hidden = (gate / (1.0 + jnp.exp(-gate)) * up).astype(BF16)
+    peers = rows_ref.shape[0] // CAP
+    part = out_ref.shape[1] // PAIRS
     copies = []
-    for c in range(PAIRS):
-        output = jnp.dot(
-            hidden[c * span : (c + 1) * span], down_ref[...], preferred_element_type=F32
-        ).astype(BF16)
-
-        def write(g, block):
-            out_ref[g * 128 : (g + 1) * 128, c * part : (c + 1) * part] = block
-
-        fold(output, write)
+
+    def finish(c, output):
+        fold(output[:peers], out_ref, 2 * c)
+        fold(output[peers:], out_ref, 2 * c + 1)
         lanes = pl.ds(c * part, part)
         copies.append(
             pltpu.make_async_copy(out_ref.at[:, lanes], out_hbm.at[:, lanes], sems.at[c])
         )
         copies[c].start()
+
+    def hidden_of(rows):
+        gate = jnp.dot(rows, gate_ref[...], preferred_element_type=F32)
+        up = jnp.dot(rows, up_ref[...], preferred_element_type=F32)
+        return (gate / (1.0 + jnp.exp(-gate)) * up).astype(BF16)
+
+    def output_of(hidden):
+        return jnp.dot(hidden, down_ref[...], preferred_element_type=F32)
+
+    unfold_slots(wire_ref, rows_ref, range(CAP))
+    hidden = hidden_of(rows_ref[...])
+    for c in range(PAIRS):
+        finish(c, output_of(hidden[c * 2 * peers : (c + 1) * 2 * peers]))
     for copy in copies:
         copy.wait()
 
@@ -446,12 +460,7 @@
     high = gates.astype(BF16)
     low = (gates - high.astype(F32)).astype(BF16)
     stacked = jnp.concatenate([high, low], axis=0)
-    part = wire_ref.shape[1] // PAIRS
-    span = rows_ref.shape[0] // PAIRS
-    for c in range(PAIRS):
-        unfold(
-            wire_ref.at[:, pl.ds(c * part, part)], rows_ref.at[pl.ds(c * span, span)]
-        )
+    unfold(wire_ref, rows_ref)
     fetch.wait()
     copies = []
     for n in range(blocks):

time: 185 us -> 184 us (level)
  no operation moved by 1% of the time
where the time goes in v5:
time: 184 us
  blocking collectives  69.8 us (38%)
  waiting for transfers between devices  57.9 us (31%)
  Pallas kernels  37.3 us (20%)
  starting transfers between devices  18.2 us (10%)
    all_to_all x1, blocking collectives, exchange(): lax.all_to_all(values.reshape(wire_shape), ('sp', 'dp'), split_axis=0, co...  45.9 us
    all_to_all x1, waiting for transfers between devices, exchange(): lax.all_to_all(values.reshape(wire_shape), ('sp', 'dp'), split_axis=0, co...  36.3 us
    all_to_all x1, blocking collectives, per_device(): lax.all_to_all(outgoing, 'sp', split_axis=0, concat_axis=0, tiled=True)  24 us
    ppermute x7, waiting for transfers between devices, shift(): return lax.ppermute(values, 'dp', [(d, place(d)) for d in range(size)])  11.6 us
    pallas_call x1, Pallas kernels, attend(): pl.pallas_call(attend_kernel, grid=(length // block,), in_specs=[pl.Block...  10.9 us
    ppermute x7, starting transfers between devices, shift(): return lax.ppermute(values, 'dp', [(d, place(d)) for d in range(size)])  9.99 us
    all_to_all x1, waiting for transfers between devices, per_device(): lax.all_to_all(attention.reshape(-1, tokens, attention.shape[1]), 'sp', s...  9.97 us
    pallas_call x1, Pallas kernels, expert(): pl.pallas_call(expert_kernel, in_specs=[vmem] * 4, out_specs=pl.BlockSpec...  7.74 us
  transfers between devices with their start and end apart: 9, of which 3 were waited for; matrix products, arithmetic and copies ran while one was open for 0% of the time, Pallas kernels for 11%

profile of v5, /device:TPU:1, one launch (start us, length us, event | category | flops | bytes accessed | tf_op | source)
XLA Modules:
  0.0 183.9 jit_solution(14153928068086149552)
XLA Ops:
  0.0 2.0 %collective-permute-start.1 = (bf16[2048,256]{1,0:T(8,128)(2,1)}, bf16[2048,256]{1,0:T(8,128)(2,1)S(1)}, u32[]{:S(2)}, u32[]{:S(2)}) collective-permute-start(bf16[2048,256]{1,0:T(8,128)(2,1)} %refs_0_.1), channel_id=1, source_target_pairs={{0,6},{1,3},{2,0},{3,5},{4,2},{5,7},{6,4},{7,1},{8,14},{9,11},{10,... | collective-permute-start | bytes 3145736 | tf_op jit(solution)/shard_map/ppermute | solution.py:506
  2.0 1.3 collective-permute-start
  3.3 3.1 %prepare.1 = bf16[16,128,256]{2,1,0:T(8,128)(2,1)S(1)} custom-call(s32[1]{0:T(128)} %bitcast.block_ref, bf16[128,16,128]{2,1,0:T(8,128)(2,1)} %bitcast.32, bf16[128,16,128]{2,1,0:T(8,128)(2,1)} %bitcast.33, f32[2,128,128]{2,1,0:T(8,128)} %constant.62.clone.col_ref, f32[16,2,2,128]{3,2,1,0:T(2,128)} %constant.63.clone.row_ref, f32[1,64]{1,0:T(1,128)} %bitcast.35, ...), custom_call_target="tpu_custom_call" | custom-call | tf_op jit(solution)/shard_map/prepare/pallas_call | solution.py:121
  6.4 24.0 %all_to_all.20 = bf16[16,128,256]{2,1,0:T(8,128)(2,1)S(1)} all-to-all(bf16[16,128,256]{2,1,0:T(8,128)(2,1)S(1)} %prepare.1), channel_id=1, replica_groups=mesh['sp'=16,'dp'=8] {'sp'}, dimensions={0} | all-to-all | bytes 2097152 | tf_op jit(solution)/shard_map/all_to_all | solution.py:546
  30.4 0.0 copy-start.4
  30.4 0.0 collective-permute-done.1.refs_1_
  30.4 0.1 collective-permute-start.5
  30.5 2.2 %collective-permute-start.2 = (bf16[2048,256]{1,0:T(8,128)(2,1)S(1)}, bf16[2048,256]{1,0:T(8,128)(2,1)}, u32[]{:S(2)}, u32[]{:S(2)}) collective-permute-start(bf16[2048,256]{1,0:T(8,128)(2,1)S(1)} %copy-done.3), channel_id=1, source_target_pairs={{0,1},{1,0},{2,3},{3,2},{4,5},{5,4},{6,7},{7,6},{8,9},{9,8},{10,11... | collective-permute-start | bytes 3145736 | tf_op jit(solution)/shard_map/ppermute | solution.py:506
  32.7 0.0 collective-permute-start.3
  32.7 0.5 collective-permute-start.4
  33.2 11.6 %collective-permute-done.5.refs_6_ = bf16[2048,256]{1,0:T(8,128)(2,1)} collective-permute-done((bf16[2048,256]{1,0:T(8,128)(2,1)}, bf16[2048,256]{1,0:T(8,128)(2,1)}, u32[]{:S(2)}, u32[]{:S(2)}) %collective-permute-start.5) | collective-permute-done | bytes 1048608 | tf_op jit(solution)/shard_map/ppermute | solution.py:506
  44.8 4.0 %collective-permute-start.6 = (bf16[2048,256]{1,0:T(8,128)(2,1)}, bf16[2048,256]{1,0:T(8,128)(2,1)}, u32[]{:S(2)}, u32[]{:S(2)}) collective-permute-start(bf16[2048,256]{1,0:T(8,128)(2,1)} %collective-permute-done.5.refs_6_), channel_id=1, source_target_pairs={{0,1},{1,0},{2,3},{3,2},{4,5},{5,4},{6,7},{7,6},{8,9},{9,8},{10,11... | collective-permute-start | bytes 3145736 | tf_op jit(solution)/shard_map/ppermute | solution.py:506
  48.7 10.9 %attend.1 = bf16[2048,128]{1,0:T(8,128)(2,1)} custom-call(bf16[2048,256]{1,0:T(8,128)(2,1)S(1)} %bitcast.21, bf16[2048,256]{1,0:T(8,128)(2,1)S(1)} %bitcast.22), custom_call_target="tpu_custom_call" | custom-call | tf_op jit(solution)/shard_map/attend/pallas_call | solution.py:188
  59.6 3.6 %all-to-all-start.1 = ((bf16[16,128,128]{2,1,0:T(8,128)(2,1)}), bf16[16,128,128]{2,1,0:T(8,128)(2,1)S(1)}, u32[]{:S(2)}, u32[]{:S(2)}) async-start(bf16[16,128,128]{2,1,0:T(8,128)(2,1)} %bitcast.31), calls=%async_computation.1 | async-start | bytes 1048576 | tf_op jit(solution)/shard_map/all_to_all | solution.py:551
  63.2 0.1 copy.20
  63.4 0.1 copy.21
  63.5 1.0 route.1
  64.5 0.0 collective-permute-done.2.refs_3_
  64.5 10.0 %all-to-all-done.1.heads_ref = bf16[16,128,128]{2,1,0:T(8,128)(2,1)S(1)} async-done(((bf16[16,128,128]{2,1,0:T(8,128)(2,1)}), bf16[16,128,128]{2,1,0:T(8,128)(2,1)S(1)}, u32[]{:S(2)}, u32[]{:S(2)}) %all-to-all-start.1) | async-done | bytes 524320 | tf_op jit(solution)/shard_map/all_to_all | solution.py:551
  74.5 0.0 collective-permute-done.4.refs_5_
  74.5 0.0 collective-permute-done.3.refs_4_
  74.5 0.0 collective-permute-done.6.refs_7_
  74.5 6.2 %project.1 = (f32[128,2048]{1,0:T(8,128)}, bf16[128,2048]{1,0:T(8,128)(2,1)}, bf16[1024,1536]{1,0:T(8,128)(2,1)S(1)}) custom-call(s32[8]{0:T(128)S(1)} %fusion.columns_ref, bf16[16,128,128]{2,1,0:T(8,128)(2,1)S(1)} %all-to-all-done.1.heads_ref, bf16[2048,256]{1,0:T(8,128)(2,1)S(1)} %copy-done.3, bf16[2048,256]{1,0:T(8,128)(2,1)S(1)} %collective-permute-done.1.refs_1_, ...), custom_call_target="tpu_custom_call" | custom-call | tf_op jit(solution)/shard_map/project/pallas_call | solution.py:332
  80.7 0.0 copy-start
  80.8 0.0 copy-start.1
  80.8 0.0 copy-start.2
  80.8 45.9 %all_to_all.21 = bf16[128,8,1536]{2,1,0:T(8,128)(2,1)S(1)} all-to-all(bf16[128,8,1536]{2,1,0:T(8,128)(2,1)S(1)} %bitcast.23), channel_id=1, replica_groups=mesh['sp'=16,'dp'=8] {'sp','dp'}, dimensions={0} | all-to-all | bytes 6291456 | tf_op jit(solution)/shard_map/all_to_all | solution.py:575
  126.7 7.7 %expert.1 = bf16[1024,1536]{1,0:T(8,128)(2,1)} custom-call(bf16[1024,1536]{1,0:T(8,128)(2,1)S(1)} %bitcast.20, bf16[2048,512]{1,0:T(8,128)(2,1)S(1)} %bitcast.24, bf16[2048,512]{1,0:T(8,128)(2,1)S(1)} %bitcast.25, bf16[512,2048]{1,0:T(8,128)(2,1)S(1)} %bitcast.26), custom_call_target="tpu_custom_call" | custom-call | tf_op jit(solution)/shard_map/expert/pallas_call | solution.py:398
  134.4 4.7 %all-to-all-start.3 = ((bf16[128,8,1536]{2,1,0:T(8,128)(2,1)}), bf16[128,8,1536]{2,1,0:T(8,128)(2,1)S(1)}, u32[]{:S(2)}, u32[]{:S(2)}) async-start(bf16[128,8,1536]{2,1,0:T(8,128)(2,1)} %bitcast.30), calls=%async_computation.3 | async-start | bytes 6291456 | tf_op jit(solution)/shard_map/all_to_all | solution.py:575
  139.1 5.3 %shared.1.base_hbm = f32[128,2048]{1,0:T(8,128)} custom-call(bf16[128,2048]{1,0:T(8,128)(2,1)} %get-tuple-element.19.normed_ref, f32[128,2048]{1,0:T(8,128)} %get-tuple-element.20.mixed_ref, bf16[2048,512]{1,0:T(8,128)(2,1)} %gate_ref.1, bf16[2048,512]{1,0:T(8,128)(2,1)} %up_ref.1, bf16[512,2048]{1,0:T(8,128)(2,1)} %down_ref.1), custom_call_target="tpu_custom_call" | custom-call | tf_op jit(solution)/shard_map/shared/pallas_call | solution.py:436
  144.4 36.3 %all-to-all-done.3 = bf16[128,8,1536]{2,1,0:T(8,128)(2,1)S(1)} async-done(((bf16[128,8,1536]{2,1,0:T(8,128)(2,1)}), bf16[128,8,1536]{2,1,0:T(8,128)(2,1)S(1)}, u32[]{:S(2)}, u32[]{:S(2)}) %all-to-all-start.3) | async-done | bytes 3145760 | tf_op jit(solution)/shard_map/all_to_all | solution.py:575
  180.7 3.1 %combine.1 = bf16[128,2048]{1,0:T(8,128)(2,1)} custom-call(bf16[1024,1536]{1,0:T(8,128)(2,1)S(1)} %bitcast.19, f32[128,768]{1,0:T(8,128)S(1)} %get-tuple-element.18.gates_ref, f32[128,2048]{1,0:T(8,128)} %shared.1.base_hbm), custom_call_target="tpu_custom_call" | custom-call | tf_op jit(solution)/shard_map/combine/pallas_call | solution.py:483
  (16 shorter events, 0.0 us)
Async XLA Ops:
  0.0 30.4 %collective-permute-start.1 = (bf16[2048,256]{1,0:T(8,128)(2,1)}, bf16[2048,256]{1,0:T(8,128)(2,1)S(1)}, u32[]{:S(2)}, u32[]{:S(2)}) collective-permute-start(bf16[2048,256]{1,0:T(8,128)(2,1)} %refs_0_.1), channel_id=1, source_target_pairs={{0,6},{1,3},{2,0},{3,5},{4,2},{5,7},{6,4},{7,1},{8,14},{9,11},{10,... | collective-permute-start | bytes 3145736 | tf_op jit(solution)/shard_map/ppermute | solution.py:506
  2.0 28.4 %collective-permute-start = (bf16[2048,256]{1,0:T(8,128)(2,1)}, bf16[2048,256]{1,0:T(8,128)(2,1)}, u32[]{:S(2)}, u32[]{:S(2)}) collective-permute-start(bf16[2048,256]{1,0:T(8,128)(2,1)} %refs_0_.1), channel_id=1, source_target_pairs={{0,2},{1,7},{2,4},{3,1},{4,6},{5,3},{6,0},{7,5},{8,10},{9,15},{10,... | collective-permute-start | bytes 3145736 | tf_op jit(solution)/shard_map/ppermute | solution.py:506
  3.3 27.2 %copy-start.3 = (bf16[2048,256]{1,0:T(8,128)(2,1)S(1)}, bf16[2048,256]{1,0:T(8,128)(2,1)}, u32[]{:S(2)}) copy-start(bf16[2048,256]{1,0:T(8,128)(2,1)} %refs_0_.1) | copy-start | bytes 3145732
  30.4 32.8 %copy-start.5 = (s32[1,128,4]{1,2,0:T(4,128)S(1)}, s32[1,128,4]{1,2,0:T(4,128)}, u32[]{:S(2)}) copy-start(s32[1,128,4]{1,2,0:T(4,128)} %param.26) | copy-start | bytes 6148
  30.4 33.0 %copy-start.6 = (f32[1,128,4]{1,2,0:T(4,128)S(1)}, f32[1,128,4]{1,2,0:T(4,128)}, u32[]{:S(2)}) copy-start(f32[1,128,4]{1,2,0:T(4,128)} %param.27) | copy-start | bytes 6148
  30.4 34.0 %copy-start.7 = (s32[8]{0:T(128)S(1)}, s32[8]{0:T(128)}, u32[]{:S(2)}) copy-start(s32[8]{0:T(128)} %constant.65.clone) | copy-start | bytes 100
  30.4 34.1 %copy-start.8 = (s32[8]{0:T(128)S(1)}, s32[8]{0:T(128)}, u32[]{:S(2)}) copy-start(s32[8]{0:T(128)} %constant.64.clone) | copy-start | bytes 100
  30.4 44.1 %copy-start.4 = (f32[2048]{0:T(1024)S(1)}, f32[2048]{0:T(1024)}, u32[]{:S(2)}) copy-start(f32[2048]{0:T(1024)} %param.23) | copy-start | bytes 24580
  30.4 14.3 %collective-permute-start.5 = (bf16[2048,256]{1,0:T(8,128)(2,1)}, bf16[2048,256]{1,0:T(8,128)(2,1)}, u32[]{:S(2)}, u32[]{:S(2)}) collective-permute-start(bf16[2048,256]{1,0:T(8,128)(2,1)} %collective-permute-done.refs_2_), channel_id=1, source_target_pairs={{0,2},{1,7},{2,4},{3,1},{4,6},{5,3},{6,0},{7,5},{8,10},{9,15},{10,... | collective-permute-start | bytes 3145736 | tf_op jit(solution)/shard_map/ppermute | solution.py:506
  30.5 34.0 %collective-permute-start.2 = (bf16[2048,256]{1,0:T(8,128)(2,1)S(1)}, bf16[2048,256]{1,0:T(8,128)(2,1)}, u32[]{:S(2)}, u32[]{:S(2)}) collective-permute-start(bf16[2048,256]{1,0:T(8,128)(2,1)S(1)} %copy-done.3), channel_id=1, source_target_pairs={{0,1},{1,0},{2,3},{3,2},{4,5},{5,4},{6,7},{7,6},{8,9},{9,8},{10,11... | collective-permute-start | bytes 3145736 | tf_op jit(solution)/shard_map/ppermute | solution.py:506
  32.7 41.8 %collective-permute-start.3 = (bf16[2048,256]{1,0:T(8,128)(2,1)}, bf16[2048,256]{1,0:T(8,128)(2,1)}, u32[]{:S(2)}, u32[]{:S(2)}) collective-permute-start(bf16[2048,256]{1,0:T(8,128)(2,1)} %collective-permute-done.refs_2_), channel_id=1, source_target_pairs={{0,1},{1,0},{2,3},{3,2},{4,5},{5,4},{6,7},{7,6},{8,9},{9,8},{10,11... | collective-permute-start | bytes 3145736 | tf_op jit(solution)/shard_map/ppermute | solution.py:506
  32.7 41.8 %collective-permute-start.4 = (bf16[2048,256]{1,0:T(8,128)(2,1)S(1)}, bf16[2048,256]{1,0:T(8,128)(2,1)}, u32[]{:S(2)}, u32[]{:S(2)}) collective-permute-start(bf16[2048,256]{1,0:T(8,128)(2,1)S(1)} %collective-permute-done.1.refs_1_), channel_id=1, source_target_pairs={{0,1},{1,0},{2,3},{3,2},{4,5},{5,4},{6,7},{7,6},{8,9},{9,8},{10,11... | collective-permute-start | bytes 3145736 | tf_op jit(solution)/shard_map/ppermute | solution.py:506
  44.8 29.7 %collective-permute-start.6 = (bf16[2048,256]{1,0:T(8,128)(2,1)}, bf16[2048,256]{1,0:T(8,128)(2,1)}, u32[]{:S(2)}, u32[]{:S(2)}) collective-permute-start(bf16[2048,256]{1,0:T(8,128)(2,1)} %collective-permute-done.5.refs_6_), channel_id=1, source_target_pairs={{0,1},{1,0},{2,3},{3,2},{4,5},{5,4},{6,7},{7,6},{8,9},{9,8},{10,11... | collective-permute-start | bytes 3145736 | tf_op jit(solution)/shard_map/ppermute | solution.py:506
  59.6 14.8 %all-to-all-start.1 = ((bf16[16,128,128]{2,1,0:T(8,128)(2,1)}), bf16[16,128,128]{2,1,0:T(8,128)(2,1)S(1)}, u32[]{:S(2)}, u32[]{:S(2)}) async-start(bf16[16,128,128]{2,1,0:T(8,128)(2,1)} %bitcast.31), calls=%async_computation.1 | async-start | bytes 1048576 | tf_op jit(solution)/shard_map/all_to_all | solution.py:551
  80.7 45.9 %copy-start = (bf16[1,2048,512]{2,1,0:T(8,128)(2,1)S(1)}, bf16[1,2048,512]{2,1,0:T(8,128)(2,1)}, u32[]{:S(2)}) copy-start(bf16[1,2048,512]{2,1,0:T(8,128)(2,1)} %param.31) | copy-start | bytes 6291460
  80.8 45.9 %copy-start.1 = (bf16[1,2048,512]{2,1,0:T(8,128)(2,1)S(1)}, bf16[1,2048,512]{2,1,0:T(8,128)(2,1)}, u32[]{:S(2)}) copy-start(bf16[1,2048,512]{2,1,0:T(8,128)(2,1)} %param.32) | copy-start | bytes 6291460
  80.8 45.9 %copy-start.2 = (bf16[1,512,2048]{2,1,0:T(8,128)(2,1)S(1)}, bf16[1,512,2048]{2,1,0:T(8,128)(2,1)}, u32[]{:S(2)}) copy-start(bf16[1,512,2048]{2,1,0:T(8,128)(2,1)} %param.33) | copy-start | bytes 6291460
  134.4 46.3 %all-to-all-start.3 = ((bf16[128,8,1536]{2,1,0:T(8,128)(2,1)}), bf16[128,8,1536]{2,1,0:T(8,128)(2,1)S(1)}, u32[]{:S(2)}, u32[]{:S(2)}) async-start(bf16[128,8,1536]{2,1,0:T(8,128)(2,1)} %bitcast.30), calls=%async_computation.3 | async-start | bytes 6291456 | tf_op jit(solution)/shard_map/all_to_all | solution.py:575

commit v6 on v5

--- a/solution.py
+++ b/solution.py
@@ -153,7 +153,7 @@
         values_ref[:, 128:] = jnp.ones_like(values_ref[:, 128:])
 
     first = iota((1, 128), 1) < HD
-    block = 512
+    block = 1024
     parts = [(r, head) for r in range(q_ref.shape[0] // block) for head in range(2)]
 
     def score(part):
@@ -184,7 +184,7 @@
 
 def attend(rows):
     length, width = rows.shape
-    block = 512
+    block = 1024
     return pl.pallas_call(
         attend_kernel,
         grid=(length // block,),
@@ -195,7 +195,7 @@
         out_specs=pl.BlockSpec((block, 128), lambda i: (i, 0)),
         out_shape=pltpu.HBM((length, 128), BF16),
         scratch_shapes=[pltpu.VMEM((length, 128), BF16), pltpu.VMEM((length, 256), BF16)],
-        compiler_params=limit(24),
+        compiler_params=limit(32),
         name="attend",
     )(rows, rows)
 

time: 184 us -> 184 us (level)
  no operation moved by 1% of the time
where the time goes in v6:
time: 184 us; the launch traced here: 183 us
  blocking collectives  69.8 us (38%)
  waiting for transfers between devices  57.7 us (31%)
  Pallas kernels  36.8 us (20%)
  starting transfers between devices  18.4 us (10%)
    all_to_all x1, blocking collectives, exchange(): lax.all_to_all(values.reshape(wire_shape), ('sp', 'dp'), split_axis=0, co...  45.9 us
    all_to_all x1, waiting for transfers between devices, exchange(): lax.all_to_all(values.reshape(wire_shape), ('sp', 'dp'), split_axis=0, co...  36.3 us
    all_to_all x1, blocking collectives, per_device(): lax.all_to_all(outgoing, 'sp', split_axis=0, concat_axis=0, tiled=True)  24 us
    ppermute x7, waiting for transfers between devices, shift(): return lax.ppermute(values, 'dp', [(d, place(d)) for d in range(size)])  11.6 us
    pallas_call x1, Pallas kernels, attend(): pl.pallas_call(attend_kernel, grid=(length // block,), in_specs=[pl.Block...  10.4 us
    ppermute x7, starting transfers between devices, shift(): return lax.ppermute(values, 'dp', [(d, place(d)) for d in range(size)])  9.99 us
    all_to_all x1, waiting for transfers between devices, per_device(): lax.all_to_all(attention.reshape(-1, tokens, attention.shape[1]), 'sp', s...  9.8 us
    pallas_call x1, Pallas kernels, expert(): pl.pallas_call(expert_kernel, in_specs=[vmem] * 4, out_specs=pl.BlockSpec...  7.74 us
  transfers between devices with their start and end apart: 9, of which 3 were waited for; matrix products, arithmetic and copies ran while one was open for 0% of the time, Pallas kernels for 11%

profile of v6, /device:TPU:1, one launch (start us, length us, event | category | flops | bytes accessed | tf_op | source)
XLA Modules:
  0.0 183.5 jit_solution(184374032708748919)
XLA Ops:
  0.0 2.0 %collective-permute-start.1 = (bf16[2048,256]{1,0:T(8,128)(2,1)}, bf16[2048,256]{1,0:T(8,128)(2,1)S(1)}, u32[]{:S(2)}, u32[]{:S(2)}) collective-permute-start(bf16[2048,256]{1,0:T(8,128)(2,1)} %refs_0_.1), channel_id=1, source_target_pairs={{0,6},{1,3},{2,0},{3,5},{4,2},{5,7},{6,4},{7,1},{8,14},{9,11},{10,... | collective-permute-start | bytes 3145736 | tf_op jit(solution)/shard_map/ppermute | solution.py:506
  2.0 1.3 collective-permute-start
  3.3 3.1 %prepare.1 = bf16[16,128,256]{2,1,0:T(8,128)(2,1)S(1)} custom-call(s32[1]{0:T(128)} %bitcast.block_ref, bf16[128,16,128]{2,1,0:T(8,128)(2,1)} %bitcast.32, bf16[128,16,128]{2,1,0:T(8,128)(2,1)} %bitcast.33, f32[2,128,128]{2,1,0:T(8,128)} %constant.62.clone.col_ref, f32[16,2,2,128]{3,2,1,0:T(2,128)} %constant.63.clone.row_ref, f32[1,64]{1,0:T(1,128)} %bitcast.35, ...), custom_call_target="tpu_custom_call" | custom-call | tf_op jit(solution)/shard_map/prepare/pallas_call | solution.py:121
  6.4 24.0 %all_to_all.20 = bf16[16,128,256]{2,1,0:T(8,128)(2,1)S(1)} all-to-all(bf16[16,128,256]{2,1,0:T(8,128)(2,1)S(1)} %prepare.1), channel_id=1, replica_groups=mesh['sp'=16,'dp'=8] {'sp'}, dimensions={0} | all-to-all | bytes 2097152 | tf_op jit(solution)/shard_map/all_to_all | solution.py:546
  30.4 0.0 copy-start.4
  30.4 0.0 collective-permute-done.1.refs_1_
  30.4 0.0 collective-permute-done.refs_2_
  30.4 0.1 collective-permute-start.5
  30.5 2.2 %collective-permute-start.2 = (bf16[2048,256]{1,0:T(8,128)(2,1)S(1)}, bf16[2048,256]{1,0:T(8,128)(2,1)}, u32[]{:S(2)}, u32[]{:S(2)}) collective-permute-start(bf16[2048,256]{1,0:T(8,128)(2,1)S(1)} %copy-done.3), channel_id=1, source_target_pairs={{0,1},{1,0},{2,3},{3,2},{4,5},{5,4},{6,7},{7,6},{8,9},{9,8},{10,11... | collective-permute-start | bytes 3145736 | tf_op jit(solution)/shard_map/ppermute | solution.py:506
  32.7 0.0 collective-permute-start.3
  32.7 0.5 collective-permute-start.4
  33.2 11.6 %collective-permute-done.5.refs_6_ = bf16[2048,256]{1,0:T(8,128)(2,1)} collective-permute-done((bf16[2048,256]{1,0:T(8,128)(2,1)}, bf16[2048,256]{1,0:T(8,128)(2,1)}, u32[]{:S(2)}, u32[]{:S(2)}) %collective-permute-start.5) | collective-permute-done | bytes 1048608 | tf_op jit(solution)/shard_map/ppermute | solution.py:506
  44.8 4.0 %collective-permute-start.6 = (bf16[2048,256]{1,0:T(8,128)(2,1)}, bf16[2048,256]{1,0:T(8,128)(2,1)}, u32[]{:S(2)}, u32[]{:S(2)}) collective-permute-start(bf16[2048,256]{1,0:T(8,128)(2,1)} %collective-permute-done.5.refs_6_), channel_id=1, source_target_pairs={{0,1},{1,0},{2,3},{3,2},{4,5},{5,4},{6,7},{7,6},{8,9},{9,8},{10,11... | collective-permute-start | bytes 3145736 | tf_op jit(solution)/shard_map/ppermute | solution.py:506
  48.7 10.4 %attend.1 = bf16[2048,128]{1,0:T(8,128)(2,1)} custom-call(bf16[2048,256]{1,0:T(8,128)(2,1)S(1)} %bitcast.21, bf16[2048,256]{1,0:T(8,128)(2,1)S(1)} %bitcast.22), custom_call_target="tpu_custom_call" | custom-call | tf_op jit(solution)/shard_map/attend/pallas_call | solution.py:188
  59.2 3.8 %all-to-all-start.1 = ((bf16[16,128,128]{2,1,0:T(8,128)(2,1)}), bf16[16,128,128]{2,1,0:T(8,128)(2,1)S(1)}, u32[]{:S(2)}, u32[]{:S(2)}) async-start(bf16[16,128,128]{2,1,0:T(8,128)(2,1)} %bitcast.31), calls=%async_computation.1 | async-start | bytes 1048576 | tf_op jit(solution)/shard_map/all_to_all | solution.py:551
  63.0 0.1 copy.20
  63.1 0.1 copy.21
  63.2 1.0 route.1
  64.2 9.8 %all-to-all-done.1.heads_ref = bf16[16,128,128]{2,1,0:T(8,128)(2,1)S(1)} async-done(((bf16[16,128,128]{2,1,0:T(8,128)(2,1)}), bf16[16,128,128]{2,1,0:T(8,128)(2,1)S(1)}, u32[]{:S(2)}, u32[]{:S(2)}) %all-to-all-start.1) | async-done | bytes 524320 | tf_op jit(solution)/shard_map/all_to_all | solution.py:551
  74.0 0.0 collective-permute-done.4.refs_5_
  74.0 0.0 collective-permute-done.3.refs_4_
  74.0 0.0 collective-permute-done.6.refs_7_
  74.0 6.2 %project.1 = (f32[128,2048]{1,0:T(8,128)}, bf16[128,2048]{1,0:T(8,128)(2,1)}, bf16[1024,1536]{1,0:T(8,128)(2,1)S(1)}) custom-call(s32[8]{0:T(128)S(1)} %fusion.columns_ref, bf16[16,128,128]{2,1,0:T(8,128)(2,1)S(1)} %all-to-all-done.1.heads_ref, bf16[2048,256]{1,0:T(8,128)(2,1)S(1)} %copy-done.3, bf16[2048,256]{1,0:T(8,128)(2,1)S(1)} %collective-permute-done.1.refs_1_, ...), custom_call_target="tpu_custom_call" | custom-call | tf_op jit(solution)/shard_map/project/pallas_call | solution.py:332
  80.3 0.0 copy-start
  80.3 0.0 copy-start.1
  80.3 0.0 copy-start.2
  80.3 45.9 %all_to_all.21 = bf16[128,8,1536]{2,1,0:T(8,128)(2,1)S(1)} all-to-all(bf16[128,8,1536]{2,1,0:T(8,128)(2,1)S(1)} %bitcast.23), channel_id=1, replica_groups=mesh['sp'=16,'dp'=8] {'sp','dp'}, dimensions={0} | all-to-all | bytes 6291456 | tf_op jit(solution)/shard_map/all_to_all | solution.py:575
  126.2 7.7 %expert.1 = bf16[1024,1536]{1,0:T(8,128)(2,1)} custom-call(bf16[1024,1536]{1,0:T(8,128)(2,1)S(1)} %bitcast.20, bf16[2048,512]{1,0:T(8,128)(2,1)S(1)} %bitcast.24, bf16[2048,512]{1,0:T(8,128)(2,1)S(1)} %bitcast.25, bf16[512,2048]{1,0:T(8,128)(2,1)S(1)} %bitcast.26), custom_call_target="tpu_custom_call" | custom-call | tf_op jit(solution)/shard_map/expert/pallas_call | solution.py:398
  133.9 4.7 %all-to-all-start.3 = ((bf16[128,8,1536]{2,1,0:T(8,128)(2,1)}), bf16[128,8,1536]{2,1,0:T(8,128)(2,1)S(1)}, u32[]{:S(2)}, u32[]{:S(2)}) async-start(bf16[128,8,1536]{2,1,0:T(8,128)(2,1)} %bitcast.30), calls=%async_computation.3 | async-start | bytes 6291456 | tf_op jit(solution)/shard_map/all_to_all | solution.py:575
  138.6 5.3 %shared.1.base_hbm = f32[128,2048]{1,0:T(8,128)} custom-call(bf16[128,2048]{1,0:T(8,128)(2,1)} %get-tuple-element.19.normed_ref, f32[128,2048]{1,0:T(8,128)} %get-tuple-element.20.mixed_ref, bf16[2048,512]{1,0:T(8,128)(2,1)} %gate_ref.1, bf16[2048,512]{1,0:T(8,128)(2,1)} %up_ref.1, bf16[512,2048]{1,0:T(8,128)(2,1)} %down_ref.1), custom_call_target="tpu_custom_call" | custom-call | tf_op jit(solution)/shard_map/shared/pallas_call | solution.py:436
  143.9 36.3 %all-to-all-done.3 = bf16[128,8,1536]{2,1,0:T(8,128)(2,1)S(1)} async-done(((bf16[128,8,1536]{2,1,0:T(8,128)(2,1)}), bf16[128,8,1536]{2,1,0:T(8,128)(2,1)S(1)}, u32[]{:S(2)}, u32[]{:S(2)}) %all-to-all-start.3) | async-done | bytes 3145760 | tf_op jit(solution)/shard_map/all_to_all | solution.py:575
  180.2 3.1 %combine.1 = bf16[128,2048]{1,0:T(8,128)(2,1)} custom-call(bf16[1024,1536]{1,0:T(8,128)(2,1)S(1)} %bitcast.19, f32[128,768]{1,0:T(8,128)S(1)} %get-tuple-element.18.gates_ref, f32[128,2048]{1,0:T(8,128)} %shared.1.base_hbm), custom_call_target="tpu_custom_call" | custom-call | tf_op jit(solution)/shard_map/combine/pallas_call | solution.py:483
  (16 shorter events, 0.0 us)
Async XLA Ops:
  0.0 30.4 %collective-permute-start.1 = (bf16[2048,256]{1,0:T(8,128)(2,1)}, bf16[2048,256]{1,0:T(8,128)(2,1)S(1)}, u32[]{:S(2)}, u32[]{:S(2)}) collective-permute-start(bf16[2048,256]{1,0:T(8,128)(2,1)} %refs_0_.1), channel_id=1, source_target_pairs={{0,6},{1,3},{2,0},{3,5},{4,2},{5,7},{6,4},{7,1},{8,14},{9,11},{10,... | collective-permute-start | bytes 3145736 | tf_op jit(solution)/shard_map/ppermute | solution.py:506
  2.0 28.4 %collective-permute-start = (bf16[2048,256]{1,0:T(8,128)(2,1)}, bf16[2048,256]{1,0:T(8,128)(2,1)}, u32[]{:S(2)}, u32[]{:S(2)}) collective-permute-start(bf16[2048,256]{1,0:T(8,128)(2,1)} %refs_0_.1), channel_id=1, source_target_pairs={{0,2},{1,7},{2,4},{3,1},{4,6},{5,3},{6,0},{7,5},{8,10},{9,15},{10,... | collective-permute-start | bytes 3145736 | tf_op jit(solution)/shard_map/ppermute | solution.py:506
  3.3 27.2 %copy-start.3 = (bf16[2048,256]{1,0:T(8,128)(2,1)S(1)}, bf16[2048,256]{1,0:T(8,128)(2,1)}, u32[]{:S(2)}) copy-start(bf16[2048,256]{1,0:T(8,128)(2,1)} %refs_0_.1) | copy-start | bytes 3145732
  30.4 32.5 %copy-start.5 = (s32[1,128,4]{1,2,0:T(4,128)S(1)}, s32[1,128,4]{1,2,0:T(4,128)}, u32[]{:S(2)}) copy-start(s32[1,128,4]{1,2,0:T(4,128)} %param.26) | copy-start | bytes 6148
  30.4 32.7 %copy-start.6 = (f32[1,128,4]{1,2,0:T(4,128)S(1)}, f32[1,128,4]{1,2,0:T(4,128)}, u32[]{:S(2)}) copy-start(f32[1,128,4]{1,2,0:T(4,128)} %param.27) | copy-start | bytes 6148
  30.4 33.8 %copy-start.7 = (s32[8]{0:T(128)S(1)}, s32[8]{0:T(128)}, u32[]{:S(2)}) copy-start(s32[8]{0:T(128)} %constant.65.clone) | copy-start | bytes 100
  30.4 33.8 %copy-start.8 = (s32[8]{0:T(128)S(1)}, s32[8]{0:T(128)}, u32[]{:S(2)}) copy-start(s32[8]{0:T(128)} %constant.64.clone) | copy-start | bytes 100
  30.4 43.6 %copy-start.4 = (f32[2048]{0:T(1024)S(1)}, f32[2048]{0:T(1024)}, u32[]{:S(2)}) copy-start(f32[2048]{0:T(1024)} %param.23) | copy-start | bytes 24580
  30.4 14.3 %collective-permute-start.5 = (bf16[2048,256]{1,0:T(8,128)(2,1)}, bf16[2048,256]{1,0:T(8,128)(2,1)}, u32[]{:S(2)}, u32[]{:S(2)}) collective-permute-start(bf16[2048,256]{1,0:T(8,128)(2,1)} %collective-permute-done.refs_2_), channel_id=1, source_target_pairs={{0,2},{1,7},{2,4},{3,1},{4,6},{5,3},{6,0},{7,5},{8,10},{9,15},{10,... | collective-permute-start | bytes 3145736 | tf_op jit(solution)/shard_map/ppermute | solution.py:506
  30.5 33.7 %collective-permute-start.2 = (bf16[2048,256]{1,0:T(8,128)(2,1)S(1)}, bf16[2048,256]{1,0:T(8,128)(2,1)}, u32[]{:S(2)}, u32[]{:S(2)}) collective-permute-start(bf16[2048,256]{1,0:T(8,128)(2,1)S(1)} %copy-done.3), channel_id=1, source_target_pairs={{0,1},{1,0},{2,3},{3,2},{4,5},{5,4},{6,7},{7,6},{8,9},{9,8},{10,11... | collective-permute-start | bytes 3145736 | tf_op jit(solution)/shard_map/ppermute | solution.py:506
  32.7 41.3 %collective-permute-start.3 = (bf16[2048,256]{1,0:T(8,128)(2,1)}, bf16[2048,256]{1,0:T(8,128)(2,1)}, u32[]{:S(2)}, u32[]{:S(2)}) collective-permute-start(bf16[2048,256]{1,0:T(8,128)(2,1)} %collective-permute-done.refs_2_), channel_id=1, source_target_pairs={{0,1},{1,0},{2,3},{3,2},{4,5},{5,4},{6,7},{7,6},{8,9},{9,8},{10,11... | collective-permute-start | bytes 3145736 | tf_op jit(solution)/shard_map/ppermute | solution.py:506
  32.7 41.3 %collective-permute-start.4 = (bf16[2048,256]{1,0:T(8,128)(2,1)S(1)}, bf16[2048,256]{1,0:T(8,128)(2,1)}, u32[]{:S(2)}, u32[]{:S(2)}) collective-permute-start(bf16[2048,256]{1,0:T(8,128)(2,1)S(1)} %collective-permute-done.1.refs_1_), channel_id=1, source_target_pairs={{0,1},{1,0},{2,3},{3,2},{4,5},{5,4},{6,7},{7,6},{8,9},{9,8},{10,11... | collective-permute-start | bytes 3145736 | tf_op jit(solution)/shard_map/ppermute | solution.py:506
  44.8 29.3 %collective-permute-start.6 = (bf16[2048,256]{1,0:T(8,128)(2,1)}, bf16[2048,256]{1,0:T(8,128)(2,1)}, u32[]{:S(2)}, u32[]{:S(2)}) collective-permute-start(bf16[2048,256]{1,0:T(8,128)(2,1)} %collective-permute-done.5.refs_6_), channel_id=1, source_target_pairs={{0,1},{1,0},{2,3},{3,2},{4,5},{5,4},{6,7},{7,6},{8,9},{9,8},{10,11... | collective-permute-start | bytes 3145736 | tf_op jit(solution)/shard_map/ppermute | solution.py:506
  59.2 14.9 %all-to-all-start.1 = ((bf16[16,128,128]{2,1,0:T(8,128)(2,1)}), bf16[16,128,128]{2,1,0:T(8,128)(2,1)S(1)}, u32[]{:S(2)}, u32[]{:S(2)}) async-start(bf16[16,128,128]{2,1,0:T(8,128)(2,1)} %bitcast.31), calls=%async_computation.1 | async-start | bytes 1048576 | tf_op jit(solution)/shard_map/all_to_all | solution.py:551
  80.3 45.9 %copy-start = (bf16[1,2048,512]{2,1,0:T(8,128)(2,1)S(1)}, bf16[1,2048,512]{2,1,0:T(8,128)(2,1)}, u32[]{:S(2)}) copy-start(bf16[1,2048,512]{2,1,0:T(8,128)(2,1)} %param.31) | copy-start | bytes 6291460
  80.3 45.9 %copy-start.1 = (bf16[1,2048,512]{2,1,0:T(8,128)(2,1)S(1)}, bf16[1,2048,512]{2,1,0:T(8,128)(2,1)}, u32[]{:S(2)}) copy-start(bf16[1,2048,512]{2,1,0:T(8,128)(2,1)} %param.32) | copy-start | bytes 6291460
  80.3 45.9 %copy-start.2 = (bf16[1,512,2048]{2,1,0:T(8,128)(2,1)S(1)}, bf16[1,512,2048]{2,1,0:T(8,128)(2,1)}, u32[]{:S(2)}) copy-start(bf16[1,512,2048]{2,1,0:T(8,128)(2,1)} %param.33) | copy-start | bytes 6291460
  133.9 46.3 %all-to-all-start.3 = ((bf16[128,8,1536]{2,1,0:T(8,128)(2,1)}), bf16[128,8,1536]{2,1,0:T(8,128)(2,1)S(1)}, u32[]{:S(2)}, u32[]{:S(2)}) async-start(bf16[128,8,1536]{2,1,0:T(8,128)(2,1)} %bitcast.30), calls=%async_computation.3 | async-start | bytes 6291456 | tf_op jit(solution)/shard_map/all_to_all | solution.py:575
